TPU v7x, 32 devices: a whole 2x2x4 slice. The times are simulated.
32 devices in a mesh: sp: 8 (over z, x), tp: 4 (over y, core).
Axes of the slice: x: 2, y: 2, z: 4, core: 2. Of those that a mesh axis runs over, the one named last changes fastest.
Arguments:
- tokens: bfloat16 [4096, 4096], P('sp', 'tp'), may hold values from -8 to 8
- w_key: bfloat16 [4096, 2048], P(None, 'tp'), may hold values from -0.09375 to 0.09375
- w_value: bfloat16 [4096, 2048], P(None, 'tp'), may hold values from -0.09375 to 0.09375
- w_beta: bfloat16 [4096, 16], replicated, may hold values from -0.09375 to 0.09375
- w_decay: bfloat16 [4096, 16], replicated, may hold values from -0.09375 to 0.09375
- beta_bias: float32 [16], replicated, may hold values from -6 to -4
- decay_rate: float32 [16], replicated, as said below
- forgetting_increment: float32 [16, 4096], P('tp', 'sp')
- new_query: bfloat16 [16, 128], P('tp', 'sp'), may hold values from -6 to 6
- read_gain: bfloat16 [128], replicated, may hold values from 0.099609375 to 1.8984375
Outputs:
- state_cache: bfloat16 [16, 128, 128], P('tp', 'sp')
- first_read: float32 [16, 128], P('tp')
Inputs may be any that keep to these rules, and one draw needn't show every extreme that they name: `decay_rate`: positive.
All inputs are finite; a program needn't handle non-finite values.
Results may differ from a plain program's by a relative error of at most 0.0075.
Values may be sent and summed in bfloat16 or wider, within the bound.
No kernel may reach another device: no remote copies, remote signals or barrier semaphores. Data moves between devices by JAX's collectives and lax.ppermute only.
A program may use at most 64 MiB of HBM per device.

v0:
```python
import functools

import jax
import jax.numpy as jnp
from jax import lax
from jax.experimental import pallas as pl
from jax.experimental.pallas import tpu as pltpu
from jax.sharding import PartitionSpec as P


DK = 128
DV = 128
CHUNK = 128
SUB = 8

norm_eps = 1e-06
bf16 = jnp.bfloat16
f32 = jnp.float32


def flip(axis, mask):
    return [(i, i ^ mask) for i in range(lax.axis_size(axis))]


def swap(x, axis, mask):
    return lax.ppermute(x, axis, flip(axis, mask))


def dot(left, right):
    return jnp.dot(left.astype(bf16), right.astype(bf16), preferred_element_type=f32)


def dot_exact(left, right):
    return jnp.dot(left, right, precision=lax.Precision.HIGHEST, preferred_element_type=f32)


def dot_nt(left, right):
    return lax.dot_general(
        left.astype(bf16), right.astype(bf16), (((1,), (1,)), ((), ())), preferred_element_type=f32
    )


def dot_tn(left, right):
    return lax.dot_general(
        left.astype(bf16), right.astype(bf16), (((0,), (0,)), ((), ())), preferred_element_type=f32
    )


def unit_inverses(lowers, size):
    row = lax.broadcasted_iota(jnp.int32, (size, size), 0)
    col = lax.broadcasted_iota(jnp.int32, (size, size), 1)
    identity = jnp.where(row == col, 1.0, 0.0)

    def same(width):
        return (row // width) == (col // width)

    width = min(16, size)
    inner = [jnp.where(same(width), low, 0.0) for low in lowers]
    results = [identity - low for low in inner]
    powers = inner
    covered = 2
    while covered < width:
        powers = [dot(p, p) for p in powers]
        results = [r + dot(r, p) for r, p in zip(results, powers)]
        covered *= 2
    while width < size:
        off = jnp.logical_and(same(2 * width), jnp.logical_not(same(width)))
        right = [dot(jnp.where(off, low, 0.0), r) for low, r in zip(lowers, results)]
        results = [r - dot(r, x) for r, x in zip(results, right)]
        width *= 2
    return results


def load_kernel(wk_hbm, wv_hbm, wk_ref, wv_ref, sems):
    copies = [
        pltpu.make_async_copy(wk_hbm, wk_ref, sems.at[0]),
        pltpu.make_async_copy(wv_hbm, wv_ref, sems.at[1]),
    ]
    for copy in copies:
        copy.start()
    for copy in copies:
        copy.wait()


def chunk_kernel(heads, index, last, masks, *refs):
    pieces = len(masks)
    piece_refs = refs[:pieces]
    wk_ref, wv_ref, wg_ref, small_ref, forget_ref = refs[pieces : pieces + 5]
    rest = refs[pieces + 5 :]
    if index > 0:
        state_ref, rest = rest[0], rest[1:]
    if last or index == 0:
        query_ref, rest = rest[0], rest[1:]
    if index == 0 and not last:
        rest[0][0:heads, :] = query_ref[...].astype(f32)
    size, width = piece_refs[0].shape
    rank = lax.axis_index("tp")
    starts = [pl.multiple_of((rank ^ m) * width, width) for m in masks]

    gates = None
    for start, piece_ref in zip(starts, piece_refs):
        g = dot_nt(wg_ref[:, pl.ds(start, width)], piece_ref[...])
        gates = g if gates is None else gates + g
    total_heads = heads * lax.axis_size("tp")
    lane = lax.broadcasted_iota(jnp.int32, (SUB, DK), 1)
    head = lax.broadcasted_iota(jnp.int32, (SUB, DK), 0) + rank * heads
    small = small_ref[0:1, :]
    bias = jnp.sum(jnp.where(lane == head, small, 0.0), axis=1, keepdims=True)
    rate = jnp.sum(jnp.where(lane == head + total_heads, small, 0.0), axis=1, keepdims=True)
    forget = forget_ref[:, index * size : (index + 1) * size]
    if heads < SUB:
        forget = jnp.concatenate([forget, jnp.zeros((SUB - heads, size), f32)], axis=0)
    beta_row = jax.nn.sigmoid(gates[0:SUB] + bias)
    log_row = forget - rate * jax.nn.softplus(gates[SUB : 2 * SUB])
    row = lax.broadcasted_iota(jnp.int32, (size, size), 0)
    col = lax.broadcasted_iota(jnp.int32, (size, size), 1)
    cum_row = dot_exact(log_row, jnp.where(row <= col, 1.0, 0.0))
    total = cum_row[:, size - 1 : size]
    stacked = jnp.concatenate(
        [
            beta_row,
            cum_row,
            beta_row * jnp.exp(cum_row),
            jnp.exp(total - cum_row),
            jnp.zeros((DK - 4 * SUB, size), f32),
        ],
        axis=0,
    )
    columns = stacked.T
    keep = jnp.exp(total)

    key_acc = value_acc = None
    for start, piece_ref in zip(starts, piece_refs):
        rows = pl.ds(start, width)
        x = piece_ref[...]
        k = jnp.dot(x, wk_ref[rows, :], preferred_element_type=f32)
        key_acc = k if key_acc is None else key_acc + k
    for start, piece_ref in zip(starts, piece_refs):
        rows = pl.ds(start, width)
        x = piece_ref[...]
        v = jnp.dot(x, wv_ref[rows, :], preferred_element_type=f32)
        value_acc = v if value_acc is None else value_acc + v
    key_raw = key_acc.astype(bf16).astype(f32)
    value_raw = value_acc.astype(bf16).astype(f32)

    strict = row > col
    keys, lowers, base = [], [], []
    for h in range(heads):
        kw = key_raw[:, h * DK : (h + 1) * DK]
        ku = kw * lax.rsqrt(jnp.sum(kw * kw, axis=-1, keepdims=True) + norm_eps)
        beta = columns[:, h : h + 1]
        cum = columns[:, SUB + h : SUB + h + 1]
        spread = jnp.where(strict, cum - cum_row[h : h + 1, :], 0.0)
        table = jnp.where(strict, jnp.exp(spread), 0.0)
        keys.append(ku)
        lowers.append(dot_nt(ku, ku) * table * beta)
    if index > 0:
        states = [state_ref[h] for h in range(heads)]
    else:
        kr = lax.broadcasted_iota(jnp.int32, (DK, DV + DK), 0)
        kc = lax.broadcasted_iota(jnp.int32, (DK, DV + DK), 1)
        states = [jnp.where(kc == kr + DV, 1.0, 0.0)] * heads
    for h in range(heads):
        beta = columns[:, h : h + 1]
        erase = keys[h] * columns[:, 2 * SUB + h : 2 * SUB + h + 1]
        value = value_raw[:, h * DV : (h + 1) * DV] * beta
        padded = jnp.concatenate([value, jnp.zeros((size, DK), f32)], axis=1)
        base.append(padded - dot(erase, states[h]))
    inverses = unit_inverses(lowers, size)
    fresh = [dot(inv, b) for inv, b in zip(inverses, base)]
    for h in range(heads):
        remain = keys[h] * columns[:, 3 * SUB + h : 3 * SUB + h + 1]
        new = keep[h : h + 1, :] * states[h] + dot_tn(remain, fresh[h])
        rest[-1][h] = new
    if last:
        lead = lax.axis_index("sp") % heads
        for k in range(heads):
            rest[k][0:DK, :] = rest[-1][lead ^ k].astype(bf16)
            asked = jnp.broadcast_to(query_ref[pl.ds(lead ^ k, 1), :].astype(f32), (2 * SUB, DK))
            asked = jnp.concatenate([asked, jnp.zeros((2 * SUB, DV), f32)], axis=1)
            rest[k][DK:, :] = asked.astype(bf16)


def compose(pairs):
    while len(pairs) > 1:
        merged = []
        for early, late in zip(pairs[0::2], pairs[1::2]):
            new = dot_exact(late[:, DV:], early)
            merged.append(
                jnp.concatenate([new[:, :DV] + late[:, :DV], new[:, DV:]], axis=1)
            )
        pairs = merged
    return pairs[0]


def split(x):
    high = x.astype(bf16)
    return high, (x - high.astype(f32)).astype(bf16)


def pad_rows(x, rows):
    return jnp.concatenate([x, jnp.zeros((rows - x.shape[0], x.shape[1]), x.dtype)], axis=0)


def message(high, own, query):
    half = DK // 2
    through = dot_exact(query, own)
    a, b = own[:, DV:], own[:, :DV]
    body = jnp.where(high, jnp.concatenate([a[:half], b[:half]], axis=0), b)
    ah, al = split(through[0:1, DV:])
    bh, bl = split(through[0:1, :DV])
    tail = pad_rows(jnp.concatenate([ah, al, bh, bl], axis=0).astype(f32), 16)
    return through, jnp.concatenate([body, tail], axis=0).astype(bf16)


def late_side(mask):
    return lax.rem(lax.div(lax.axis_index("sp"), jnp.int32(mask)), jnp.int32(2)) == 1


def finish(total, query, out):
    out[0][...] = total
    through, send = message(late_side(lax.axis_size("sp") // 2), total, query)
    out[1][...] = through
    if len(out) > 2:
        out[2][...] = send


def compose_kernel(heads, final, *refs):
    own_ref, got = refs[0], refs[1:heads]
    out, scratch = refs[heads:-1], refs[-1]
    lead = lax.axis_index("sp") % heads
    scratch[lead] = own_ref[:DK, :].astype(f32)
    query = own_ref[DK:, :DK].astype(f32)[:SUB]
    for k in range(1, heads):
        scratch[lead ^ k] = got[k - 1][:DK, :].astype(f32)
        query = query + got[k - 1][DK:, :DK].astype(f32)[:SUB]
    total = compose([scratch[i] for i in range(heads)])
    if final:
        finish(total, query, out)
    else:
        out[0][...] = total
        out[1][...] = query


def merge_kernel(mask, final, own_ref, got_ref, query_ref, *out):
    high = late_side(mask)
    own, got = own_ref[...], got_ref[...].astype(f32)
    early, late = jnp.where(high, got, own), jnp.where(high, own, got)
    total = compose([early, late])
    if final:
        finish(total, query_ref[...], out)
    else:
        out[0][...] = total
        out[1][...] = query_ref[...]


def rows_kernel(heads, groups, rows, own_ref, mine_ref, *refs):
    if groups > 1:
        got_ref, refs = refs[0], refs[1:]
    scratch = refs[-1]
    own, mine = own_ref[...], mine_ref[...]
    half = DK // 2
    place = lax.axis_index("sp")
    if groups > 1:
        high = late_side(lax.axis_size("sp") // 2)
        got = got_ref[...].astype(f32)
        a, b = own[:, DV:], own[:, :DV]
        early = jnp.where(high, got[:DK], b)
        late_a = jnp.where(high, a[half:], got[:half])
        late_b = jnp.where(high, b[half:], got[half:DK])
        through_a = jnp.where(high, mine[0:1, DV:], got[DK : DK + 1] + got[DK + 1 : DK + 2])
        through_b = jnp.where(high, mine[0:1, :DV], got[DK + 2 : DK + 3] + got[DK + 3 : DK + 4])
        both = dot_exact(pad_rows(jnp.concatenate([late_a, through_a], axis=0), half + 8), early)
        state = both[:half] + late_b
        read = both[half : half + 1] + through_b
    else:
        state = own[:, :DV]
        read = mine[0:1, :DV]
    members = state.shape[0] // rows
    for i in range(members):
        scratch[i] = state[i * rows : (i + 1) * rows]
    place = place % members
    rh, rl = split(read)
    tail = pad_rows(jnp.concatenate([rh, rl], axis=0).astype(f32), 16)
    for k in range(heads):
        body = scratch[place ^ k]
        refs[k][...] = jnp.concatenate([body, tail], axis=0).astype(bf16)


def final_kernel(heads, rows, small_ref, *refs):
    lead = lax.axis_index("sp") % heads
    state_ref, read_ref, scratch = refs[heads:]
    for k in range(heads):
        part = refs[k][...]
        state_ref[lead ^ k] = part[:rows]
        wide = part[rows : rows + 2].astype(f32)
        scratch[lead ^ k] = jnp.broadcast_to(wide[0:1] + wide[1:2], (SUB, DV))
    raw = jnp.concatenate([scratch[h][0:1] for h in range(heads)], axis=0)
    norm = lax.rsqrt(jnp.mean(raw * raw, axis=-1, keepdims=True) + norm_eps)
    read_ref[...] = raw * norm * small_ref[1:2, :]


def shape(dims, dtype=f32):
    return jax.ShapeDtypeStruct(dims, dtype)


vmem = pl.BlockSpec(memory_space=pltpu.VMEM)


def call(body, arrays, outs, scratch=(), mib=8, flops=0):
    return pl.pallas_call(
        body,
        out_shape=outs,
        in_specs=[vmem] * len(arrays),
        out_specs=jax.tree.map(lambda _: vmem, outs),
        scratch_shapes=list(scratch),
        compiler_params=pltpu.CompilerParams(vmem_limit_bytes=mib * 1024 * 1024),
        cost_estimate=pl.CostEstimate(flops=flops, bytes_accessed=0, transcendentals=0)
        if flops
        else None,
    )(*arrays)


def per_device(
    tokens,
    w_key,
    w_value,
    w_beta,
    w_decay,
    beta_bias,
    decay_rate,
    forgetting_increment,
    new_query,
    read_gain,
):
    heads = w_key.shape[1] // DK
    length, width = tokens.shape
    count, place = lax.axis_size("sp"), lax.axis_index("sp")
    ranks, rank = lax.axis_size("tp"), lax.axis_index("tp")
    groups = count // heads
    rows = DK // count
    chunk = min(CHUNK, length)
    chunks = length // chunk

    owns = [tokens[:chunk]]
    later = lax.optimization_barrier(tokens)
    owns += [later[c * chunk : (c + 1) * chunk] for c in range(1, chunks)]
    gathered = []
    for c in range(chunks):
        found = [(0, owns[c])]
        for hop in range(1, ranks // 2):
            found.append((2 * hop, swap(owns[c], "tp", 2 * hop)))
        found.append((1, swap(owns[c], "tp", 1)))
        found += [(m ^ 1, swap(x, "tp", 1)) for m, x in found[1:-1]]
        gathered.append(found)

    def head_rows(x):
        part = lax.dynamic_slice_in_dim(x.T, rank * heads, heads, 0)
        return jnp.pad(part, ((0, SUB - heads), (0, 0)))

    gate_weights = jnp.concatenate([head_rows(w_beta), head_rows(w_decay)], axis=0)
    named = jnp.concatenate([beta_bias, decay_rate])
    small = jnp.stack([jnp.pad(named, (0, DK - named.shape[0])), read_gain.astype(f32)])

    seat = lax.broadcasted_iota(jnp.int32, (heads, DK), 1) // rows
    query = jnp.where(seat == place, jnp.tile(new_query, (1, count)), jnp.zeros((), bf16))
    mask = heads
    while mask < count:
        query = query + swap(query, "sp", mask)
        mask *= 2

    w_key, w_value = pl.pallas_call(
        load_kernel,
        out_shape=[shape(w_key.shape, bf16), shape(w_value.shape, bf16)],
        in_specs=[pl.BlockSpec(memory_space=pltpu.HBM)] * 2,
        out_specs=[vmem] * 2,
        scratch_shapes=[pltpu.SemaphoreType.DMA((2,))],
        compiler_params=pltpu.CompilerParams(vmem_limit_bytes=20 * 1024 * 1024),
    )(*[pltpu.with_memory_space_constraint(w, pltpu.HBM) for w in (w_key, w_value)])

    state = None
    flops = 2 * chunk * width * ranks * (2 * heads * DK + DK) + heads * 24 * 2 * chunk * chunk * DK
    for c in range(chunks):
        found = gathered[c]
        last = c == chunks - 1
        arrays = [x for _, x in found] + [w_key, w_value, gate_weights, small, forgetting_increment]
        if c > 0:
            arrays.append(state)
        outs = [shape((heads, DK, DV + DK))]
        if last or c == 0:
            arrays.append(query)
        if last:
            outs = [shape((DK + 2 * SUB, DV + DK), bf16)] * heads + outs
        elif c == 0:
            outs = [shape((SUB, DK))] + outs
        result = call(
            functools.partial(chunk_kernel, heads, c, last, tuple(m for m, _ in found)),
            arrays,
            outs,
            mib=28,
            flops=flops,
        )
        state = result[-1]
        if c == 0 and not last:
            query = result[0]
    maps = result[:heads]

    got = {}
    for k in reversed(range(1, heads)):
        got[k] = swap(maps[k], "sp", k)
    done = [shape((DK, DV + DK)), shape((SUB, DV + DK))]
    if groups > 1:
        done.append(shape((DK + 16, DV), bf16))
    open_ended = [shape((DK, DV + DK)), shape((SUB, DK))]
    result = call(
        functools.partial(compose_kernel, heads, groups <= 2),
        [maps[0]] + [got[k] for k in range(1, heads)],
        done if groups <= 2 else open_ended,
        [pltpu.VMEM((heads, DK, DV + DK), f32)],
    )
    mask = heads
    while 2 * mask < count:
        final = 4 * mask == count
        partner = swap(result[0].astype(bf16), "sp", mask)
        result = call(
            functools.partial(merge_kernel, mask, final),
            [result[0], partner, result[1]],
            done if final else open_ended,
        )
        mask *= 2
    arrays = list(result[:2])
    if groups > 1:
        arrays.append(swap(result[2], "sp", count // 2))
    members = count // 2 if groups > 1 else count
    parts = call(
        functools.partial(rows_kernel, heads, groups, rows),
        arrays,
        [shape((rows + 16, DV), bf16)] * heads,
        [pltpu.VMEM((members, rows, DV), f32)],
    )
    moved = {}
    for k in reversed(range(1, heads)):
        moved[k] = swap(parts[k], "sp", k)
    own_rows, first_read = call(
        functools.partial(final_kernel, heads, rows),
        [small, parts[0]] + [moved[k] for k in range(1, heads)],
        [shape((heads, rows, DV), bf16), shape((heads, DV))],
        [pltpu.VMEM((heads, SUB, DV), f32)],
    )
    return (own_rows, first_read)


def solution(mesh):
    return jax.shard_map(
        per_device,
        mesh=mesh,
        in_specs=(
            P("sp", "tp"),
            P(None, "tp"),
            P(None, "tp"),
            P(),
            P(),
            P(),
            P(),
            P("tp", "sp"),
            P("tp", "sp"),
            P(),
        ),
        out_specs=(P("tp", "sp", None), P("tp", None)),
        check_vma=False,
    )
```

profile of v0, /device:TPU:0, one launch (start us, length us, event | category | flops | bytes accessed | tf_op | source)
XLA Modules:
  0.0 62.6 jit_solution(16992620343517753546)
XLA Ops:
  0.6 1.0 %slice.15.refs_0_ = bf16[128,1024]{1,0:T(8,128)(2,1)S(1)} slice(bf16[512,1024]{1,0:T(8,128)(2,1)} %param.10), slice={[0:128], [0:1024]} | slice | bytes 524288 | tf_op jit(solution)/shard_map/slice | solution.py:345
  1.6 3.1 %collective-permute-start.9 = (bf16[128,1024]{1,0:T(8,128)(2,1)S(1)}, bf16[128,1024]{1,0:T(8,128)(2,1)S(1)}, u32[]{:S(2)}, u32[]{:S(2)}) collective-permute-start(bf16[128,1024]{1,0:T(8,128)(2,1)S(1)} %slice.15.refs_0_), channel_id=1, source_target_pairs={{0,2},{1,3},{2,0},{3,1},{4,6},{5,7},{6,4},{7,5},{8,10},{9,11},{10,... | collective-permute-start | bytes 786440 | tf_op jit(solution)/shard_map/ppermute | solution.py:26
  5.5 2.7 %collective-permute-start.12 = (bf16[4,128]{1,0:T(4,128)(2,1)S(1)}, bf16[4,128]{1,0:T(4,128)(2,1)S(1)}, u32[]{:S(2)}, u32[]{:S(2)}) collective-permute-start(bf16[4,128]{1,0:T(4,128)(2,1)S(1)} %fusion.3), channel_id=1, source_target_pairs={{0,16},{4,20},{8,24},{12,28},{16,0},{20,4},{24,8},{28,12},{1,17},{... | collective-permute-start | bytes 3080 | tf_op jit(solution)/shard_map/ppermute | solution.py:26
  8.1 1.2 %fusion.6 = (bf16[128,1024]{1,0:T(8,128)(2,1)S(1)}, bf16[128,1024]{1,0:T(8,128)(2,1)S(1)}, bf16[128,1024]{1,0:T(8,128)(2,1)S(1)}) fusion(bf16[512,1024]{1,0:T(8,128)(2,1)} %param.10), kind=kLoop, calls=%fused_computation.20 | loop fusion | bytes 1572864 | tf_op jit(solution)/shard_map/slice | solution.py:347
  9.9 1.5 %collective-permute-start.3 = (bf16[128,1024]{1,0:T(8,128)(2,1)S(1)}, bf16[128,1024]{1,0:T(8,128)(2,1)S(1)}, u32[]{:S(2)}, u32[]{:S(2)}) collective-permute-start(bf16[128,1024]{1,0:T(8,128)(2,1)S(1)} %get-tuple-element.33.refs_0_), channel_id=1, source_target_pairs={{0,2},{1,3},{2,0},{3,1},{4,6},{5,7},{6,4},{7,5},{8,10},{9,11},{10,... | collective-permute-start | bytes 786440 | tf_op jit(solution)/shard_map/ppermute | solution.py:26
  11.4 0.9 %dynamic-slice_bitcast_fusion = (bf16[4,4096]{1,0:T(4,128)(2,1)S(1)}, bf16[4,4096]{1,0:T(4,128)(2,1)S(1)}) fusion(bf16[4096,16]{0,1:T(8,128)(2,1)} %param.14, s32[]{:T(128)S(6)} %select_n.13, bf16[4096,16]{0,1:T(8,128)(2,1)} %param.13), kind=kLoop, calls=%fused_computation.5 | loop fusion | bytes 131076 | tf_op jit(solution)/shard_map/dynamic_slice | solution.py:358
  13.0 0.7 %fusion.5 = f32[1,128]{1,0:T(1,128)S(1)} fusion(f32[16]{0:T(128)} %param.16, f32[16]{0:T(128)} %param.15), kind=kLoop, calls=%fused_computation.18 | loop fusion | flops 512 | bytes 640 | tf_op jit(solution)/shard_map/stack | solution.py:363
  13.8 3.5 %shard_map.113 = (bf16[4096,512]{1,0:T(8,128)(2,1)S(1)}, bf16[4096,512]{1,0:T(8,128)(2,1)S(1)}) custom-call(bf16[4096,512]{1,0:T(8,128)(2,1)} %wk_hbm.1, bf16[4096,512]{1,0:T(8,128)(2,1)} %wv_hbm.1), custom_call_target="tpu_custom_call" | custom-call | tf_op jit(solution)/shard_map/pallas_call | solution.py:372
  18.5 5.6 %collective-permute-done.3.refs_1_ = bf16[128,1024]{1,0:T(8,128)(2,1)S(1)} collective-permute-done((bf16[128,1024]{1,0:T(8,128)(2,1)S(1)}, bf16[128,1024]{1,0:T(8,128)(2,1)S(1)}, u32[]{:S(2)}, u32[]{:S(2)}) %collective-permute-start.3) | collective-permute-done | bytes 262176 | tf_op jit(solution)/shard_map/ppermute | solution.py:26
  24.7 3.6 %shard_map.114 = (f32[8,128]{1,0:T(8,128)S(1)}, f32[4,128,256]{2,1,0:T(8,128)S(1)}) custom-call(bf16[128,1024]{1,0:T(8,128)(2,1)S(1)} %slice.15.refs_0_, bf16[128,1024]{1,0:T(8,128)(2,1)S(1)} %collective-permute-done.9.refs_1_, bf16[128,1024]{1,0:T(8,128)(2,1)S(1)} %collective-permute-done.10.refs_2_, bf16[128,1024]{1,0:T(8,128)(2,1)S(1)} %collective-permute-done.11.refs_3_, ...), custom_call_target="tpu_custom_call" | custom-call | flops 1610612736 | tf_op jit(solution)/shard_map/pallas_call | solution.py:311
  29.0 3.6 %shard_map.115.refs_9_ = f32[4,128,256]{2,1,0:T(8,128)S(1)} custom-call(bf16[128,1024]{1,0:T(8,128)(2,1)S(1)} %get-tuple-element.32.refs_0_, bf16[128,1024]{1,0:T(8,128)(2,1)S(1)} %collective-permute-done.6.refs_1_, bf16[128,1024]{1,0:T(8,128)(2,1)S(1)} %collective-permute-done.7.refs_2_, bf16[128,1024]{1,0:T(8,128)(2,1)S(1)} %collective-permute-done.8.refs_3_, ...), custom_call_target="tpu_custom_call" | custom-call | flops 1610612736 | tf_op jit(solution)/shard_map/pallas_call | solution.py:311
  32.6 3.6 %shard_map.116.refs_9_ = f32[4,128,256]{2,1,0:T(8,128)S(1)} custom-call(bf16[128,1024]{1,0:T(8,128)(2,1)S(1)} %get-tuple-element.33.refs_0_, bf16[128,1024]{1,0:T(8,128)(2,1)S(1)} %collective-permute-done.3.refs_1_, bf16[128,1024]{1,0:T(8,128)(2,1)S(1)} %collective-permute-done.4.refs_2_, bf16[128,1024]{1,0:T(8,128)(2,1)S(1)} %collective-permute-done.5.refs_3_, ...), custom_call_target="tpu_custom_call" | custom-call | flops 1610612736 | tf_op jit(solution)/shard_map/pallas_call | solution.py:311
  36.3 4.4 %shard_map.117 = (bf16[144,256]{1,0:T(8,128)(2,1)S(1)}, bf16[144,256]{1,0:T(8,128)(2,1)S(1)}, bf16[144,256]{1,0:T(8,128)(2,1)S(1)}, bf16[144,256]{1,0:T(8,128)(2,1)S(1)}, f32[4,128,256]{2,1,0:T(8,128)}) custom-call(bf16[128,1024]{1,0:T(8,128)(2,1)S(1)} %get-tuple-element.34.refs_0_, bf16[128,1024]{1,0:T(8,128)(2,1)S(1)} %collective-permute-done.refs_1_, ...), custom_call_target="tpu_custom_call" | custom-call | flops 1610612736 | tf_op jit(solution)/shard_map/pallas_call | solution.py:311
  40.7 1.5 %collective-permute-start.13 = (bf16[144,256]{1,0:T(8,128)(2,1)S(1)}, bf16[144,256]{1,0:T(8,128)(2,1)S(1)}, u32[]{:S(2)}, u32[]{:S(2)}) collective-permute-start(bf16[144,256]{1,0:T(8,128)(2,1)S(1)} %get-tuple-element.22), channel_id=1, source_target_pairs={{0,4},{4,0},{8,12},{12,8},{16,20},{20,16},{24,28},{28,24},{1,5},{5... | collective-permute-start | bytes 221192 | tf_op jit(solution)/shard_map/ppermute | solution.py:26
  42.2 1.6 %collective-permute-start.14 = (bf16[144,256]{1,0:T(8,128)(2,1)S(1)}, bf16[144,256]{1,0:T(8,128)(2,1)S(1)}, u32[]{:S(2)}, u32[]{:S(2)}) collective-permute-start(bf16[144,256]{1,0:T(8,128)(2,1)S(1)} %get-tuple-element.23), channel_id=1, source_target_pairs={{0,8},{4,12},{8,0},{12,4},{16,24},{20,28},{24,16},{28,20},{1,9},{5... | collective-permute-start | bytes 221192 | tf_op jit(solution)/shard_map/ppermute | solution.py:26
  44.2 1.2 %collective-permute-done.13.refs_1_ = bf16[144,256]{1,0:T(8,128)(2,1)S(1)} collective-permute-done((bf16[144,256]{1,0:T(8,128)(2,1)S(1)}, bf16[144,256]{1,0:T(8,128)(2,1)S(1)}, u32[]{:S(2)}, u32[]{:S(2)}) %collective-permute-start.13) | collective-permute-done | bytes 73760 | tf_op jit(solution)/shard_map/ppermute | solution.py:26
  45.4 1.5 %collective-permute-done.14.refs_2_ = bf16[144,256]{1,0:T(8,128)(2,1)S(1)} collective-permute-done((bf16[144,256]{1,0:T(8,128)(2,1)S(1)}, bf16[144,256]{1,0:T(8,128)(2,1)S(1)}, u32[]{:S(2)}, u32[]{:S(2)}) %collective-permute-start.14) | collective-permute-done | bytes 73760 | tf_op jit(solution)/shard_map/ppermute | solution.py:26
  46.9 2.1 %collective-permute-done.15.refs_3_ = bf16[144,256]{1,0:T(8,128)(2,1)S(1)} collective-permute-done((bf16[144,256]{1,0:T(8,128)(2,1)S(1)}, bf16[144,256]{1,0:T(8,128)(2,1)S(1)}, u32[]{:S(2)}, u32[]{:S(2)}) %collective-permute-start.15) | collective-permute-done | bytes 73760 | tf_op jit(solution)/shard_map/ppermute | solution.py:26
  49.0 0.9 %shard_map.118 = (f32[128,256]{1,0:T(8,128)S(1)}, f32[8,256]{1,0:T(8,128)S(1)}, bf16[144,128]{1,0:T(8,128)(2,1)S(1)}) custom-call(bf16[144,256]{1,0:T(8,128)(2,1)S(1)} %get-tuple-element.21.refs_0_, bf16[144,256]{1,0:T(8,128)(2,1)S(1)} %collective-permute-done.13.refs_1_, bf16[144,256]{1,0:T(8,128)(2,1)S(1)} %collective-permute-done.14.refs_2_, ...), custom_call_target="tpu_custom_call" | custom-call | tf_op jit(solution)/shard_map/pallas_call | solution.py:311
  50.0 1.9 %collective-permute-start.16 = (bf16[144,128]{1,0:T(8,128)(2,1)S(1)}, bf16[144,128]{1,0:T(8,128)(2,1)S(1)}, u32[]{:S(2)}, u32[]{:S(2)}) collective-permute-start(bf16[144,128]{1,0:T(8,128)(2,1)S(1)} %get-tuple-element.27), channel_id=1, source_target_pairs={{0,16},{4,20},{8,24},{12,28},{16,0},{20,4},{24,8},{28,12},{1,17},{... | collective-permute-start | bytes 110600 | tf_op jit(solution)/shard_map/ppermute | solution.py:26
  51.8 3.4 %collective-permute-done.16.refs_0_ = bf16[144,128]{1,0:T(8,128)(2,1)S(1)} collective-permute-done((bf16[144,128]{1,0:T(8,128)(2,1)S(1)}, bf16[144,128]{1,0:T(8,128)(2,1)S(1)}, u32[]{:S(2)}, u32[]{:S(2)}) %collective-permute-start.16) | collective-permute-done | bytes 36896 | tf_op jit(solution)/shard_map/ppermute | solution.py:26
  55.8 1.6 %collective-permute-start.18 = (bf16[32,128]{1,0:T(8,128)(2,1)S(1)}, bf16[32,128]{1,0:T(8,128)(2,1)S(1)}, u32[]{:S(2)}, u32[]{:S(2)}) collective-permute-start(bf16[32,128]{1,0:T(8,128)(2,1)S(1)} %get-tuple-element.30), channel_id=1, source_target_pairs={{0,8},{4,12},{8,0},{12,4},{16,24},{20,28},{24,16},{28,20},{1,9},{5... | collective-permute-start | bytes 24584 | tf_op jit(solution)/shard_map/ppermute | solution.py:26
  57.4 1.7 %collective-permute-start.19 = (bf16[32,128]{1,0:T(8,128)(2,1)S(1)}, bf16[32,128]{1,0:T(8,128)(2,1)S(1)}, u32[]{:S(2)}, u32[]{:S(2)}) collective-permute-start(bf16[32,128]{1,0:T(8,128)(2,1)S(1)} %get-tuple-element.31), channel_id=1, source_target_pairs={{0,12},{4,8},{8,4},{12,0},{16,28},{20,24},{24,20},{28,16},{1,13},{... | collective-permute-start | bytes 24584 | tf_op jit(solution)/shard_map/ppermute | solution.py:26
  59.4 2.5 %collective-permute-done.19.refs_3_ = bf16[32,128]{1,0:T(8,128)(2,1)S(1)} collective-permute-done((bf16[32,128]{1,0:T(8,128)(2,1)S(1)}, bf16[32,128]{1,0:T(8,128)(2,1)S(1)}, u32[]{:S(2)}, u32[]{:S(2)}) %collective-permute-start.19) | collective-permute-done | bytes 8224 | tf_op jit(solution)/shard_map/ppermute | solution.py:26
  (39 shorter events, 6.6 us)
Async XLA Ops:
  1.6 12.1 %collective-permute-start.9 = (bf16[128,1024]{1,0:T(8,128)(2,1)S(1)}, bf16[128,1024]{1,0:T(8,128)(2,1)S(1)}, u32[]{:S(2)}, u32[]{:S(2)}) collective-permute-start(bf16[128,1024]{1,0:T(8,128)(2,1)S(1)} %slice.15.refs_0_), channel_id=1, source_target_pairs={{0,2},{1,3},{2,0},{3,1},{4,6},{5,7},{6,4},{7,5},{8,10},{9,11},{10,... | collective-permute-start | bytes 786440 | tf_op jit(solution)/shard_map/ppermute | solution.py:26
  4.7 13.2 %collective-permute-start.10 = (bf16[128,1024]{1,0:T(8,128)(2,1)S(1)}, bf16[128,1024]{1,0:T(8,128)(2,1)S(1)}, u32[]{:S(2)}, u32[]{:S(2)}) collective-permute-start(bf16[128,1024]{1,0:T(8,128)(2,1)S(1)} %slice.15.refs_0_), channel_id=1, source_target_pairs={{0,1},{1,0},{2,3},{3,2},{4,5},{5,4},{6,7},{7,6},{8,9},{9,8},{10,11... | collective-permute-start | bytes 786440 | tf_op jit(solution)/shard_map/ppermute | solution.py:26
  5.5 11.8 %collective-permute-start.12 = (bf16[4,128]{1,0:T(4,128)(2,1)S(1)}, bf16[4,128]{1,0:T(4,128)(2,1)S(1)}, u32[]{:S(2)}, u32[]{:S(2)}) collective-permute-start(bf16[4,128]{1,0:T(4,128)(2,1)S(1)} %fusion.3), channel_id=1, source_target_pairs={{0,16},{4,20},{8,24},{12,28},{16,0},{20,4},{24,8},{28,12},{1,17},{... | collective-permute-start | bytes 3080 | tf_op jit(solution)/shard_map/ppermute | solution.py:26
  9.3 9.2 %collective-permute-start.6 = (bf16[128,1024]{1,0:T(8,128)(2,1)S(1)}, bf16[128,1024]{1,0:T(8,128)(2,1)S(1)}, u32[]{:S(2)}, u32[]{:S(2)}) collective-permute-start(bf16[128,1024]{1,0:T(8,128)(2,1)S(1)} %get-tuple-element.32.refs_0_), channel_id=1, source_target_pairs={{0,2},{1,3},{2,0},{3,1},{4,6},{5,7},{6,4},{7,5},{8,10},{9,11},{10,... | collective-permute-start | bytes 786440 | tf_op jit(solution)/shard_map/ppermute | solution.py:26
  9.9 14.3 %collective-permute-start.3 = (bf16[128,1024]{1,0:T(8,128)(2,1)S(1)}, bf16[128,1024]{1,0:T(8,128)(2,1)S(1)}, u32[]{:S(2)}, u32[]{:S(2)}) collective-permute-start(bf16[128,1024]{1,0:T(8,128)(2,1)S(1)} %get-tuple-element.33.refs_0_), channel_id=1, source_target_pairs={{0,2},{1,3},{2,0},{3,1},{4,6},{5,7},{6,4},{7,5},{8,10},{9,11},{10,... | collective-permute-start | bytes 786440 | tf_op jit(solution)/shard_map/ppermute | solution.py:26
  13.7 10.4 %collective-permute-start.11 = (bf16[128,1024]{1,0:T(8,128)(2,1)S(1)}, bf16[128,1024]{1,0:T(8,128)(2,1)S(1)}, u32[]{:S(2)}, u32[]{:S(2)}) collective-permute-start(bf16[128,1024]{1,0:T(8,128)(2,1)S(1)} %collective-permute-done.9.refs_1_), channel_id=1, source_target_pairs={{0,1},{1,0},{2,3},{3,2},{4,5},{5,4},{6,7},{7,6},{8,9},{9,8},{10,11... | collective-permute-start | bytes 786440 | tf_op jit(solution)/shard_map/ppermute | solution.py:26
  13.8 10.9 %copy-start = (f32[4,512]{1,0:T(4,128)S(1)}, f32[4,512]{1,0:T(4,128)}, u32[]{:S(2)}) copy-start(f32[4,512]{1,0:T(4,128)} %refs_8_.7) | copy-start | bytes 24580
  17.3 11.0 %collective-permute-start.7 = (bf16[128,1024]{1,0:T(8,128)(2,1)S(1)}, bf16[128,1024]{1,0:T(8,128)(2,1)S(1)}, u32[]{:S(2)}, u32[]{:S(2)}) collective-permute-start(bf16[128,1024]{1,0:T(8,128)(2,1)S(1)} %get-tuple-element.32.refs_0_), channel_id=1, source_target_pairs={{0,1},{1,0},{2,3},{3,2},{4,5},{5,4},{6,7},{7,6},{8,9},{9,8},{10,11... | collective-permute-start | bytes 786440 | tf_op jit(solution)/shard_map/ppermute | solution.py:26
  17.8 11.2 %collective-permute-start = (bf16[128,1024]{1,0:T(8,128)(2,1)S(1)}, bf16[128,1024]{1,0:T(8,128)(2,1)S(1)}, u32[]{:S(2)}, u32[]{:S(2)}) collective-permute-start(bf16[128,1024]{1,0:T(8,128)(2,1)S(1)} %get-tuple-element.34.refs_0_), channel_id=1, source_target_pairs={{0,2},{1,3},{2,0},{3,1},{4,6},{5,7},{6,4},{7,5},{8,10},{9,11},{10,... | collective-permute-start | bytes 786440 | tf_op jit(solution)/shard_map/ppermute | solution.py:26
  18.5 10.5 %collective-permute-start.8 = (bf16[128,1024]{1,0:T(8,128)(2,1)S(1)}, bf16[128,1024]{1,0:T(8,128)(2,1)S(1)}, u32[]{:S(2)}, u32[]{:S(2)}) collective-permute-start(bf16[128,1024]{1,0:T(8,128)(2,1)S(1)} %collective-permute-done.6.refs_1_), channel_id=1, source_target_pairs={{0,1},{1,0},{2,3},{3,2},{4,5},{5,4},{6,7},{7,6},{8,9},{9,8},{10,11... | collective-permute-start | bytes 786440 | tf_op jit(solution)/shard_map/ppermute | solution.py:26
  24.1 8.5 %collective-permute-start.4 = (bf16[128,1024]{1,0:T(8,128)(2,1)S(1)}, bf16[128,1024]{1,0:T(8,128)(2,1)S(1)}, u32[]{:S(2)}, u32[]{:S(2)}) collective-permute-start(bf16[128,1024]{1,0:T(8,128)(2,1)S(1)} %get-tuple-element.33.refs_0_), channel_id=1, source_target_pairs={{0,1},{1,0},{2,3},{3,2},{4,5},{5,4},{6,7},{7,6},{8,9},{9,8},{10,11... | collective-permute-start | bytes 786440 | tf_op jit(solution)/shard_map/ppermute | solution.py:26
  24.1 8.5 %collective-permute-start.5 = (bf16[128,1024]{1,0:T(8,128)(2,1)S(1)}, bf16[128,1024]{1,0:T(8,128)(2,1)S(1)}, u32[]{:S(2)}, u32[]{:S(2)}) collective-permute-start(bf16[128,1024]{1,0:T(8,128)(2,1)S(1)} %collective-permute-done.3.refs_1_), channel_id=1, source_target_pairs={{0,1},{1,0},{2,3},{3,2},{4,5},{5,4},{6,7},{7,6},{8,9},{9,8},{10,11... | collective-permute-start | bytes 786440 | tf_op jit(solution)/shard_map/ppermute | solution.py:26
  28.3 8.0 %collective-permute-start.1 = (bf16[128,1024]{1,0:T(8,128)(2,1)S(1)}, bf16[128,1024]{1,0:T(8,128)(2,1)S(1)}, u32[]{:S(2)}, u32[]{:S(2)}) collective-permute-start(bf16[128,1024]{1,0:T(8,128)(2,1)S(1)} %get-tuple-element.34.refs_0_), channel_id=1, source_target_pairs={{0,1},{1,0},{2,3},{3,2},{4,5},{5,4},{6,7},{7,6},{8,9},{9,8},{10,11... | collective-permute-start | bytes 786440 | tf_op jit(solution)/shard_map/ppermute | solution.py:26
  29.0 7.2 %collective-permute-start.2 = (bf16[128,1024]{1,0:T(8,128)(2,1)S(1)}, bf16[128,1024]{1,0:T(8,128)(2,1)S(1)}, u32[]{:S(2)}, u32[]{:S(2)}) collective-permute-start(bf16[128,1024]{1,0:T(8,128)(2,1)S(1)} %collective-permute-done.refs_1_), channel_id=1, source_target_pairs={{0,1},{1,0},{2,3},{3,2},{4,5},{5,4},{6,7},{7,6},{8,9},{9,8},{10,11... | collective-permute-start | bytes 786440 | tf_op jit(solution)/shard_map/ppermute | solution.py:26
  40.7 4.7 %collective-permute-start.13 = (bf16[144,256]{1,0:T(8,128)(2,1)S(1)}, bf16[144,256]{1,0:T(8,128)(2,1)S(1)}, u32[]{:S(2)}, u32[]{:S(2)}) collective-permute-start(bf16[144,256]{1,0:T(8,128)(2,1)S(1)} %get-tuple-element.22), channel_id=1, source_target_pairs={{0,4},{4,0},{8,12},{12,8},{16,20},{20,16},{24,28},{28,24},{1,5},{5... | collective-permute-start | bytes 221192 | tf_op jit(solution)/shard_map/ppermute | solution.py:26
  42.2 4.7 %collective-permute-start.14 = (bf16[144,256]{1,0:T(8,128)(2,1)S(1)}, bf16[144,256]{1,0:T(8,128)(2,1)S(1)}, u32[]{:S(2)}, u32[]{:S(2)}) collective-permute-start(bf16[144,256]{1,0:T(8,128)(2,1)S(1)} %get-tuple-element.23), channel_id=1, source_target_pairs={{0,8},{4,12},{8,0},{12,4},{16,24},{20,28},{24,16},{28,20},{1,9},{5... | collective-permute-start | bytes 221192 | tf_op jit(solution)/shard_map/ppermute | solution.py:26
  43.7 5.3 %collective-permute-start.15 = (bf16[144,256]{1,0:T(8,128)(2,1)S(1)}, bf16[144,256]{1,0:T(8,128)(2,1)S(1)}, u32[]{:S(2)}, u32[]{:S(2)}) collective-permute-start(bf16[144,256]{1,0:T(8,128)(2,1)S(1)} %get-tuple-element.24), channel_id=1, source_target_pairs={{0,12},{4,8},{8,4},{12,0},{16,28},{20,24},{24,20},{28,16},{1,13},{... | collective-permute-start | bytes 221192 | tf_op jit(solution)/shard_map/ppermute | solution.py:26
  50.0 5.3 %collective-permute-start.16 = (bf16[144,128]{1,0:T(8,128)(2,1)S(1)}, bf16[144,128]{1,0:T(8,128)(2,1)S(1)}, u32[]{:S(2)}, u32[]{:S(2)}) collective-permute-start(bf16[144,128]{1,0:T(8,128)(2,1)S(1)} %get-tuple-element.27), channel_id=1, source_target_pairs={{0,16},{4,20},{8,24},{12,28},{16,0},{20,4},{24,8},{28,12},{1,17},{... | collective-permute-start | bytes 110600 | tf_op jit(solution)/shard_map/ppermute | solution.py:26
  55.5 3.7 %collective-permute-start.17 = (bf16[32,128]{1,0:T(8,128)(2,1)S(1)}, bf16[32,128]{1,0:T(8,128)(2,1)S(1)}, u32[]{:S(2)}, u32[]{:S(2)}) collective-permute-start(bf16[32,128]{1,0:T(8,128)(2,1)S(1)} %get-tuple-element.29), channel_id=1, source_target_pairs={{0,4},{4,0},{8,12},{12,8},{16,20},{20,16},{24,28},{28,24},{1,5},{5... | collective-permute-start | bytes 24584 | tf_op jit(solution)/shard_map/ppermute | solution.py:26
  55.8 3.7 %collective-permute-start.18 = (bf16[32,128]{1,0:T(8,128)(2,1)S(1)}, bf16[32,128]{1,0:T(8,128)(2,1)S(1)}, u32[]{:S(2)}, u32[]{:S(2)}) collective-permute-start(bf16[32,128]{1,0:T(8,128)(2,1)S(1)} %get-tuple-element.30), channel_id=1, source_target_pairs={{0,8},{4,12},{8,0},{12,4},{16,24},{20,28},{24,16},{28,20},{1,9},{5... | collective-permute-start | bytes 24584 | tf_op jit(solution)/shard_map/ppermute | solution.py:26
  57.4 4.5 %collective-permute-start.19 = (bf16[32,128]{1,0:T(8,128)(2,1)S(1)}, bf16[32,128]{1,0:T(8,128)(2,1)S(1)}, u32[]{:S(2)}, u32[]{:S(2)}) collective-permute-start(bf16[32,128]{1,0:T(8,128)(2,1)S(1)} %get-tuple-element.31), channel_id=1, source_target_pairs={{0,12},{4,8},{8,4},{12,0},{16,28},{20,24},{24,20},{28,16},{1,13},{... | collective-permute-start | bytes 24584 | tf_op jit(solution)/shard_map/ppermute | solution.py:26
where the time goes:
time: 62.8 us; the launch traced here: 62.6 us
  Pallas kernels  20.5 us (33%)
  starting transfers between devices  18.4 us (29%)
  waiting for transfers between devices  17.6 us (28%)
  local copies, waits for them, and re-layouts  3.82 us (6%)
  other arithmetic  1.47 us (2%)
  between operations  0.79 us (1%)
    ppermute x20, starting transfers between devices, swap(): return lax.ppermute(x, axis, flip(axis, mask))  18.4 us
    ppermute x20, waiting for transfers between devices, swap(): return lax.ppermute(x, axis, flip(axis, mask))  17.6 us
    pallas_call x7, Pallas kernels, call(): pl.pallas_call(body, out_shape=outs, in_specs=[vmem] * len(arrays), out_s...  17 us
    pallas_call x1, Pallas kernels, per_device(): pl.pallas_call(load_kernel, out_shape=[shape(w_key.shape, bf16), shape(w_...  3.49 us
    another operation x3, other arithmetic, per_device(): jnp.stack([jnp.pad(named, (0, DK - named.shape[0])), read_gain.astype(f32)])  1.42 us
  transfers between devices with their start and end apart: 20, of which 10 were waited for; matrix products, arithmetic and copies ran while one was open for 7% of the time, Pallas kernels for 23%

commit v1 on v0

--- a/solution.py
+++ b/solution.py
@@ -30,8 +30,25 @@
     return jnp.dot(left.astype(bf16), right.astype(bf16), preferred_element_type=f32)
 
 
-def dot_exact(left, right):
-    return jnp.dot(left, right, precision=lax.Precision.HIGHEST, preferred_element_type=f32)
+def split(x):
+    high = x.astype(bf16)
+    return high, (x - high.astype(f32)).astype(bf16)
+
+
+def dot3(left, right):
+    lh, ll = split(left)
+    rh, rl = split(right)
+    return dot(lh, rh) + (dot(lh, rl) + dot(ll, rh))
+
+
+def dot_ones(left, ones):
+    high, rest = split(left)
+    mid = rest
+    low = (left - high.astype(f32) - mid.astype(f32)).astype(bf16)
+    n = left.shape[0]
+    parts = jnp.concatenate([high.astype(f32), mid.astype(f32), low.astype(f32)], axis=0)
+    out = dot(parts, ones)
+    return out[:n] + out[n : 2 * n] + out[2 * n :]
 
 
 def dot_nt(left, right):
@@ -71,13 +88,60 @@
     return results
 
 
-def load_kernel(wk_hbm, wv_hbm, wk_ref, wv_ref, sems):
-    copies = [
-        pltpu.make_async_copy(wk_hbm, wk_ref, sems.at[0]),
-        pltpu.make_async_copy(wv_hbm, wv_ref, sems.at[1]),
+def prepare_kernel(heads, *refs):
+    wk_hbm, wv_hbm = refs[:2]
+    wk_ref, wv_ref, wg_ref, small_ref, forget_ref, query_ref = refs[8:14]
+    few, sems = refs[14:20], refs[20]
+    wb_ref, wd_ref, bias_ref, rate_ref, forget_in, query_in = few
+    lead = lax.axis_index("sp") % heads
+    first = lax.axis_index("tp") * heads
+    early = [
+        pltpu.make_async_copy(hbm, ref, sems.at[2 * heads + i])
+        for i, (hbm, ref) in enumerate(zip(refs[2:8], few))
     ]
-    for copy in copies:
+    copies = []
+    for k in range(heads):
+        source = pl.ds(pl.multiple_of((lead ^ k) * DK, DK), DK)
+        target = pl.ds(k * DK, DK)
+        for i, (hbm, ref) in enumerate(((wk_hbm, wk_ref), (wv_hbm, wv_ref))):
+            copies.append(
+                pltpu.make_async_copy(hbm.at[:, source], ref.at[:, target], sems.at[2 * k + i])
+            )
+    for copy in early + copies:
         copy.start()
+    for copy in early:
+        copy.wait()
+    many = bias_ref.shape[1]
+    row = lax.broadcasted_iota(jnp.int32, (2 * SUB, 2 * many), 0)
+    col = lax.broadcasted_iota(jnp.int32, (2 * SUB, 2 * many), 1)
+    k = row & (SUB - 1)
+    wanted = first + (lead ^ k) + jnp.where(row >= SUB, many, 0)
+    pick = jnp.where(jnp.logical_and(col == wanted, k < heads), 1.0, 0.0)
+    both = jnp.concatenate([wb_ref[...], wd_ref[...]], axis=0)
+    wg_ref[...] = dot(pick, both).astype(bf16)
+    row = lax.broadcasted_iota(jnp.int32, (SUB, many), 0)
+    col = lax.broadcasted_iota(jnp.int32, (SUB, many), 1)
+    mine = col == first + (lead ^ row)
+    bias = jnp.sum(jnp.where(mine, bias_ref[...], 0.0), axis=1, keepdims=True)
+    rate = jnp.sum(jnp.where(mine, rate_ref[...], 0.0), axis=1, keepdims=True)
+    lane = lax.broadcasted_iota(jnp.int32, (SUB, DK), 1)
+    small_ref[...] = jnp.where(lane == 0, bias, jnp.where(lane == 1, rate, 0.0))
+    seats = query_in.shape[1]
+    place = lax.axis_index("sp") * seats
+    row = lax.broadcasted_iota(jnp.int32, (seats, DK), 0)
+    col = lax.broadcasted_iota(jnp.int32, (seats, DK), 1)
+    query = dot(query_in[...], jnp.where(col == row + place, 1.0, 0.0))
+    forget = forget_in[...]
+    size = forget.shape[1]
+    wide = lax.broadcasted_iota(jnp.int32, (SUB, size), 0)
+    slim = lax.broadcasted_iota(jnp.int32, (SUB, DK), 0)
+    forget_out = jnp.zeros((SUB, size), f32)
+    query_out = jnp.zeros((SUB, DK), f32)
+    for h in range(heads):
+        forget_out = jnp.where((lead ^ wide) == h, forget[h : h + 1], forget_out)
+        query_out = jnp.where((lead ^ slim) == h, query[h : h + 1], query_out)
+    forget_ref[...] = forget_out
+    query_ref[...] = query_out
     for copy in copies:
         copy.wait()
 
@@ -89,10 +153,8 @@
     rest = refs[pieces + 5 :]
     if index > 0:
         state_ref, rest = rest[0], rest[1:]
-    if last or index == 0:
+    if last:
         query_ref, rest = rest[0], rest[1:]
-    if index == 0 and not last:
-        rest[0][0:heads, :] = query_ref[...].astype(f32)
     size, width = piece_refs[0].shape
     rank = lax.axis_index("tp")
     starts = [pl.multiple_of((rank ^ m) * width, width) for m in masks]
@@ -101,20 +163,13 @@
     for start, piece_ref in zip(starts, piece_refs):
         g = dot_nt(wg_ref[:, pl.ds(start, width)], piece_ref[...])
         gates = g if gates is None else gates + g
-    total_heads = heads * lax.axis_size("tp")
-    lane = lax.broadcasted_iota(jnp.int32, (SUB, DK), 1)
-    head = lax.broadcasted_iota(jnp.int32, (SUB, DK), 0) + rank * heads
-    small = small_ref[0:1, :]
-    bias = jnp.sum(jnp.where(lane == head, small, 0.0), axis=1, keepdims=True)
-    rate = jnp.sum(jnp.where(lane == head + total_heads, small, 0.0), axis=1, keepdims=True)
+    bias, rate = small_ref[:, 0:1], small_ref[:, 1:2]
     forget = forget_ref[:, index * size : (index + 1) * size]
-    if heads < SUB:
-        forget = jnp.concatenate([forget, jnp.zeros((SUB - heads, size), f32)], axis=0)
     beta_row = jax.nn.sigmoid(gates[0:SUB] + bias)
     log_row = forget - rate * jax.nn.softplus(gates[SUB : 2 * SUB])
     row = lax.broadcasted_iota(jnp.int32, (size, size), 0)
     col = lax.broadcasted_iota(jnp.int32, (size, size), 1)
-    cum_row = dot_exact(log_row, jnp.where(row <= col, 1.0, 0.0))
+    cum_row = dot_ones(log_row, jnp.where(row <= col, 1.0, 0.0))
     total = cum_row[:, size - 1 : size]
     stacked = jnp.concatenate(
         [
@@ -171,58 +226,55 @@
     for h in range(heads):
         remain = keys[h] * columns[:, 3 * SUB + h : 3 * SUB + h + 1]
         new = keep[h : h + 1, :] * states[h] + dot_tn(remain, fresh[h])
-        rest[-1][h] = new
-    if last:
-        lead = lax.axis_index("sp") % heads
-        for k in range(heads):
-            rest[k][0:DK, :] = rest[-1][lead ^ k].astype(bf16)
-            asked = jnp.broadcast_to(query_ref[pl.ds(lead ^ k, 1), :].astype(f32), (2 * SUB, DK))
+        if last:
+            rest[h][0:DK, :] = new.astype(bf16)
+            asked = jnp.broadcast_to(query_ref[h : h + 1, :], (2 * SUB, DK))
             asked = jnp.concatenate([asked, jnp.zeros((2 * SUB, DV), f32)], axis=1)
-            rest[k][DK:, :] = asked.astype(bf16)
-
-
-def compose(pairs):
+            rest[h][DK:, :] = asked.astype(bf16)
+        else:
+            rest[-1][h] = new
+
+
+def compose(pairs, product):
     while len(pairs) > 1:
         merged = []
         for early, late in zip(pairs[0::2], pairs[1::2]):
-            new = dot_exact(late[:, DV:], early)
-            merged.append(
-                jnp.concatenate([new[:, :DV] + late[:, :DV], new[:, DV:]], axis=1)
-            )
-        pairs = merged
+            new = product(late[:, DV:], early)
+            merged.append(jnp.concatenate([new[:, :DV] + late[:, :DV], new[:, DV:]], axis=1))
+        pairs, product = merged, dot3
     return pairs[0]
-
-
-def split(x):
-    high = x.astype(bf16)
-    return high, (x - high.astype(f32)).astype(bf16)
 
 
 def pad_rows(x, rows):
     return jnp.concatenate([x, jnp.zeros((rows - x.shape[0], x.shape[1]), x.dtype)], axis=0)
 
 
-def message(high, own, query):
+def late_side(mask):
+    return lax.rem(lax.div(lax.axis_index("sp"), jnp.int32(mask)), jnp.int32(2)) == 1
+
+
+def finish(total, query, out):
+    out[0][...] = total
+    out[1][...] = query
+    if len(out) == 2:
+        return
     half = DK // 2
-    through = dot_exact(query, own)
-    a, b = own[:, DV:], own[:, :DV]
+    through = dot3(query, total)
+    a, b = total[:, DV:], total[:, :DV]
+    high = late_side(lax.axis_size("sp") // 2)
     body = jnp.where(high, jnp.concatenate([a[:half], b[:half]], axis=0), b)
     ah, al = split(through[0:1, DV:])
     bh, bl = split(through[0:1, :DV])
-    tail = pad_rows(jnp.concatenate([ah, al, bh, bl], axis=0).astype(f32), 16)
-    return through, jnp.concatenate([body, tail], axis=0).astype(bf16)
-
-
-def late_side(mask):
-    return lax.rem(lax.div(lax.axis_index("sp"), jnp.int32(mask)), jnp.int32(2)) == 1
-
-
-def finish(total, query, out):
-    out[0][...] = total
-    through, send = message(late_side(lax.axis_size("sp") // 2), total, query)
-    out[1][...] = through
-    if len(out) > 2:
-        out[2][...] = send
+    tail = [query[0:1]] + [x.astype(f32) for x in (ah, al, bh, bl)]
+    tail = pad_rows(jnp.concatenate(tail, axis=0), 2 * SUB)
+    out[2][0:DK, :] = body.astype(bf16)
+    out[2][DK:, :] = tail.astype(bf16)
+
+
+def passed_on(total, query):
+    asked = jnp.concatenate([query, query], axis=0)
+    asked = jnp.concatenate([asked, jnp.zeros((2 * SUB, DV), f32)], axis=1)
+    return jnp.concatenate([total, asked], axis=0).astype(bf16)
 
 
 def compose_kernel(heads, final, *refs):
@@ -230,35 +282,37 @@
     out, scratch = refs[heads:-1], refs[-1]
     lead = lax.axis_index("sp") % heads
     scratch[lead] = own_ref[:DK, :].astype(f32)
-    query = own_ref[DK:, :DK].astype(f32)[:SUB]
+    query = own_ref[DK:, :DK].astype(f32)
     for k in range(1, heads):
         scratch[lead ^ k] = got[k - 1][:DK, :].astype(f32)
-        query = query + got[k - 1][DK:, :DK].astype(f32)[:SUB]
-    total = compose([scratch[i] for i in range(heads)])
+        query = query + got[k - 1][DK:, :DK].astype(f32)
+    total = compose([scratch[i] for i in range(heads)], dot)
+    query = query[:SUB]
     if final:
         finish(total, query, out)
     else:
-        out[0][...] = total
-        out[1][...] = query
-
-
-def merge_kernel(mask, final, own_ref, got_ref, query_ref, *out):
+        out[0][...], out[1][...] = total, query
+        out[2][...] = passed_on(total, query)
+
+
+def merge_kernel(mask, final, own_ref, query_ref, got_ref, *out):
     high = late_side(mask)
-    own, got = own_ref[...], got_ref[...].astype(f32)
+    own, got = own_ref[...], got_ref[:DK, :].astype(f32)
+    query = query_ref[...] + got_ref[DK:, :DK].astype(f32)[:SUB]
     early, late = jnp.where(high, got, own), jnp.where(high, own, got)
-    total = compose([early, late])
+    total = compose([early, late], dot3)
     if final:
-        finish(total, query_ref[...], out)
+        finish(total, query, out)
     else:
-        out[0][...] = total
-        out[1][...] = query_ref[...]
-
-
-def rows_kernel(heads, groups, rows, own_ref, mine_ref, *refs):
+        out[0][...], out[1][...] = total, query
+        out[2][...] = passed_on(total, query)
+
+
+def rows_kernel(heads, groups, rows, own_ref, query_ref, *refs):
     if groups > 1:
         got_ref, refs = refs[0], refs[1:]
     scratch = refs[-1]
-    own, mine = own_ref[...], mine_ref[...]
+    own, query = own_ref[...], query_ref[...]
     half = DK // 2
     place = lax.axis_index("sp")
     if groups > 1:
@@ -268,26 +322,29 @@
         early = jnp.where(high, got[:DK], b)
         late_a = jnp.where(high, a[half:], got[:half])
         late_b = jnp.where(high, b[half:], got[half:DK])
-        through_a = jnp.where(high, mine[0:1, DV:], got[DK : DK + 1] + got[DK + 1 : DK + 2])
-        through_b = jnp.where(high, mine[0:1, :DV], got[DK + 2 : DK + 3] + got[DK + 3 : DK + 4])
-        both = dot_exact(pad_rows(jnp.concatenate([late_a, through_a], axis=0), half + 8), early)
+        tail = got[DK:]
+        cross = dot3(jnp.broadcast_to(tail[0:1], (SUB, DK)), own)[0:1]
+        through_a = jnp.where(high, cross[:, DV:], tail[1:2] + tail[2:3])
+        through_b = jnp.where(high, cross[:, :DV], tail[3:4] + tail[4:5])
+        both = dot3(pad_rows(jnp.concatenate([late_a, through_a], axis=0), half + SUB), early)
         state = both[:half] + late_b
-        read = both[half : half + 1] + through_b
+        asked = jnp.where(high, query[:, half:], query[:, :half])
+        read = dot3(asked, state)[0:1] + (both[half : half + 1] + through_b)
     else:
         state = own[:, :DV]
-        read = mine[0:1, :DV]
+        read = dot3(query, state)[0:1]
     members = state.shape[0] // rows
     for i in range(members):
         scratch[i] = state[i * rows : (i + 1) * rows]
     place = place % members
     rh, rl = split(read)
-    tail = pad_rows(jnp.concatenate([rh, rl], axis=0).astype(f32), 16)
+    tail = pad_rows(jnp.concatenate([rh.astype(f32), rl.astype(f32)], axis=0), 16)
     for k in range(heads):
         body = scratch[place ^ k]
         refs[k][...] = jnp.concatenate([body, tail], axis=0).astype(bf16)
 
 
-def final_kernel(heads, rows, small_ref, *refs):
+def final_kernel(heads, rows, gain_ref, *refs):
     lead = lax.axis_index("sp") % heads
     state_ref, read_ref, scratch = refs[heads:]
     for k in range(heads):
@@ -297,7 +354,7 @@
         scratch[lead ^ k] = jnp.broadcast_to(wide[0:1] + wide[1:2], (SUB, DV))
     raw = jnp.concatenate([scratch[h][0:1] for h in range(heads)], axis=0)
     norm = lax.rsqrt(jnp.mean(raw * raw, axis=-1, keepdims=True) + norm_eps)
-    read_ref[...] = raw * norm * small_ref[1:2, :]
+    read_ref[...] = raw * norm * gain_ref[...].astype(f32)
 
 
 def shape(dims, dtype=f32):
@@ -335,8 +392,8 @@
 ):
     heads = w_key.shape[1] // DK
     length, width = tokens.shape
-    count, place = lax.axis_size("sp"), lax.axis_index("sp")
-    ranks, rank = lax.axis_size("tp"), lax.axis_index("tp")
+    count = lax.axis_size("sp")
+    ranks = lax.axis_size("tp")
     groups = count // heads
     rows = DK // count
     chunk = min(CHUNK, length)
@@ -354,45 +411,48 @@
         found += [(m ^ 1, swap(x, "tp", 1)) for m, x in found[1:-1]]
         gathered.append(found)
 
-    def head_rows(x):
-        part = lax.dynamic_slice_in_dim(x.T, rank * heads, heads, 0)
-        return jnp.pad(part, ((0, SUB - heads), (0, 0)))
-
-    gate_weights = jnp.concatenate([head_rows(w_beta), head_rows(w_decay)], axis=0)
-    named = jnp.concatenate([beta_bias, decay_rate])
-    small = jnp.stack([jnp.pad(named, (0, DK - named.shape[0])), read_gain.astype(f32)])
-
-    seat = lax.broadcasted_iota(jnp.int32, (heads, DK), 1) // rows
-    query = jnp.where(seat == place, jnp.tile(new_query, (1, count)), jnp.zeros((), bf16))
-    mask = heads
-    while mask < count:
-        query = query + swap(query, "sp", mask)
-        mask *= 2
-
-    w_key, w_value = pl.pallas_call(
-        load_kernel,
-        out_shape=[shape(w_key.shape, bf16), shape(w_value.shape, bf16)],
-        in_specs=[pl.BlockSpec(memory_space=pltpu.HBM)] * 2,
-        out_specs=[vmem] * 2,
-        scratch_shapes=[pltpu.SemaphoreType.DMA((2,))],
-        compiler_params=pltpu.CompilerParams(vmem_limit_bytes=20 * 1024 * 1024),
-    )(*[pltpu.with_memory_space_constraint(w, pltpu.HBM) for w in (w_key, w_value)])
+    plain = [
+        pltpu.with_memory_space_constraint(x, pltpu.HBM)
+        for x in (
+            w_key,
+            w_value,
+            w_beta.T,
+            w_decay.T,
+            beta_bias[None],
+            decay_rate[None],
+            forgetting_increment,
+            new_query,
+        )
+    ]
+    w_key, w_value, gate_weights, small, forget, query = pl.pallas_call(
+        functools.partial(prepare_kernel, heads),
+        out_shape=[
+            shape(w_key.shape, bf16),
+            shape(w_value.shape, bf16),
+            shape((2 * SUB, w_beta.shape[0]), bf16),
+            shape((SUB, DK)),
+            shape((SUB, length)),
+            shape((SUB, DK)),
+        ],
+        in_specs=[pl.BlockSpec(memory_space=pltpu.HBM)] * 8,
+        out_specs=[vmem] * 6,
+        scratch_shapes=[pltpu.VMEM(x.shape, x.dtype) for x in plain[2:]]
+        + [pltpu.SemaphoreType.DMA((2 * heads + 6,))],
+        compiler_params=pltpu.CompilerParams(vmem_limit_bytes=24 * 1024 * 1024),
+    )(*plain)
 
     state = None
     flops = 2 * chunk * width * ranks * (2 * heads * DK + DK) + heads * 24 * 2 * chunk * chunk * DK
     for c in range(chunks):
         found = gathered[c]
         last = c == chunks - 1
-        arrays = [x for _, x in found] + [w_key, w_value, gate_weights, small, forgetting_increment]
+        arrays = [x for _, x in found] + [w_key, w_value, gate_weights, small, forget]
         if c > 0:
             arrays.append(state)
         outs = [shape((heads, DK, DV + DK))]
-        if last or c == 0:
+        if last:
             arrays.append(query)
-        if last:
-            outs = [shape((DK + 2 * SUB, DV + DK), bf16)] * heads + outs
-        elif c == 0:
-            outs = [shape((SUB, DK))] + outs
+            outs = [shape((DK + 2 * SUB, DV + DK), bf16)] * heads
         result = call(
             functools.partial(chunk_kernel, heads, c, last, tuple(m for m, _ in found)),
             arrays,
@@ -401,17 +461,15 @@
             flops=flops,
         )
         state = result[-1]
-        if c == 0 and not last:
-            query = result[0]
-    maps = result[:heads]
+    maps = result
 
     got = {}
     for k in reversed(range(1, heads)):
         got[k] = swap(maps[k], "sp", k)
-    done = [shape((DK, DV + DK)), shape((SUB, DV + DK))]
+    done = [shape((DK, DV + DK)), shape((SUB, DK))]
+    open_ended = done + [shape((DK + 2 * SUB, DV + DK), bf16)]
     if groups > 1:
-        done.append(shape((DK + 16, DV), bf16))
-    open_ended = [shape((DK, DV + DK)), shape((SUB, DK))]
+        done.append(shape((DK + 2 * SUB, DV), bf16))
     result = call(
         functools.partial(compose_kernel, heads, groups <= 2),
         [maps[0]] + [got[k] for k in range(1, heads)],
@@ -421,10 +479,9 @@
     mask = heads
     while 2 * mask < count:
         final = 4 * mask == count
-        partner = swap(result[0].astype(bf16), "sp", mask)
         result = call(
             functools.partial(merge_kernel, mask, final),
-            [result[0], partner, result[1]],
+            [result[0], result[1], swap(result[2], "sp", mask)],
             done if final else open_ended,
         )
         mask *= 2
@@ -443,7 +500,7 @@
         moved[k] = swap(parts[k], "sp", k)
     own_rows, first_read = call(
         functools.partial(final_kernel, heads, rows),
-        [small, parts[0]] + [moved[k] for k in range(1, heads)],
+        [read_gain[None], parts[0]] + [moved[k] for k in range(1, heads)],
         [shape((heads, rows, DV), bf16), shape((heads, DV))],
         [pltpu.VMEM((heads, SUB, DV), f32)],
     )

time: 62.8 us -> 61.1 us (0.973)
  waiting for transfers between devices: 17.6 us -> 19.7 us
  local copies, waits for them, and re-layouts: 3.82 us -> 2.14 us
  other arithmetic: 1.47 us -> 0 us
    ppermute x20 -> x19, waiting for transfers between devices: 17.6 us -> 19.7 us  [swap(): return lax.ppermute(x, axis, flip(axis, mask))]
    another operation x3 -> x0, other arithmetic: 1.42 us -> none  [per_device(): jnp.stack([jnp.pad(named, (0, DK - named.shape[0])), read_gain.astype(f32)])]
    dynamic_slice x1 -> x0, local copies, waits for them, and re-layouts: 0.91 us -> none  [head_rows(): part = lax.dynamic_slice_in_dim(x.T, rank * heads, heads, 0)]
    another operation x2 -> x0, local copies, waits for them, and re-layouts: 0.77 us -> none  [per_device(): jnp.tile(new_query, (1, count))]
    ppermute x20 -> x19, starting transfers between devices: 18.4 us -> 18.1 us  [swap(): return lax.ppermute(x, axis, flip(axis, mask))]
  transfers between devices with their start and end apart: 20 -> 19, of which waited for: 10 -> 11; matrix products, arithmetic and copies ran while one was open for 7% -> 2% of each run, Pallas kernels for 23% -> 24%
where the time goes in v1:
time: 61.1 us; the launch traced here: 60.9 us
  Pallas kernels  20.3 us (33%)
  waiting for transfers between devices  19.7 us (32%)
  starting transfers between devices  18.1 us (30%)
  local copies, waits for them, and re-layouts  2.14 us (4%)
  between operations  0.75 us (1%)
    ppermute x19, waiting for transfers between devices, swap(): return lax.ppermute(x, axis, flip(axis, mask))  19.7 us
    ppermute x19, starting transfers between devices, swap(): return lax.ppermute(x, axis, flip(axis, mask))  18.1 us
    pallas_call x7, Pallas kernels, call(): pl.pallas_call(body, out_shape=outs, in_specs=[vmem] * len(arrays), out_s...  16.4 us
    pallas_call x1, Pallas kernels, per_device(): pl.pallas_call(functools.partial(prepare_kernel, heads), out_shape=[shape...  3.84 us
  transfers between devices with their start and end apart: 19, of which 11 were waited for; matrix products, arithmetic and copies ran while one was open for 2% of the time, Pallas kernels for 24%

profile of v1, /device:TPU:0, one launch (start us, length us, event | category | flops | bytes accessed | tf_op | source)
XLA Modules:
  0.0 60.9 jit_solution(6055103830772199528)
XLA Ops:
  0.6 1.0 %slice.15.refs_0_ = bf16[128,1024]{1,0:T(8,128)(2,1)S(1)} slice(bf16[512,1024]{1,0:T(8,128)(2,1)} %param.10), slice={[0:128], [0:1024]} | slice | bytes 524288 | tf_op jit(solution)/shard_map/slice | solution.py:402
  1.6 3.1 %collective-permute-start.9 = (bf16[128,1024]{1,0:T(8,128)(2,1)S(1)}, bf16[128,1024]{1,0:T(8,128)(2,1)S(1)}, u32[]{:S(2)}, u32[]{:S(2)}) collective-permute-start(bf16[128,1024]{1,0:T(8,128)(2,1)S(1)} %slice.15.refs_0_), channel_id=1, source_target_pairs={{0,2},{1,3},{2,0},{3,1},{4,6},{5,7},{6,4},{7,5},{8,10},{9,11},{10,... | collective-permute-start | bytes 786440 | tf_op jit(solution)/shard_map/ppermute | solution.py:26
  4.7 1.2 %fusion = (bf16[128,1024]{1,0:T(8,128)(2,1)S(1)}, bf16[128,1024]{1,0:T(8,128)(2,1)S(1)}, bf16[128,1024]{1,0:T(8,128)(2,1)S(1)}) fusion(bf16[512,1024]{1,0:T(8,128)(2,1)} %param.10), kind=kLoop, calls=%fused_computation | loop fusion | bytes 1572864 | tf_op jit(solution)/shard_map/slice | solution.py:404
  6.0 1.9 %collective-permute-start.3 = (bf16[128,1024]{1,0:T(8,128)(2,1)S(1)}, bf16[128,1024]{1,0:T(8,128)(2,1)S(1)}, u32[]{:S(2)}, u32[]{:S(2)}) collective-permute-start(bf16[128,1024]{1,0:T(8,128)(2,1)S(1)} %get-tuple-element.37.refs_0_), channel_id=1, source_target_pairs={{0,2},{1,3},{2,0},{3,1},{4,6},{5,7},{6,4},{7,5},{8,10},{9,11},{10,... | collective-permute-start | bytes 786440 | tf_op jit(solution)/shard_map/ppermute | solution.py:26
  7.9 3.9 %collective-permute-done.9.refs_1_ = bf16[128,1024]{1,0:T(8,128)(2,1)S(1)} collective-permute-done((bf16[128,1024]{1,0:T(8,128)(2,1)S(1)}, bf16[128,1024]{1,0:T(8,128)(2,1)S(1)}, u32[]{:S(2)}, u32[]{:S(2)}) %collective-permute-start.9) | collective-permute-done | bytes 262176 | tf_op jit(solution)/shard_map/ppermute | solution.py:26
  12.3 2.0 %collective-permute-start = (bf16[128,1024]{1,0:T(8,128)(2,1)S(1)}, bf16[128,1024]{1,0:T(8,128)(2,1)S(1)}, u32[]{:S(2)}, u32[]{:S(2)}) collective-permute-start(bf16[128,1024]{1,0:T(8,128)(2,1)S(1)} %get-tuple-element.38.refs_0_), channel_id=1, source_target_pairs={{0,2},{1,3},{2,0},{3,1},{4,6},{5,7},{6,4},{7,5},{8,10},{9,11},{10,... | collective-permute-start | bytes 786440 | tf_op jit(solution)/shard_map/ppermute | solution.py:26
  14.4 3.1 %collective-permute-done.6.refs_1_ = bf16[128,1024]{1,0:T(8,128)(2,1)S(1)} collective-permute-done((bf16[128,1024]{1,0:T(8,128)(2,1)S(1)}, bf16[128,1024]{1,0:T(8,128)(2,1)S(1)}, u32[]{:S(2)}, u32[]{:S(2)}) %collective-permute-start.6) | collective-permute-done | bytes 262176 | tf_op jit(solution)/shard_map/ppermute | solution.py:26
  17.4 3.8 %shard_map.113 = (bf16[4096,512]{1,0:T(8,128)(2,1)S(1)}, bf16[4096,512]{1,0:T(8,128)(2,1)S(1)}, bf16[16,4096]{1,0:T(8,128)(2,1)S(1)}, f32[8,128]{1,0:T(8,128)S(1...) custom-call(bf16[4096,512]{1,0:T(8,128)(2,1)} %refs_0_.1, bf16[4096,512]{1,0:T(8,128)(2,1)} %refs_1_.1, ...), custom_call_target="tpu_custom_call" | custom-call | tf_op jit(solution)/shard_map/pallas_call | solution.py:427
  21.3 1.8 %collective-permute-done.3.refs_1_ = bf16[128,1024]{1,0:T(8,128)(2,1)S(1)} collective-permute-done((bf16[128,1024]{1,0:T(8,128)(2,1)S(1)}, bf16[128,1024]{1,0:T(8,128)(2,1)S(1)}, u32[]{:S(2)}, u32[]{:S(2)}) %collective-permute-start.3) | collective-permute-done | bytes 262176 | tf_op jit(solution)/shard_map/ppermute | solution.py:26
  23.6 3.7 %shard_map.114.refs_9_ = f32[4,128,256]{2,1,0:T(8,128)S(1)} custom-call(bf16[128,1024]{1,0:T(8,128)(2,1)S(1)} %slice.15.refs_0_, bf16[128,1024]{1,0:T(8,128)(2,1)S(1)} %collective-permute-done.9.refs_1_, bf16[128,1024]{1,0:T(8,128)(2,1)S(1)} %collective-permute-done.10.refs_2_, bf16[128,1024]{1,0:T(8,128)(2,1)S(1)} %collective-permute-done.11.refs_3_, ...), custom_call_target="tpu_custom_call" | custom-call | flops 1610612736 | tf_op jit(solution)/shard_map/pallas_call | solution.py:368
  27.8 3.7 %shard_map.115.refs_9_ = f32[4,128,256]{2,1,0:T(8,128)S(1)} custom-call(bf16[128,1024]{1,0:T(8,128)(2,1)S(1)} %get-tuple-element.36.refs_0_, bf16[128,1024]{1,0:T(8,128)(2,1)S(1)} %collective-permute-done.6.refs_1_, bf16[128,1024]{1,0:T(8,128)(2,1)S(1)} %collective-permute-done.7.refs_2_, bf16[128,1024]{1,0:T(8,128)(2,1)S(1)} %collective-permute-done.8.refs_3_, ...), custom_call_target="tpu_custom_call" | custom-call | flops 1610612736 | tf_op jit(solution)/shard_map/pallas_call | solution.py:368
  31.5 3.7 %shard_map.116.refs_9_ = f32[4,128,256]{2,1,0:T(8,128)S(1)} custom-call(bf16[128,1024]{1,0:T(8,128)(2,1)S(1)} %get-tuple-element.37.refs_0_, bf16[128,1024]{1,0:T(8,128)(2,1)S(1)} %collective-permute-done.3.refs_1_, bf16[128,1024]{1,0:T(8,128)(2,1)S(1)} %collective-permute-done.4.refs_2_, bf16[128,1024]{1,0:T(8,128)(2,1)S(1)} %collective-permute-done.5.refs_3_, ...), custom_call_target="tpu_custom_call" | custom-call | flops 1610612736 | tf_op jit(solution)/shard_map/pallas_call | solution.py:368
  35.3 3.7 %shard_map.117 = (bf16[144,256]{1,0:T(8,128)(2,1)S(1)}, bf16[144,256]{1,0:T(8,128)(2,1)S(1)}, bf16[144,256]{1,0:T(8,128)(2,1)S(1)}, bf16[144,256]{1,0:T(8,128)(2,1)S(1)}) custom-call(bf16[128,1024]{1,0:T(8,128)(2,1)S(1)} %get-tuple-element.38.refs_0_, bf16[128,1024]{1,0:T(8,128)(2,1)S(1)} %collective-permute-done.refs_1_, ...), custom_call_target="tpu_custom_call" | custom-call | flops 1610612736 | tf_op jit(solution)/shard_map/pallas_call | solution.py:368
  39.0 2.1 %collective-permute-start.12 = (bf16[144,256]{1,0:T(8,128)(2,1)S(1)}, bf16[144,256]{1,0:T(8,128)(2,1)S(1)}, u32[]{:S(2)}, u32[]{:S(2)}) collective-permute-start(bf16[144,256]{1,0:T(8,128)(2,1)S(1)} %get-tuple-element.26), channel_id=1, source_target_pairs={{0,4},{4,0},{8,12},{12,8},{16,20},{20,16},{24,28},{28,24},{1,5},{5... | collective-permute-start | bytes 221192 | tf_op jit(solution)/shard_map/ppermute | solution.py:26
  41.0 1.6 %collective-permute-start.13 = (bf16[144,256]{1,0:T(8,128)(2,1)S(1)}, bf16[144,256]{1,0:T(8,128)(2,1)S(1)}, u32[]{:S(2)}, u32[]{:S(2)}) collective-permute-start(bf16[144,256]{1,0:T(8,128)(2,1)S(1)} %get-tuple-element.27), channel_id=1, source_target_pairs={{0,8},{4,12},{8,0},{12,4},{16,24},{20,28},{24,16},{28,20},{1,9},{5... | collective-permute-start | bytes 221192 | tf_op jit(solution)/shard_map/ppermute | solution.py:26
  42.6 1.1 %collective-permute-done.12.refs_1_ = bf16[144,256]{1,0:T(8,128)(2,1)S(1)} collective-permute-done((bf16[144,256]{1,0:T(8,128)(2,1)S(1)}, bf16[144,256]{1,0:T(8,128)(2,1)S(1)}, u32[]{:S(2)}, u32[]{:S(2)}) %collective-permute-start.12) | collective-permute-done | bytes 73760 | tf_op jit(solution)/shard_map/ppermute | solution.py:26
  43.7 2.2 %collective-permute-done.13.refs_2_ = bf16[144,256]{1,0:T(8,128)(2,1)S(1)} collective-permute-done((bf16[144,256]{1,0:T(8,128)(2,1)S(1)}, bf16[144,256]{1,0:T(8,128)(2,1)S(1)}, u32[]{:S(2)}, u32[]{:S(2)}) %collective-permute-start.13) | collective-permute-done | bytes 73760 | tf_op jit(solution)/shard_map/ppermute | solution.py:26
  45.9 1.9 %collective-permute-done.14.refs_3_ = bf16[144,256]{1,0:T(8,128)(2,1)S(1)} collective-permute-done((bf16[144,256]{1,0:T(8,128)(2,1)S(1)}, bf16[144,256]{1,0:T(8,128)(2,1)S(1)}, u32[]{:S(2)}, u32[]{:S(2)}) %collective-permute-start.14) | collective-permute-done | bytes 73760 | tf_op jit(solution)/shard_map/ppermute | solution.py:26
  48.4 2.7 %collective-permute-start.15 = (bf16[144,128]{1,0:T(8,128)(2,1)S(1)}, bf16[144,128]{1,0:T(8,128)(2,1)S(1)}, u32[]{:S(2)}, u32[]{:S(2)}) collective-permute-start(bf16[144,128]{1,0:T(8,128)(2,1)S(1)} %get-tuple-element.31), channel_id=1, source_target_pairs={{0,16},{4,20},{8,24},{12,28},{16,0},{20,4},{24,8},{28,12},{1,17},{... | collective-permute-start | bytes 110600 | tf_op jit(solution)/shard_map/ppermute | solution.py:26
  51.1 2.6 %collective-permute-done.15.refs_0_ = bf16[144,128]{1,0:T(8,128)(2,1)S(1)} collective-permute-done((bf16[144,128]{1,0:T(8,128)(2,1)S(1)}, bf16[144,128]{1,0:T(8,128)(2,1)S(1)}, u32[]{:S(2)}, u32[]{:S(2)}) %collective-permute-start.15) | collective-permute-done | bytes 36896 | tf_op jit(solution)/shard_map/ppermute | solution.py:26
  54.4 1.3 %collective-permute-start.17 = (bf16[32,128]{1,0:T(8,128)(2,1)S(1)}, bf16[32,128]{1,0:T(8,128)(2,1)S(1)}, u32[]{:S(2)}, u32[]{:S(2)}) collective-permute-start(bf16[32,128]{1,0:T(8,128)(2,1)S(1)} %get-tuple-element.34), channel_id=1, source_target_pairs={{0,8},{4,12},{8,0},{12,4},{16,24},{20,28},{24,16},{28,20},{1,9},{5... | collective-permute-start | bytes 24584 | tf_op jit(solution)/shard_map/ppermute | solution.py:26
  55.7 2.0 %collective-permute-start.18 = (bf16[32,128]{1,0:T(8,128)(2,1)S(1)}, bf16[32,128]{1,0:T(8,128)(2,1)S(1)}, u32[]{:S(2)}, u32[]{:S(2)}) collective-permute-start(bf16[32,128]{1,0:T(8,128)(2,1)S(1)} %get-tuple-element.35), channel_id=1, source_target_pairs={{0,12},{4,8},{8,4},{12,0},{16,28},{20,24},{24,20},{28,16},{1,13},{... | collective-permute-start | bytes 24584 | tf_op jit(solution)/shard_map/ppermute | solution.py:26
  58.0 2.2 %collective-permute-done.18.refs_3_ = bf16[32,128]{1,0:T(8,128)(2,1)S(1)} collective-permute-done((bf16[32,128]{1,0:T(8,128)(2,1)S(1)}, bf16[32,128]{1,0:T(8,128)(2,1)S(1)}, u32[]{:S(2)}, u32[]{:S(2)}) %collective-permute-start.18) | collective-permute-done | bytes 8224 | tf_op jit(solution)/shard_map/ppermute | solution.py:26
  60.2 0.7 %shard_map.120 = (bf16[4,16,128]{2,1,0:T(8,128)(2,1)}, f32[4,128]{1,0:T(4,128)}) custom-call(bf16[1,128]{1,0:T(2,128)(2,1)S(1)} %bitcast.5, bf16[32,128]{1,0:T(8,128)(2,1)S(1)} %get-tuple-element.32.refs_0_, bf16[32,128]{1,0:T(8,128)(2,1)S(1)} %collective-permute-done.16.refs_1_, bf16[32,128]{1,0:T(8,128)(2,1)S(1)} %collective-permute-done.17.refs_2_, ...), custom_call_target="tpu_custom_call" | custom-call | tf_op jit(solution)/shard_map/pallas_call | solution.py:368
  (26 shorter events, 3.3 us)
Async XLA Ops:
  1.6 10.2 %collective-permute-start.9 = (bf16[128,1024]{1,0:T(8,128)(2,1)S(1)}, bf16[128,1024]{1,0:T(8,128)(2,1)S(1)}, u32[]{:S(2)}, u32[]{:S(2)}) collective-permute-start(bf16[128,1024]{1,0:T(8,128)(2,1)S(1)} %slice.15.refs_0_), channel_id=1, source_target_pairs={{0,2},{1,3},{2,0},{3,1},{4,6},{5,7},{6,4},{7,5},{8,10},{9,11},{10,... | collective-permute-start | bytes 786440 | tf_op jit(solution)/shard_map/ppermute | solution.py:26
  4.7 7.7 %collective-permute-start.10 = (bf16[128,1024]{1,0:T(8,128)(2,1)S(1)}, bf16[128,1024]{1,0:T(8,128)(2,1)S(1)}, u32[]{:S(2)}, u32[]{:S(2)}) collective-permute-start(bf16[128,1024]{1,0:T(8,128)(2,1)S(1)} %slice.15.refs_0_), channel_id=1, source_target_pairs={{0,1},{1,0},{2,3},{3,2},{4,5},{5,4},{6,7},{7,6},{8,9},{9,8},{10,11... | collective-permute-start | bytes 786440 | tf_op jit(solution)/shard_map/ppermute | solution.py:26
  5.8 11.6 %collective-permute-start.6 = (bf16[128,1024]{1,0:T(8,128)(2,1)S(1)}, bf16[128,1024]{1,0:T(8,128)(2,1)S(1)}, u32[]{:S(2)}, u32[]{:S(2)}) collective-permute-start(bf16[128,1024]{1,0:T(8,128)(2,1)S(1)} %get-tuple-element.36.refs_0_), channel_id=1, source_target_pairs={{0,2},{1,3},{2,0},{3,1},{4,6},{5,7},{6,4},{7,5},{8,10},{9,11},{10,... | collective-permute-start | bytes 786440 | tf_op jit(solution)/shard_map/ppermute | solution.py:26
  6.0 17.1 %collective-permute-start.3 = (bf16[128,1024]{1,0:T(8,128)(2,1)S(1)}, bf16[128,1024]{1,0:T(8,128)(2,1)S(1)}, u32[]{:S(2)}, u32[]{:S(2)}) collective-permute-start(bf16[128,1024]{1,0:T(8,128)(2,1)S(1)} %get-tuple-element.37.refs_0_), channel_id=1, source_target_pairs={{0,2},{1,3},{2,0},{3,1},{4,6},{5,7},{6,4},{7,5},{8,10},{9,11},{10,... | collective-permute-start | bytes 786440 | tf_op jit(solution)/shard_map/ppermute | solution.py:26
  11.8 11.2 %collective-permute-start.11 = (bf16[128,1024]{1,0:T(8,128)(2,1)S(1)}, bf16[128,1024]{1,0:T(8,128)(2,1)S(1)}, u32[]{:S(2)}, u32[]{:S(2)}) collective-permute-start(bf16[128,1024]{1,0:T(8,128)(2,1)S(1)} %collective-permute-done.9.refs_1_), channel_id=1, source_target_pairs={{0,1},{1,0},{2,3},{3,2},{4,5},{5,4},{6,7},{7,6},{8,9},{9,8},{10,11... | collective-permute-start | bytes 786440 | tf_op jit(solution)/shard_map/ppermute | solution.py:26
  11.8 15.4 %collective-permute-start.7 = (bf16[128,1024]{1,0:T(8,128)(2,1)S(1)}, bf16[128,1024]{1,0:T(8,128)(2,1)S(1)}, u32[]{:S(2)}, u32[]{:S(2)}) collective-permute-start(bf16[128,1024]{1,0:T(8,128)(2,1)S(1)} %get-tuple-element.36.refs_0_), channel_id=1, source_target_pairs={{0,1},{1,0},{2,3},{3,2},{4,5},{5,4},{6,7},{7,6},{8,9},{9,8},{10,11... | collective-permute-start | bytes 786440 | tf_op jit(solution)/shard_map/ppermute | solution.py:26
  12.3 15.5 %collective-permute-start = (bf16[128,1024]{1,0:T(8,128)(2,1)S(1)}, bf16[128,1024]{1,0:T(8,128)(2,1)S(1)}, u32[]{:S(2)}, u32[]{:S(2)}) collective-permute-start(bf16[128,1024]{1,0:T(8,128)(2,1)S(1)} %get-tuple-element.38.refs_0_), channel_id=1, source_target_pairs={{0,2},{1,3},{2,0},{3,1},{4,6},{5,7},{6,4},{7,5},{8,10},{9,11},{10,... | collective-permute-start | bytes 786440 | tf_op jit(solution)/shard_map/ppermute | solution.py:26
  17.4 10.4 %collective-permute-start.8 = (bf16[128,1024]{1,0:T(8,128)(2,1)S(1)}, bf16[128,1024]{1,0:T(8,128)(2,1)S(1)}, u32[]{:S(2)}, u32[]{:S(2)}) collective-permute-start(bf16[128,1024]{1,0:T(8,128)(2,1)S(1)} %collective-permute-done.6.refs_1_), channel_id=1, source_target_pairs={{0,1},{1,0},{2,3},{3,2},{4,5},{5,4},{6,7},{7,6},{8,9},{9,8},{10,11... | collective-permute-start | bytes 786440 | tf_op jit(solution)/shard_map/ppermute | solution.py:26
  23.1 8.5 %collective-permute-start.4 = (bf16[128,1024]{1,0:T(8,128)(2,1)S(1)}, bf16[128,1024]{1,0:T(8,128)(2,1)S(1)}, u32[]{:S(2)}, u32[]{:S(2)}) collective-permute-start(bf16[128,1024]{1,0:T(8,128)(2,1)S(1)} %get-tuple-element.37.refs_0_), channel_id=1, source_target_pairs={{0,1},{1,0},{2,3},{3,2},{4,5},{5,4},{6,7},{7,6},{8,9},{9,8},{10,11... | collective-permute-start | bytes 786440 | tf_op jit(solution)/shard_map/ppermute | solution.py:26
  23.1 8.5 %collective-permute-start.5 = (bf16[128,1024]{1,0:T(8,128)(2,1)S(1)}, bf16[128,1024]{1,0:T(8,128)(2,1)S(1)}, u32[]{:S(2)}, u32[]{:S(2)}) collective-permute-start(bf16[128,1024]{1,0:T(8,128)(2,1)S(1)} %collective-permute-done.3.refs_1_), channel_id=1, source_target_pairs={{0,1},{1,0},{2,3},{3,2},{4,5},{5,4},{6,7},{7,6},{8,9},{9,8},{10,11... | collective-permute-start | bytes 786440 | tf_op jit(solution)/shard_map/ppermute | solution.py:26
  27.3 8.0 %collective-permute-start.1 = (bf16[128,1024]{1,0:T(8,128)(2,1)S(1)}, bf16[128,1024]{1,0:T(8,128)(2,1)S(1)}, u32[]{:S(2)}, u32[]{:S(2)}) collective-permute-start(bf16[128,1024]{1,0:T(8,128)(2,1)S(1)} %get-tuple-element.38.refs_0_), channel_id=1, source_target_pairs={{0,1},{1,0},{2,3},{3,2},{4,5},{5,4},{6,7},{7,6},{8,9},{9,8},{10,11... | collective-permute-start | bytes 786440 | tf_op jit(solution)/shard_map/ppermute | solution.py:26
  27.8 7.4 %collective-permute-start.2 = (bf16[128,1024]{1,0:T(8,128)(2,1)S(1)}, bf16[128,1024]{1,0:T(8,128)(2,1)S(1)}, u32[]{:S(2)}, u32[]{:S(2)}) collective-permute-start(bf16[128,1024]{1,0:T(8,128)(2,1)S(1)} %collective-permute-done.refs_1_), channel_id=1, source_target_pairs={{0,1},{1,0},{2,3},{3,2},{4,5},{5,4},{6,7},{7,6},{8,9},{9,8},{10,11... | collective-permute-start | bytes 786440 | tf_op jit(solution)/shard_map/ppermute | solution.py:26
  35.3 25.0 %copy-start = (bf16[128]{0:T(256)(128)(2,1)S(1)}, bf16[128]{0:T(256)(128)(2,1)}, u32[]{:S(2)}) copy-start(bf16[128]{0:T(256)(128)(2,1)} %param.19) | copy-start | bytes 772
  39.0 4.7 %collective-permute-start.12 = (bf16[144,256]{1,0:T(8,128)(2,1)S(1)}, bf16[144,256]{1,0:T(8,128)(2,1)S(1)}, u32[]{:S(2)}, u32[]{:S(2)}) collective-permute-start(bf16[144,256]{1,0:T(8,128)(2,1)S(1)} %get-tuple-element.26), channel_id=1, source_target_pairs={{0,4},{4,0},{8,12},{12,8},{16,20},{20,16},{24,28},{28,24},{1,5},{5... | collective-permute-start | bytes 221192 | tf_op jit(solution)/shard_map/ppermute | solution.py:26
  41.0 4.9 %collective-permute-start.13 = (bf16[144,256]{1,0:T(8,128)(2,1)S(1)}, bf16[144,256]{1,0:T(8,128)(2,1)S(1)}, u32[]{:S(2)}, u32[]{:S(2)}) collective-permute-start(bf16[144,256]{1,0:T(8,128)(2,1)S(1)} %get-tuple-element.27), channel_id=1, source_target_pairs={{0,8},{4,12},{8,0},{12,4},{16,24},{20,28},{24,16},{28,20},{1,9},{5... | collective-permute-start | bytes 221192 | tf_op jit(solution)/shard_map/ppermute | solution.py:26
  42.6 5.3 %collective-permute-start.14 = (bf16[144,256]{1,0:T(8,128)(2,1)S(1)}, bf16[144,256]{1,0:T(8,128)(2,1)S(1)}, u32[]{:S(2)}, u32[]{:S(2)}) collective-permute-start(bf16[144,256]{1,0:T(8,128)(2,1)S(1)} %get-tuple-element.28), channel_id=1, source_target_pairs={{0,12},{4,8},{8,4},{12,0},{16,28},{20,24},{24,20},{28,16},{1,13},{... | collective-permute-start | bytes 221192 | tf_op jit(solution)/shard_map/ppermute | solution.py:26
  48.4 5.3 %collective-permute-start.15 = (bf16[144,128]{1,0:T(8,128)(2,1)S(1)}, bf16[144,128]{1,0:T(8,128)(2,1)S(1)}, u32[]{:S(2)}, u32[]{:S(2)}) collective-permute-start(bf16[144,128]{1,0:T(8,128)(2,1)S(1)} %get-tuple-element.31), channel_id=1, source_target_pairs={{0,16},{4,20},{8,24},{12,28},{16,0},{20,4},{24,8},{28,12},{1,17},{... | collective-permute-start | bytes 110600 | tf_op jit(solution)/shard_map/ppermute | solution.py:26
  54.2 3.7 %collective-permute-start.16 = (bf16[32,128]{1,0:T(8,128)(2,1)S(1)}, bf16[32,128]{1,0:T(8,128)(2,1)S(1)}, u32[]{:S(2)}, u32[]{:S(2)}) collective-permute-start(bf16[32,128]{1,0:T(8,128)(2,1)S(1)} %get-tuple-element.33), channel_id=1, source_target_pairs={{0,4},{4,0},{8,12},{12,8},{16,20},{20,16},{24,28},{28,24},{1,5},{5... | collective-permute-start | bytes 24584 | tf_op jit(solution)/shard_map/ppermute | solution.py:26
  54.4 3.7 %collective-permute-start.17 = (bf16[32,128]{1,0:T(8,128)(2,1)S(1)}, bf16[32,128]{1,0:T(8,128)(2,1)S(1)}, u32[]{:S(2)}, u32[]{:S(2)}) collective-permute-start(bf16[32,128]{1,0:T(8,128)(2,1)S(1)} %get-tuple-element.34), channel_id=1, source_target_pairs={{0,8},{4,12},{8,0},{12,4},{16,24},{20,28},{24,16},{28,20},{1,9},{5... | collective-permute-start | bytes 24584 | tf_op jit(solution)/shard_map/ppermute | solution.py:26
  55.7 4.5 %collective-permute-start.18 = (bf16[32,128]{1,0:T(8,128)(2,1)S(1)}, bf16[32,128]{1,0:T(8,128)(2,1)S(1)}, u32[]{:S(2)}, u32[]{:S(2)}) collective-permute-start(bf16[32,128]{1,0:T(8,128)(2,1)S(1)} %get-tuple-element.35), channel_id=1, source_target_pairs={{0,12},{4,8},{8,4},{12,0},{16,28},{20,24},{24,20},{28,16},{1,13},{... | collective-permute-start | bytes 24584 | tf_op jit(solution)/shard_map/ppermute | solution.py:26

commit v2 on v1

--- a/solution.py
+++ b/solution.py
@@ -66,26 +66,55 @@
 def unit_inverses(lowers, size):
     row = lax.broadcasted_iota(jnp.int32, (size, size), 0)
     col = lax.broadcasted_iota(jnp.int32, (size, size), 1)
-    identity = jnp.where(row == col, 1.0, 0.0)
-
-    def same(width):
-        return (row // width) == (col // width)
-
     width = min(16, size)
-    inner = [jnp.where(same(width), low, 0.0) for low in lowers]
-    results = [identity - low for low in inner]
+    near = (row // width) == (col // width)
+    inner = [jnp.where(near, low, 0.0) for low in lowers]
+    results = [jnp.where(row == col, 1.0, 0.0) - low for low in inner]
     powers = inner
     covered = 2
     while covered < width:
         powers = [dot(p, p) for p in powers]
         results = [r + dot(r, p) for r, p in zip(results, powers)]
         covered *= 2
-    while width < size:
-        off = jnp.logical_and(same(2 * width), jnp.logical_not(same(width)))
-        right = [dot(jnp.where(off, low, 0.0), r) for low, r in zip(lowers, results)]
-        results = [r - dot(r, x) for r, x in zip(results, right)]
-        width *= 2
+    if width == size:
+        return results
+    powers = [dot(r, jnp.where(near, 0.0, low)) for r, low in zip(results, lowers)]
+    results = [r - dot(p, r) for r, p in zip(results, powers)]
+    covered = 2
+    while covered * width < size:
+        powers = [dot(p, p) for p in powers]
+        results = [r + dot(p, r) for r, p in zip(results, powers)]
+        covered *= 2
     return results
+
+
+def project(masks, piece_refs, wk_ref, wv_ref, wg_ref, sums):
+    rank = lax.axis_index("tp")
+    gates, keys, values = sums
+    placed = []
+    for m, ref in zip(masks, piece_refs):
+        width = ref.shape[1]
+        placed.append((pl.ds(pl.multiple_of((rank ^ m) * width, width), width), ref))
+    for rows, ref in placed:
+        g = dot_nt(wg_ref[:, rows], ref[...])
+        gates = g if gates is None else gates + g
+    for rows, ref in placed:
+        k = jnp.dot(ref[...], wk_ref[rows, :], preferred_element_type=f32)
+        keys = k if keys is None else keys + k
+    for rows, ref in placed:
+        v = jnp.dot(ref[...], wv_ref[rows, :], preferred_element_type=f32)
+        values = v if values is None else values + v
+    return gates, keys, values
+
+
+def part_kernel(masks, prior, *refs):
+    pieces = len(masks)
+    weights, rest = refs[pieces : pieces + 3], refs[pieces + 3 :]
+    sums = (None, None, None)
+    if prior:
+        sums, rest = tuple(ref[...] for ref in rest[:3]), rest[3:]
+    for ref, x in zip(rest, project(masks, refs[:pieces], *weights, sums)):
+        ref[...] = x
 
 
 def prepare_kernel(heads, *refs):
@@ -146,23 +175,20 @@
         copy.wait()
 
 
-def chunk_kernel(heads, index, last, masks, *refs):
+def chunk_kernel(heads, index, last, masks, prior, *refs):
     pieces = len(masks)
     piece_refs = refs[:pieces]
     wk_ref, wv_ref, wg_ref, small_ref, forget_ref = refs[pieces : pieces + 5]
     rest = refs[pieces + 5 :]
+    sums = (None, None, None)
+    if prior:
+        sums, rest = tuple(ref[...] for ref in rest[:3]), rest[3:]
     if index > 0:
         state_ref, rest = rest[0], rest[1:]
     if last:
         query_ref, rest = rest[0], rest[1:]
-    size, width = piece_refs[0].shape
-    rank = lax.axis_index("tp")
-    starts = [pl.multiple_of((rank ^ m) * width, width) for m in masks]
-
-    gates = None
-    for start, piece_ref in zip(starts, piece_refs):
-        g = dot_nt(wg_ref[:, pl.ds(start, width)], piece_ref[...])
-        gates = g if gates is None else gates + g
+    gates, key_acc, value_acc = project(masks, piece_refs, wk_ref, wv_ref, wg_ref, sums)
+    size = key_acc.shape[0]
     bias, rate = small_ref[:, 0:1], small_ref[:, 1:2]
     forget = forget_ref[:, index * size : (index + 1) * size]
     beta_row = jax.nn.sigmoid(gates[0:SUB] + bias)
@@ -184,17 +210,6 @@
     columns = stacked.T
     keep = jnp.exp(total)
 
-    key_acc = value_acc = None
-    for start, piece_ref in zip(starts, piece_refs):
-        rows = pl.ds(start, width)
-        x = piece_ref[...]
-        k = jnp.dot(x, wk_ref[rows, :], preferred_element_type=f32)
-        key_acc = k if key_acc is None else key_acc + k
-    for start, piece_ref in zip(starts, piece_refs):
-        rows = pl.ds(start, width)
-        x = piece_ref[...]
-        v = jnp.dot(x, wv_ref[rows, :], preferred_element_type=f32)
-        value_acc = v if value_acc is None else value_acc + v
     key_raw = key_acc.astype(bf16).astype(f32)
     value_raw = value_acc.astype(bf16).astype(f32)
 
@@ -443,10 +458,31 @@
 
     state = None
     flops = 2 * chunk * width * ranks * (2 * heads * DK + DK) + heads * 24 * 2 * chunk * chunk * DK
+    weights = [w_key, w_value, gate_weights]
+    sums_shape = [shape((2 * SUB, chunk)), shape((chunk, heads * DK)), shape((chunk, heads * DV))]
+
+    def part(found, sums):
+        return call(
+            functools.partial(part_kernel, tuple(m for m, _ in found), len(sums) > 0),
+            [x for _, x in found] + weights + sums,
+            sums_shape,
+            mib=16,
+            flops=2 * chunk * width * len(found) * (2 * heads * DK + DK),
+        )
+
     for c in range(chunks):
         found = gathered[c]
         last = c == chunks - 1
-        arrays = [x for _, x in found] + [w_key, w_value, gate_weights, small, forget]
+        sums = []
+        if c > 0:
+            here = [f for f in found if f[0] < 2]
+            found = [f for f in found if f[0] >= 2]
+            sums = list(part(here, sums))
+        if last and len(found) > 1:
+            near = [f for f in found if f[0] % 2 == 0]
+            found = [f for f in found if f[0] % 2 == 1]
+            sums = list(part(near, sums))
+        arrays = [x for _, x in found] + weights + [small, forget] + sums
         if c > 0:
             arrays.append(state)
         outs = [shape((heads, DK, DV + DK))]
@@ -454,7 +490,9 @@
             arrays.append(query)
             outs = [shape((DK + 2 * SUB, DV + DK), bf16)] * heads
         result = call(
-            functools.partial(chunk_kernel, heads, c, last, tuple(m for m, _ in found)),
+            functools.partial(
+                chunk_kernel, heads, c, last, tuple(m for m, _ in found), len(sums) > 0
+            ),
             arrays,
             outs,
             mib=28,

time: 61.1 us -> 63.2 us (1.034)
  waiting for transfers between devices: 19.7 us -> 21 us
  Pallas kernels: 20.3 us -> 21 us
    ppermute x19, waiting for transfers between devices: 19.7 us -> 21 us  [swap(): return lax.ppermute(x, axis, flip(axis, mask))]
    pallas_call x7 -> x11, Pallas kernels: 16.4 us -> 17.1 us  [call(): pl.pallas_call(body, out_shape=outs, in_specs=[vmem] * len(arrays), out_s...]
  transfers between devices with their start and end apart: 19 -> 19, of which waited for: 11 -> 11; matrix products, arithmetic and copies ran while one was open for 2% -> 2% of each run, Pallas kernels for 24% -> 26%
where the time goes in v2:
time: 63.2 us; the launch traced here: 63.1 us
  waiting for transfers between devices  21 us (33%)
  Pallas kernels  21 us (33%)
  starting transfers between devices  18.2 us (29%)
  local copies, waits for them, and re-layouts  2.13 us (3%)
  between operations  0.78 us (1%)
    ppermute x19, waiting for transfers between devices, swap(): return lax.ppermute(x, axis, flip(axis, mask))  21 us
    ppermute x19, starting transfers between devices, swap(): return lax.ppermute(x, axis, flip(axis, mask))  18.2 us
    pallas_call x11, Pallas kernels, call(): pl.pallas_call(body, out_shape=outs, in_specs=[vmem] * len(arrays), out_s...  17.1 us
    pallas_call x1, Pallas kernels, per_device(): pl.pallas_call(functools.partial(prepare_kernel, heads), out_shape=[shape...  3.84 us
  transfers between devices with their start and end apart: 19, of which 11 were waited for; matrix products, arithmetic and copies ran while one was open for 2% of the time, Pallas kernels for 26%

profile of v2, /device:TPU:0, one launch (start us, length us, event | category | flops | bytes accessed | tf_op | source)
XLA Modules:
  0.0 63.1 jit_solution(13973787340504462217)
XLA Ops:
  0.6 1.0 %slice.15.refs_0_ = bf16[128,1024]{1,0:T(8,128)(2,1)S(1)} slice(bf16[512,1024]{1,0:T(8,128)(2,1)} %param.10), slice={[0:128], [0:1024]} | slice | bytes 524288 | tf_op jit(solution)/shard_map/slice | solution.py:417
  1.6 3.1 %collective-permute-start.9 = (bf16[128,1024]{1,0:T(8,128)(2,1)S(1)}, bf16[128,1024]{1,0:T(8,128)(2,1)S(1)}, u32[]{:S(2)}, u32[]{:S(2)}) collective-permute-start(bf16[128,1024]{1,0:T(8,128)(2,1)S(1)} %slice.15.refs_0_), channel_id=1, source_target_pairs={{0,2},{1,3},{2,0},{3,1},{4,6},{5,7},{6,4},{7,5},{8,10},{9,11},{10,... | collective-permute-start | bytes 786440 | tf_op jit(solution)/shard_map/ppermute | solution.py:26
  4.7 1.2 %fusion = (bf16[128,1024]{1,0:T(8,128)(2,1)S(1)}, bf16[128,1024]{1,0:T(8,128)(2,1)S(1)}, bf16[128,1024]{1,0:T(8,128)(2,1)S(1)}) fusion(bf16[512,1024]{1,0:T(8,128)(2,1)} %param.10), kind=kLoop, calls=%fused_computation | loop fusion | bytes 1572864 | tf_op jit(solution)/shard_map/slice | solution.py:419
  6.4 2.0 %collective-permute-start.6 = (bf16[128,1024]{1,0:T(8,128)(2,1)S(1)}, bf16[128,1024]{1,0:T(8,128)(2,1)S(1)}, u32[]{:S(2)}, u32[]{:S(2)}) collective-permute-start(bf16[128,1024]{1,0:T(8,128)(2,1)S(1)} %get-tuple-element.60.refs_0_), channel_id=1, source_target_pairs={{0,2},{1,3},{2,0},{3,1},{4,6},{5,7},{6,4},{7,5},{8,10},{9,11},{10,... | collective-permute-start | bytes 786440 | tf_op jit(solution)/shard_map/ppermute | solution.py:26
  8.4 3.4 %collective-permute-done.9.refs_1_ = bf16[128,1024]{1,0:T(8,128)(2,1)S(1)} collective-permute-done((bf16[128,1024]{1,0:T(8,128)(2,1)S(1)}, bf16[128,1024]{1,0:T(8,128)(2,1)S(1)}, u32[]{:S(2)}, u32[]{:S(2)}) %collective-permute-start.9) | collective-permute-done | bytes 262176 | tf_op jit(solution)/shard_map/ppermute | solution.py:26
  11.8 2.0 %collective-permute-start.3 = (bf16[128,1024]{1,0:T(8,128)(2,1)S(1)}, bf16[128,1024]{1,0:T(8,128)(2,1)S(1)}, u32[]{:S(2)}, u32[]{:S(2)}) collective-permute-start(bf16[128,1024]{1,0:T(8,128)(2,1)S(1)} %get-tuple-element.61.refs_0_), channel_id=1, source_target_pairs={{0,2},{1,3},{2,0},{3,1},{4,6},{5,7},{6,4},{7,5},{8,10},{9,11},{10,... | collective-permute-start | bytes 786440 | tf_op jit(solution)/shard_map/ppermute | solution.py:26
  14.1 3.4 %collective-permute-done.refs_0_ = bf16[128,1024]{1,0:T(8,128)(2,1)S(1)} collective-permute-done((bf16[128,1024]{1,0:T(8,128)(2,1)S(1)}, bf16[128,1024]{1,0:T(8,128)(2,1)S(1)}, u32[]{:S(2)}, u32[]{:S(2)}) %collective-permute-start) | collective-permute-done | bytes 262176 | tf_op jit(solution)/shard_map/ppermute | solution.py:26
  17.4 3.8 %shard_map.113 = (bf16[4096,512]{1,0:T(8,128)(2,1)S(1)}, bf16[4096,512]{1,0:T(8,128)(2,1)S(1)}, bf16[16,4096]{1,0:T(8,128)(2,1)S(1)}, f32[8,128]{1,0:T(8,128)S(1...) custom-call(bf16[4096,512]{1,0:T(8,128)(2,1)} %refs_0_.1, bf16[4096,512]{1,0:T(8,128)(2,1)} %refs_1_.1, ...), custom_call_target="tpu_custom_call" | custom-call | tf_op jit(solution)/shard_map/pallas_call | solution.py:442
  23.3 0.9 %shard_map.117 = (f32[16,128]{1,0:T(8,128)S(1)}, f32[128,512]{1,0:T(8,128)S(1)}, f32[128,512]{1,0:T(8,128)S(1)}) custom-call(bf16[128,1024]{1,0:T(8,128)(2,1)S(1)} %get-tuple-element.60.refs_0_, bf16[128,1024]{1,0:T(8,128)(2,1)S(1)} %collective-permute-done.8.refs_1_, bf16[4096,512]{1,0:T(8,128)(2,1)S(1)} %get-tuple-element.31.refs_2_.refs_1_.refs_4_, ...), custom_call_target="tpu_custom_call" | custom-call | flops 603979776 | tf_op jit(solution)/shard_map/pallas_call | solution.py:383
  24.5 3.3 %collective-permute-done.3.refs_0_ = bf16[128,1024]{1,0:T(8,128)(2,1)S(1)} collective-permute-done((bf16[128,1024]{1,0:T(8,128)(2,1)S(1)}, bf16[128,1024]{1,0:T(8,128)(2,1)S(1)}, u32[]{:S(2)}, u32[]{:S(2)}) %collective-permute-start.3) | collective-permute-done | bytes 262176 | tf_op jit(solution)/shard_map/ppermute | solution.py:26
  28.7 3.7 %shard_map.118.refs_10_ = f32[4,128,256]{2,1,0:T(8,128)S(1)} custom-call(bf16[128,1024]{1,0:T(8,128)(2,1)S(1)} %slice.15.refs_0_, bf16[128,1024]{1,0:T(8,128)(2,1)S(1)} %collective-permute-done.9.refs_1_, bf16[128,1024]{1,0:T(8,128)(2,1)S(1)} %collective-permute-done.10.refs_2_, bf16[128,1024]{1,0:T(8,128)(2,1)S(1)} %collective-permute-done.11.refs_3_, ...), custom_call_target="tpu_custom_call" | custom-call | flops 1610612736 | tf_op jit(solution)/shard_map/pallas_call | solution.py:383
  32.4 3.0 %shard_map.119.refs_10_ = f32[4,128,256]{2,1,0:T(8,128)S(1)} custom-call(bf16[128,1024]{1,0:T(8,128)(2,1)S(1)} %collective-permute-done.6.refs_0_, bf16[128,1024]{1,0:T(8,128)(2,1)S(1)} %collective-permute-done.7.refs_1_, bf16[4096,512]{1,0:T(8,128)(2,1)S(1)} %get-tuple-element.31.refs_2_.refs_1_.refs_4_, ...), custom_call_target="tpu_custom_call" | custom-call | flops 1610612736 | tf_op jit(solution)/shard_map/pallas_call | solution.py:383
  35.4 3.0 %shard_map.120.refs_9_ = f32[4,128,256]{2,1,0:T(8,128)S(1)} custom-call(bf16[128,1024]{1,0:T(8,128)(2,1)S(1)} %collective-permute-done.3.refs_0_, bf16[128,1024]{1,0:T(8,128)(2,1)S(1)} %collective-permute-done.4.refs_1_, bf16[4096,512]{1,0:T(8,128)(2,1)S(1)} %get-tuple-element.31.refs_2_.refs_1_.refs_4_, ...), custom_call_target="tpu_custom_call" | custom-call | flops 1610612736 | tf_op jit(solution)/shard_map/pallas_call | solution.py:383
  38.4 2.7 %shard_map.121 = (bf16[144,256]{1,0:T(8,128)(2,1)S(1)}, bf16[144,256]{1,0:T(8,128)(2,1)S(1)}, bf16[144,256]{1,0:T(8,128)(2,1)S(1)}, bf16[144,256]{1,0:T(8,128)(2,1)S(1)}) custom-call(bf16[128,1024]{1,0:T(8,128)(2,1)S(1)} %collective-permute-done.1.refs_0_, bf16[4096,512]{1,0:T(8,128)(2,1)S(1)} %get-tuple-element.31.refs_2_.refs_1_.refs_4_, ...), custom_call_target="tpu_custom_call" | custom-call | flops 1610612736 | tf_op jit(solution)/shard_map/pallas_call | solution.py:383
  41.1 1.8 %collective-permute-start.12 = (bf16[144,256]{1,0:T(8,128)(2,1)S(1)}, bf16[144,256]{1,0:T(8,128)(2,1)S(1)}, u32[]{:S(2)}, u32[]{:S(2)}) collective-permute-start(bf16[144,256]{1,0:T(8,128)(2,1)S(1)} %get-tuple-element.50), channel_id=1, source_target_pairs={{0,4},{4,0},{8,12},{12,8},{16,20},{20,16},{24,28},{28,24},{1,5},{5... | collective-permute-start | bytes 221192 | tf_op jit(solution)/shard_map/ppermute | solution.py:26
  42.9 1.6 %collective-permute-start.13 = (bf16[144,256]{1,0:T(8,128)(2,1)S(1)}, bf16[144,256]{1,0:T(8,128)(2,1)S(1)}, u32[]{:S(2)}, u32[]{:S(2)}) collective-permute-start(bf16[144,256]{1,0:T(8,128)(2,1)S(1)} %get-tuple-element.51), channel_id=1, source_target_pairs={{0,8},{4,12},{8,0},{12,4},{16,24},{20,28},{24,16},{28,20},{1,9},{5... | collective-permute-start | bytes 221192 | tf_op jit(solution)/shard_map/ppermute | solution.py:26
  44.7 1.2 %collective-permute-done.12.refs_1_ = bf16[144,256]{1,0:T(8,128)(2,1)S(1)} collective-permute-done((bf16[144,256]{1,0:T(8,128)(2,1)S(1)}, bf16[144,256]{1,0:T(8,128)(2,1)S(1)}, u32[]{:S(2)}, u32[]{:S(2)}) %collective-permute-start.12) | collective-permute-done | bytes 73760 | tf_op jit(solution)/shard_map/ppermute | solution.py:26
  45.9 1.7 %collective-permute-done.13.refs_2_ = bf16[144,256]{1,0:T(8,128)(2,1)S(1)} collective-permute-done((bf16[144,256]{1,0:T(8,128)(2,1)S(1)}, bf16[144,256]{1,0:T(8,128)(2,1)S(1)}, u32[]{:S(2)}, u32[]{:S(2)}) %collective-permute-start.13) | collective-permute-done | bytes 73760 | tf_op jit(solution)/shard_map/ppermute | solution.py:26
  47.6 2.1 %collective-permute-done.14.refs_3_ = bf16[144,256]{1,0:T(8,128)(2,1)S(1)} collective-permute-done((bf16[144,256]{1,0:T(8,128)(2,1)S(1)}, bf16[144,256]{1,0:T(8,128)(2,1)S(1)}, u32[]{:S(2)}, u32[]{:S(2)}) %collective-permute-start.14) | collective-permute-done | bytes 73760 | tf_op jit(solution)/shard_map/ppermute | solution.py:26
  50.3 2.6 %collective-permute-start.15 = (bf16[144,128]{1,0:T(8,128)(2,1)S(1)}, bf16[144,128]{1,0:T(8,128)(2,1)S(1)}, u32[]{:S(2)}, u32[]{:S(2)}) collective-permute-start(bf16[144,128]{1,0:T(8,128)(2,1)S(1)} %get-tuple-element.55), channel_id=1, source_target_pairs={{0,16},{4,20},{8,24},{12,28},{16,0},{20,4},{24,8},{28,12},{1,17},{... | collective-permute-start | bytes 110600 | tf_op jit(solution)/shard_map/ppermute | solution.py:26
  52.9 2.7 %collective-permute-done.15.refs_0_ = bf16[144,128]{1,0:T(8,128)(2,1)S(1)} collective-permute-done((bf16[144,128]{1,0:T(8,128)(2,1)S(1)}, bf16[144,128]{1,0:T(8,128)(2,1)S(1)}, u32[]{:S(2)}, u32[]{:S(2)}) %collective-permute-start.15) | collective-permute-done | bytes 36896 | tf_op jit(solution)/shard_map/ppermute | solution.py:26
  56.3 1.6 %collective-permute-start.17 = (bf16[32,128]{1,0:T(8,128)(2,1)S(1)}, bf16[32,128]{1,0:T(8,128)(2,1)S(1)}, u32[]{:S(2)}, u32[]{:S(2)}) collective-permute-start(bf16[32,128]{1,0:T(8,128)(2,1)S(1)} %get-tuple-element.58), channel_id=1, source_target_pairs={{0,8},{4,12},{8,0},{12,4},{16,24},{20,28},{24,16},{28,20},{1,9},{5... | collective-permute-start | bytes 24584 | tf_op jit(solution)/shard_map/ppermute | solution.py:26
  57.8 1.7 %collective-permute-start.18 = (bf16[32,128]{1,0:T(8,128)(2,1)S(1)}, bf16[32,128]{1,0:T(8,128)(2,1)S(1)}, u32[]{:S(2)}, u32[]{:S(2)}) collective-permute-start(bf16[32,128]{1,0:T(8,128)(2,1)S(1)} %get-tuple-element.59), channel_id=1, source_target_pairs={{0,12},{4,8},{8,4},{12,0},{16,28},{20,24},{24,20},{28,16},{1,13},{... | collective-permute-start | bytes 24584 | tf_op jit(solution)/shard_map/ppermute | solution.py:26
  59.9 2.5 %collective-permute-done.18.refs_3_ = bf16[32,128]{1,0:T(8,128)(2,1)S(1)} collective-permute-done((bf16[32,128]{1,0:T(8,128)(2,1)S(1)}, bf16[32,128]{1,0:T(8,128)(2,1)S(1)}, u32[]{:S(2)}, u32[]{:S(2)}) %collective-permute-start.18) | collective-permute-done | bytes 8224 | tf_op jit(solution)/shard_map/ppermute | solution.py:26
  (30 shorter events, 6.5 us)
Async XLA Ops:
  1.6 10.2 %collective-permute-start.9 = (bf16[128,1024]{1,0:T(8,128)(2,1)S(1)}, bf16[128,1024]{1,0:T(8,128)(2,1)S(1)}, u32[]{:S(2)}, u32[]{:S(2)}) collective-permute-start(bf16[128,1024]{1,0:T(8,128)(2,1)S(1)} %slice.15.refs_0_), channel_id=1, source_target_pairs={{0,2},{1,3},{2,0},{3,1},{4,6},{5,7},{6,4},{7,5},{8,10},{9,11},{10,... | collective-permute-start | bytes 786440 | tf_op jit(solution)/shard_map/ppermute | solution.py:26
  5.8 6.0 %collective-permute-start.8 = (bf16[128,1024]{1,0:T(8,128)(2,1)S(1)}, bf16[128,1024]{1,0:T(8,128)(2,1)S(1)}, u32[]{:S(2)}, u32[]{:S(2)}) collective-permute-start(bf16[128,1024]{1,0:T(8,128)(2,1)S(1)} %get-tuple-element.60.refs_0_), channel_id=1, source_target_pairs={{0,1},{1,0},{2,3},{3,2},{4,5},{5,4},{6,7},{7,6},{8,9},{9,8},{10,11... | collective-permute-start | bytes 786440 | tf_op jit(solution)/shard_map/ppermute | solution.py:26
  5.9 7.9 %collective-permute-start.2 = (bf16[128,1024]{1,0:T(8,128)(2,1)S(1)}, bf16[128,1024]{1,0:T(8,128)(2,1)S(1)}, u32[]{:S(2)}, u32[]{:S(2)}) collective-permute-start(bf16[128,1024]{1,0:T(8,128)(2,1)S(1)} %get-tuple-element.62.refs_0_), channel_id=1, source_target_pairs={{0,1},{1,0},{2,3},{3,2},{4,5},{5,4},{6,7},{7,6},{8,9},{9,8},{10,11... | collective-permute-start | bytes 786440 | tf_op jit(solution)/shard_map/ppermute | solution.py:26
  6.4 11.0 %collective-permute-start = (bf16[128,1024]{1,0:T(8,128)(2,1)S(1)}, bf16[128,1024]{1,0:T(8,128)(2,1)S(1)}, u32[]{:S(2)}, u32[]{:S(2)}) collective-permute-start(bf16[128,1024]{1,0:T(8,128)(2,1)S(1)} %get-tuple-element.62.refs_0_), channel_id=1, source_target_pairs={{0,2},{1,3},{2,0},{3,1},{4,6},{5,7},{6,4},{7,5},{8,10},{9,11},{10,... | collective-permute-start | bytes 786440 | tf_op jit(solution)/shard_map/ppermute | solution.py:26
  6.4 16.6 %collective-permute-start.6 = (bf16[128,1024]{1,0:T(8,128)(2,1)S(1)}, bf16[128,1024]{1,0:T(8,128)(2,1)S(1)}, u32[]{:S(2)}, u32[]{:S(2)}) collective-permute-start(bf16[128,1024]{1,0:T(8,128)(2,1)S(1)} %get-tuple-element.60.refs_0_), channel_id=1, source_target_pairs={{0,2},{1,3},{2,0},{3,1},{4,6},{5,7},{6,4},{7,5},{8,10},{9,11},{10,... | collective-permute-start | bytes 786440 | tf_op jit(solution)/shard_map/ppermute | solution.py:26
  11.8 12.3 %collective-permute-start.5 = (bf16[128,1024]{1,0:T(8,128)(2,1)S(1)}, bf16[128,1024]{1,0:T(8,128)(2,1)S(1)}, u32[]{:S(2)}, u32[]{:S(2)}) collective-permute-start(bf16[128,1024]{1,0:T(8,128)(2,1)S(1)} %get-tuple-element.61.refs_0_), channel_id=1, source_target_pairs={{0,1},{1,0},{2,3},{3,2},{4,5},{5,4},{6,7},{7,6},{8,9},{9,8},{10,11... | collective-permute-start | bytes 786440 | tf_op jit(solution)/shard_map/ppermute | solution.py:26
  11.8 16.0 %collective-permute-start.3 = (bf16[128,1024]{1,0:T(8,128)(2,1)S(1)}, bf16[128,1024]{1,0:T(8,128)(2,1)S(1)}, u32[]{:S(2)}, u32[]{:S(2)}) collective-permute-start(bf16[128,1024]{1,0:T(8,128)(2,1)S(1)} %get-tuple-element.61.refs_0_), channel_id=1, source_target_pairs={{0,2},{1,3},{2,0},{3,1},{4,6},{5,7},{6,4},{7,5},{8,10},{9,11},{10,... | collective-permute-start | bytes 786440 | tf_op jit(solution)/shard_map/ppermute | solution.py:26
  13.8 14.8 %collective-permute-start.10 = (bf16[128,1024]{1,0:T(8,128)(2,1)S(1)}, bf16[128,1024]{1,0:T(8,128)(2,1)S(1)}, u32[]{:S(2)}, u32[]{:S(2)}) collective-permute-start(bf16[128,1024]{1,0:T(8,128)(2,1)S(1)} %slice.15.refs_0_), channel_id=1, source_target_pairs={{0,1},{1,0},{2,3},{3,2},{4,5},{5,4},{6,7},{7,6},{8,9},{9,8},{10,11... | collective-permute-start | bytes 786440 | tf_op jit(solution)/shard_map/ppermute | solution.py:26
  17.4 11.3 %collective-permute-start.11 = (bf16[128,1024]{1,0:T(8,128)(2,1)S(1)}, bf16[128,1024]{1,0:T(8,128)(2,1)S(1)}, u32[]{:S(2)}, u32[]{:S(2)}) collective-permute-start(bf16[128,1024]{1,0:T(8,128)(2,1)S(1)} %collective-permute-done.9.refs_1_), channel_id=1, source_target_pairs={{0,1},{1,0},{2,3},{3,2},{4,5},{5,4},{6,7},{7,6},{8,9},{9,8},{10,11... | collective-permute-start | bytes 786440 | tf_op jit(solution)/shard_map/ppermute | solution.py:26
  23.1 9.3 %collective-permute-start.7 = (bf16[128,1024]{1,0:T(8,128)(2,1)S(1)}, bf16[128,1024]{1,0:T(8,128)(2,1)S(1)}, u32[]{:S(2)}, u32[]{:S(2)}) collective-permute-start(bf16[128,1024]{1,0:T(8,128)(2,1)S(1)} %collective-permute-done.6.refs_0_), channel_id=1, source_target_pairs={{0,1},{1,0},{2,3},{3,2},{4,5},{5,4},{6,7},{7,6},{8,9},{9,8},{10,11... | collective-permute-start | bytes 786440 | tf_op jit(solution)/shard_map/ppermute | solution.py:26
  24.1 14.3 %collective-permute-start.1 = (bf16[128,1024]{1,0:T(8,128)(2,1)S(1)}, bf16[128,1024]{1,0:T(8,128)(2,1)S(1)}, u32[]{:S(2)}, u32[]{:S(2)}) collective-permute-start(bf16[128,1024]{1,0:T(8,128)(2,1)S(1)} %collective-permute-done.refs_0_), channel_id=1, source_target_pairs={{0,1},{1,0},{2,3},{3,2},{4,5},{5,4},{6,7},{7,6},{8,9},{9,8},{10,11... | collective-permute-start | bytes 786440 | tf_op jit(solution)/shard_map/ppermute | solution.py:26
  27.8 7.6 %collective-permute-start.4 = (bf16[128,1024]{1,0:T(8,128)(2,1)S(1)}, bf16[128,1024]{1,0:T(8,128)(2,1)S(1)}, u32[]{:S(2)}, u32[]{:S(2)}) collective-permute-start(bf16[128,1024]{1,0:T(8,128)(2,1)S(1)} %collective-permute-done.3.refs_0_), channel_id=1, source_target_pairs={{0,1},{1,0},{2,3},{3,2},{4,5},{5,4},{6,7},{7,6},{8,9},{9,8},{10,11... | collective-permute-start | bytes 786440 | tf_op jit(solution)/shard_map/ppermute | solution.py:26
  38.4 23.9 %copy-start = (bf16[128]{0:T(256)(128)(2,1)S(1)}, bf16[128]{0:T(256)(128)(2,1)}, u32[]{:S(2)}) copy-start(bf16[128]{0:T(256)(128)(2,1)} %param.19) | copy-start | bytes 772
  41.1 4.8 %collective-permute-start.12 = (bf16[144,256]{1,0:T(8,128)(2,1)S(1)}, bf16[144,256]{1,0:T(8,128)(2,1)S(1)}, u32[]{:S(2)}, u32[]{:S(2)}) collective-permute-start(bf16[144,256]{1,0:T(8,128)(2,1)S(1)} %get-tuple-element.50), channel_id=1, source_target_pairs={{0,4},{4,0},{8,12},{12,8},{16,20},{20,16},{24,28},{28,24},{1,5},{5... | collective-permute-start | bytes 221192 | tf_op jit(solution)/shard_map/ppermute | solution.py:26
  42.9 4.7 %collective-permute-start.13 = (bf16[144,256]{1,0:T(8,128)(2,1)S(1)}, bf16[144,256]{1,0:T(8,128)(2,1)S(1)}, u32[]{:S(2)}, u32[]{:S(2)}) collective-permute-start(bf16[144,256]{1,0:T(8,128)(2,1)S(1)} %get-tuple-element.51), channel_id=1, source_target_pairs={{0,8},{4,12},{8,0},{12,4},{16,24},{20,28},{24,16},{28,20},{1,9},{5... | collective-permute-start | bytes 221192 | tf_op jit(solution)/shard_map/ppermute | solution.py:26
  44.5 5.3 %collective-permute-start.14 = (bf16[144,256]{1,0:T(8,128)(2,1)S(1)}, bf16[144,256]{1,0:T(8,128)(2,1)S(1)}, u32[]{:S(2)}, u32[]{:S(2)}) collective-permute-start(bf16[144,256]{1,0:T(8,128)(2,1)S(1)} %get-tuple-element.52), channel_id=1, source_target_pairs={{0,12},{4,8},{8,4},{12,0},{16,28},{20,24},{24,20},{28,16},{1,13},{... | collective-permute-start | bytes 221192 | tf_op jit(solution)/shard_map/ppermute | solution.py:26
  50.3 5.3 %collective-permute-start.15 = (bf16[144,128]{1,0:T(8,128)(2,1)S(1)}, bf16[144,128]{1,0:T(8,128)(2,1)S(1)}, u32[]{:S(2)}, u32[]{:S(2)}) collective-permute-start(bf16[144,128]{1,0:T(8,128)(2,1)S(1)} %get-tuple-element.55), channel_id=1, source_target_pairs={{0,16},{4,20},{8,24},{12,28},{16,0},{20,4},{24,8},{28,12},{1,17},{... | collective-permute-start | bytes 110600 | tf_op jit(solution)/shard_map/ppermute | solution.py:26
  56.0 3.7 %collective-permute-start.16 = (bf16[32,128]{1,0:T(8,128)(2,1)S(1)}, bf16[32,128]{1,0:T(8,128)(2,1)S(1)}, u32[]{:S(2)}, u32[]{:S(2)}) collective-permute-start(bf16[32,128]{1,0:T(8,128)(2,1)S(1)} %get-tuple-element.57), channel_id=1, source_target_pairs={{0,4},{4,0},{8,12},{12,8},{16,20},{20,16},{24,28},{28,24},{1,5},{5... | collective-permute-start | bytes 24584 | tf_op jit(solution)/shard_map/ppermute | solution.py:26
  56.3 3.7 %collective-permute-start.17 = (bf16[32,128]{1,0:T(8,128)(2,1)S(1)}, bf16[32,128]{1,0:T(8,128)(2,1)S(1)}, u32[]{:S(2)}, u32[]{:S(2)}) collective-permute-start(bf16[32,128]{1,0:T(8,128)(2,1)S(1)} %get-tuple-element.58), channel_id=1, source_target_pairs={{0,8},{4,12},{8,0},{12,4},{16,24},{20,28},{24,16},{28,20},{1,9},{5... | collective-permute-start | bytes 24584 | tf_op jit(solution)/shard_map/ppermute | solution.py:26
  57.8 4.5 %collective-permute-start.18 = (bf16[32,128]{1,0:T(8,128)(2,1)S(1)}, bf16[32,128]{1,0:T(8,128)(2,1)S(1)}, u32[]{:S(2)}, u32[]{:S(2)}) collective-permute-start(bf16[32,128]{1,0:T(8,128)(2,1)S(1)} %get-tuple-element.59), channel_id=1, source_target_pairs={{0,12},{4,8},{8,4},{12,0},{16,28},{20,24},{24,20},{28,16},{1,13},{... | collective-permute-start | bytes 24584 | tf_op jit(solution)/shard_map/ppermute | solution.py:26

commit v3 on v2

--- a/solution.py
+++ b/solution.py
@@ -54,12 +54,6 @@
 def dot_nt(left, right):
     return lax.dot_general(
         left.astype(bf16), right.astype(bf16), (((1,), (1,)), ((), ())), preferred_element_type=f32
-    )
-
-
-def dot_tn(left, right):
-    return lax.dot_general(
-        left.astype(bf16), right.astype(bf16), (((0,), (0,)), ((), ())), preferred_element_type=f32
     )
 
 
@@ -195,52 +189,40 @@
     log_row = forget - rate * jax.nn.softplus(gates[SUB : 2 * SUB])
     row = lax.broadcasted_iota(jnp.int32, (size, size), 0)
     col = lax.broadcasted_iota(jnp.int32, (size, size), 1)
-    cum_row = dot_ones(log_row, jnp.where(row <= col, 1.0, 0.0))
-    total = cum_row[:, size - 1 : size]
-    stacked = jnp.concatenate(
-        [
-            beta_row,
-            cum_row,
-            beta_row * jnp.exp(cum_row),
-            jnp.exp(total - cum_row),
-            jnp.zeros((DK - 4 * SUB, size), f32),
-        ],
-        axis=0,
-    )
-    columns = stacked.T
-    keep = jnp.exp(total)
+    strict = row > col
+    after = dot_ones(log_row, jnp.where(strict, 1.0, 0.0))
+    keep = jnp.exp(after[:, 0:1] + log_row[:, 0:1])
+    remain = jnp.exp(after)
 
     key_raw = key_acc.astype(bf16).astype(f32)
-    value_raw = value_acc.astype(bf16).astype(f32)
-
-    strict = row > col
-    keys, lowers, base = [], [], []
+    value_raw = value_acc.astype(bf16)
+    keys, lowers = [], []
     for h in range(heads):
         kw = key_raw[:, h * DK : (h + 1) * DK]
         ku = kw * lax.rsqrt(jnp.sum(kw * kw, axis=-1, keepdims=True) + norm_eps)
-        beta = columns[:, h : h + 1]
-        cum = columns[:, SUB + h : SUB + h + 1]
-        spread = jnp.where(strict, cum - cum_row[h : h + 1, :], 0.0)
-        table = jnp.where(strict, jnp.exp(spread), 0.0)
         keys.append(ku)
-        lowers.append(dot_nt(ku, ku) * table * beta)
+        lowers.append(jnp.where(strict, dot_nt(ku, ku), 0.0) * beta_row[h : h + 1, :])
     if index > 0:
         states = [state_ref[h] for h in range(heads)]
     else:
         kr = lax.broadcasted_iota(jnp.int32, (DK, DV + DK), 0)
         kc = lax.broadcasted_iota(jnp.int32, (DK, DV + DK), 1)
         states = [jnp.where(kc == kr + DV, 1.0, 0.0)] * heads
+    rights, turned = [], []
     for h in range(heads):
-        beta = columns[:, h : h + 1]
-        erase = keys[h] * columns[:, 2 * SUB + h : 2 * SUB + h + 1]
-        value = value_raw[:, h * DV : (h + 1) * DV] * beta
-        padded = jnp.concatenate([value, jnp.zeros((size, DK), f32)], axis=1)
-        base.append(padded - dot(erase, states[h]))
-    inverses = unit_inverses(lowers, size)
-    fresh = [dot(inv, b) for inv, b in zip(inverses, base)]
+        value = value_raw[:, h * DV : (h + 1) * DV]
+        padded = jnp.concatenate([value, jnp.zeros((size, DK), bf16)], axis=1)
+        seen = dot(keys[h], states[h]).astype(bf16)
+        rights.append(jnp.concatenate([padded, seen], axis=0))
+        turned.append(keys[h].T * beta_row[h : h + 1, :])
+    fresh = []
+    for h, inverse in enumerate(unit_inverses(lowers, size)):
+        left = jnp.concatenate(
+            [inverse * remain[h : h + 1, :], inverse * -keep[h : h + 1, :]], axis=1
+        )
+        fresh.append(dot(left, rights[h]))
     for h in range(heads):
-        remain = keys[h] * columns[:, 3 * SUB + h : 3 * SUB + h + 1]
-        new = keep[h : h + 1, :] * states[h] + dot_tn(remain, fresh[h])
+        new = keep[h : h + 1, :] * states[h] + dot(turned[h], fresh[h])
         if last:
             rest[h][0:DK, :] = new.astype(bf16)
             asked = jnp.broadcast_to(query_ref[h : h + 1, :], (2 * SUB, DK))

time: 63.2 us -> 61.4 us (0.972)
  Pallas kernels: 21 us -> 19.1 us
    pallas_call x11, Pallas kernels: 17.1 us -> 15.3 us  [call(): pl.pallas_call(body, out_shape=outs, in_specs=[vmem] * len(arrays), out_s...]
  transfers between devices with their start and end apart: 19 -> 19, of which waited for: 11 -> 11; matrix products, arithmetic and copies ran while one was open for 2% -> 2% of each run, Pallas kernels for 26% -> 25%
where the time goes in v3:
time: 61.4 us; the launch traced here: 61.2 us
  waiting for transfers between devices  21.1 us (34%)
  Pallas kernels  19.1 us (31%)
  starting transfers between devices  18.2 us (30%)
  local copies, waits for them, and re-layouts  2.13 us (3%)
  between operations  0.78 us (1%)
    ppermute x19, waiting for transfers between devices, swap(): return lax.ppermute(x, axis, flip(axis, mask))  21.1 us
    ppermute x19, starting transfers between devices, swap(): return lax.ppermute(x, axis, flip(axis, mask))  18.2 us
    pallas_call x11, Pallas kernels, call(): pl.pallas_call(body, out_shape=outs, in_specs=[vmem] * len(arrays), out_s...  15.3 us
    pallas_call x1, Pallas kernels, per_device(): pl.pallas_call(functools.partial(prepare_kernel, heads), out_shape=[shape...  3.84 us
  transfers between devices with their start and end apart: 19, of which 11 were waited for; matrix products, arithmetic and copies ran while one was open for 2% of the time, Pallas kernels for 25%

profile of v3, /device:TPU:0, one launch (start us, length us, event | category | flops | bytes accessed | tf_op | source)
XLA Modules:
  0.0 61.2 jit_solution(3078450203916207695)
XLA Ops:
  0.6 1.0 %slice.15.refs_0_ = bf16[128,1024]{1,0:T(8,128)(2,1)S(1)} slice(bf16[512,1024]{1,0:T(8,128)(2,1)} %param.10), slice={[0:128], [0:1024]} | slice | bytes 524288 | tf_op jit(solution)/shard_map/slice | solution.py:399
  1.6 3.1 %collective-permute-start.9 = (bf16[128,1024]{1,0:T(8,128)(2,1)S(1)}, bf16[128,1024]{1,0:T(8,128)(2,1)S(1)}, u32[]{:S(2)}, u32[]{:S(2)}) collective-permute-start(bf16[128,1024]{1,0:T(8,128)(2,1)S(1)} %slice.15.refs_0_), channel_id=1, source_target_pairs={{0,2},{1,3},{2,0},{3,1},{4,6},{5,7},{6,4},{7,5},{8,10},{9,11},{10,... | collective-permute-start | bytes 786440 | tf_op jit(solution)/shard_map/ppermute | solution.py:26
  4.7 1.2 %fusion = (bf16[128,1024]{1,0:T(8,128)(2,1)S(1)}, bf16[128,1024]{1,0:T(8,128)(2,1)S(1)}, bf16[128,1024]{1,0:T(8,128)(2,1)S(1)}) fusion(bf16[512,1024]{1,0:T(8,128)(2,1)} %param.10), kind=kLoop, calls=%fused_computation | loop fusion | bytes 1572864 | tf_op jit(solution)/shard_map/slice | solution.py:401
  6.4 2.0 %collective-permute-start.6 = (bf16[128,1024]{1,0:T(8,128)(2,1)S(1)}, bf16[128,1024]{1,0:T(8,128)(2,1)S(1)}, u32[]{:S(2)}, u32[]{:S(2)}) collective-permute-start(bf16[128,1024]{1,0:T(8,128)(2,1)S(1)} %get-tuple-element.60.refs_0_), channel_id=1, source_target_pairs={{0,2},{1,3},{2,0},{3,1},{4,6},{5,7},{6,4},{7,5},{8,10},{9,11},{10,... | collective-permute-start | bytes 786440 | tf_op jit(solution)/shard_map/ppermute | solution.py:26
  8.4 3.4 %collective-permute-done.9.refs_1_ = bf16[128,1024]{1,0:T(8,128)(2,1)S(1)} collective-permute-done((bf16[128,1024]{1,0:T(8,128)(2,1)S(1)}, bf16[128,1024]{1,0:T(8,128)(2,1)S(1)}, u32[]{:S(2)}, u32[]{:S(2)}) %collective-permute-start.9) | collective-permute-done | bytes 262176 | tf_op jit(solution)/shard_map/ppermute | solution.py:26
  11.8 2.0 %collective-permute-start.3 = (bf16[128,1024]{1,0:T(8,128)(2,1)S(1)}, bf16[128,1024]{1,0:T(8,128)(2,1)S(1)}, u32[]{:S(2)}, u32[]{:S(2)}) collective-permute-start(bf16[128,1024]{1,0:T(8,128)(2,1)S(1)} %get-tuple-element.61.refs_0_), channel_id=1, source_target_pairs={{0,2},{1,3},{2,0},{3,1},{4,6},{5,7},{6,4},{7,5},{8,10},{9,11},{10,... | collective-permute-start | bytes 786440 | tf_op jit(solution)/shard_map/ppermute | solution.py:26
  14.1 3.4 %collective-permute-done.refs_0_ = bf16[128,1024]{1,0:T(8,128)(2,1)S(1)} collective-permute-done((bf16[128,1024]{1,0:T(8,128)(2,1)S(1)}, bf16[128,1024]{1,0:T(8,128)(2,1)S(1)}, u32[]{:S(2)}, u32[]{:S(2)}) %collective-permute-start) | collective-permute-done | bytes 262176 | tf_op jit(solution)/shard_map/ppermute | solution.py:26
  17.4 3.8 %shard_map.113 = (bf16[4096,512]{1,0:T(8,128)(2,1)S(1)}, bf16[4096,512]{1,0:T(8,128)(2,1)S(1)}, bf16[16,4096]{1,0:T(8,128)(2,1)S(1)}, f32[8,128]{1,0:T(8,128)S(1...) custom-call(bf16[4096,512]{1,0:T(8,128)(2,1)} %refs_0_.1, bf16[4096,512]{1,0:T(8,128)(2,1)} %refs_1_.1, ...), custom_call_target="tpu_custom_call" | custom-call | tf_op jit(solution)/shard_map/pallas_call | solution.py:424
  23.3 0.9 %shard_map.117 = (f32[16,128]{1,0:T(8,128)S(1)}, f32[128,512]{1,0:T(8,128)S(1)}, f32[128,512]{1,0:T(8,128)S(1)}) custom-call(bf16[128,1024]{1,0:T(8,128)(2,1)S(1)} %get-tuple-element.60.refs_0_, bf16[128,1024]{1,0:T(8,128)(2,1)S(1)} %collective-permute-done.8.refs_1_, bf16[4096,512]{1,0:T(8,128)(2,1)S(1)} %get-tuple-element.31.refs_2_.refs_1_.refs_4_, ...), custom_call_target="tpu_custom_call" | custom-call | flops 603979776 | tf_op jit(solution)/shard_map/pallas_call | solution.py:365
  24.5 3.3 %collective-permute-done.3.refs_0_ = bf16[128,1024]{1,0:T(8,128)(2,1)S(1)} collective-permute-done((bf16[128,1024]{1,0:T(8,128)(2,1)S(1)}, bf16[128,1024]{1,0:T(8,128)(2,1)S(1)}, u32[]{:S(2)}, u32[]{:S(2)}) %collective-permute-start.3) | collective-permute-done | bytes 262176 | tf_op jit(solution)/shard_map/ppermute | solution.py:26
  28.7 3.2 %shard_map.118.refs_10_ = f32[4,128,256]{2,1,0:T(8,128)S(1)} custom-call(bf16[128,1024]{1,0:T(8,128)(2,1)S(1)} %slice.15.refs_0_, bf16[128,1024]{1,0:T(8,128)(2,1)S(1)} %collective-permute-done.9.refs_1_, bf16[128,1024]{1,0:T(8,128)(2,1)S(1)} %collective-permute-done.10.refs_2_, bf16[128,1024]{1,0:T(8,128)(2,1)S(1)} %collective-permute-done.11.refs_3_, ...), custom_call_target="tpu_custom_call" | custom-call | flops 1610612736 | tf_op jit(solution)/shard_map/pallas_call | solution.py:365
  31.9 2.5 %shard_map.119.refs_10_ = f32[4,128,256]{2,1,0:T(8,128)S(1)} custom-call(bf16[128,1024]{1,0:T(8,128)(2,1)S(1)} %collective-permute-done.6.refs_0_, bf16[128,1024]{1,0:T(8,128)(2,1)S(1)} %collective-permute-done.7.refs_1_, bf16[4096,512]{1,0:T(8,128)(2,1)S(1)} %get-tuple-element.31.refs_2_.refs_1_.refs_4_, ...), custom_call_target="tpu_custom_call" | custom-call | flops 1610612736 | tf_op jit(solution)/shard_map/pallas_call | solution.py:365
  34.4 2.5 %shard_map.120.refs_9_ = f32[4,128,256]{2,1,0:T(8,128)S(1)} custom-call(bf16[128,1024]{1,0:T(8,128)(2,1)S(1)} %collective-permute-done.3.refs_0_, bf16[128,1024]{1,0:T(8,128)(2,1)S(1)} %collective-permute-done.4.refs_1_, bf16[4096,512]{1,0:T(8,128)(2,1)S(1)} %get-tuple-element.31.refs_2_.refs_1_.refs_4_, ...), custom_call_target="tpu_custom_call" | custom-call | flops 1610612736 | tf_op jit(solution)/shard_map/pallas_call | solution.py:365
  36.9 2.3 %shard_map.121 = (bf16[144,256]{1,0:T(8,128)(2,1)S(1)}, bf16[144,256]{1,0:T(8,128)(2,1)S(1)}, bf16[144,256]{1,0:T(8,128)(2,1)S(1)}, bf16[144,256]{1,0:T(8,128)(2,1)S(1)}) custom-call(bf16[128,1024]{1,0:T(8,128)(2,1)S(1)} %collective-permute-done.1.refs_0_, bf16[4096,512]{1,0:T(8,128)(2,1)S(1)} %get-tuple-element.31.refs_2_.refs_1_.refs_4_, ...), custom_call_target="tpu_custom_call" | custom-call | flops 1610612736 | tf_op jit(solution)/shard_map/pallas_call | solution.py:365
  39.2 1.8 %collective-permute-start.12 = (bf16[144,256]{1,0:T(8,128)(2,1)S(1)}, bf16[144,256]{1,0:T(8,128)(2,1)S(1)}, u32[]{:S(2)}, u32[]{:S(2)}) collective-permute-start(bf16[144,256]{1,0:T(8,128)(2,1)S(1)} %get-tuple-element.50), channel_id=1, source_target_pairs={{0,4},{4,0},{8,12},{12,8},{16,20},{20,16},{24,28},{28,24},{1,5},{5... | collective-permute-start | bytes 221192 | tf_op jit(solution)/shard_map/ppermute | solution.py:26
  41.0 1.6 %collective-permute-start.13 = (bf16[144,256]{1,0:T(8,128)(2,1)S(1)}, bf16[144,256]{1,0:T(8,128)(2,1)S(1)}, u32[]{:S(2)}, u32[]{:S(2)}) collective-permute-start(bf16[144,256]{1,0:T(8,128)(2,1)S(1)} %get-tuple-element.51), channel_id=1, source_target_pairs={{0,8},{4,12},{8,0},{12,4},{16,24},{20,28},{24,16},{28,20},{1,9},{5... | collective-permute-start | bytes 221192 | tf_op jit(solution)/shard_map/ppermute | solution.py:26
  42.8 1.2 %collective-permute-done.12.refs_1_ = bf16[144,256]{1,0:T(8,128)(2,1)S(1)} collective-permute-done((bf16[144,256]{1,0:T(8,128)(2,1)S(1)}, bf16[144,256]{1,0:T(8,128)(2,1)S(1)}, u32[]{:S(2)}, u32[]{:S(2)}) %collective-permute-start.12) | collective-permute-done | bytes 73760 | tf_op jit(solution)/shard_map/ppermute | solution.py:26
  44.0 1.7 %collective-permute-done.13.refs_2_ = bf16[144,256]{1,0:T(8,128)(2,1)S(1)} collective-permute-done((bf16[144,256]{1,0:T(8,128)(2,1)S(1)}, bf16[144,256]{1,0:T(8,128)(2,1)S(1)}, u32[]{:S(2)}, u32[]{:S(2)}) %collective-permute-start.13) | collective-permute-done | bytes 73760 | tf_op jit(solution)/shard_map/ppermute | solution.py:26
  45.7 2.1 %collective-permute-done.14.refs_3_ = bf16[144,256]{1,0:T(8,128)(2,1)S(1)} collective-permute-done((bf16[144,256]{1,0:T(8,128)(2,1)S(1)}, bf16[144,256]{1,0:T(8,128)(2,1)S(1)}, u32[]{:S(2)}, u32[]{:S(2)}) %collective-permute-start.14) | collective-permute-done | bytes 73760 | tf_op jit(solution)/shard_map/ppermute | solution.py:26
  48.4 2.6 %collective-permute-start.15 = (bf16[144,128]{1,0:T(8,128)(2,1)S(1)}, bf16[144,128]{1,0:T(8,128)(2,1)S(1)}, u32[]{:S(2)}, u32[]{:S(2)}) collective-permute-start(bf16[144,128]{1,0:T(8,128)(2,1)S(1)} %get-tuple-element.55), channel_id=1, source_target_pairs={{0,16},{4,20},{8,24},{12,28},{16,0},{20,4},{24,8},{28,12},{1,17},{... | collective-permute-start | bytes 110600 | tf_op jit(solution)/shard_map/ppermute | solution.py:26
  51.1 2.7 %collective-permute-done.15.refs_0_ = bf16[144,128]{1,0:T(8,128)(2,1)S(1)} collective-permute-done((bf16[144,128]{1,0:T(8,128)(2,1)S(1)}, bf16[144,128]{1,0:T(8,128)(2,1)S(1)}, u32[]{:S(2)}, u32[]{:S(2)}) %collective-permute-start.15) | collective-permute-done | bytes 36896 | tf_op jit(solution)/shard_map/ppermute | solution.py:26
  54.4 1.6 %collective-permute-start.17 = (bf16[32,128]{1,0:T(8,128)(2,1)S(1)}, bf16[32,128]{1,0:T(8,128)(2,1)S(1)}, u32[]{:S(2)}, u32[]{:S(2)}) collective-permute-start(bf16[32,128]{1,0:T(8,128)(2,1)S(1)} %get-tuple-element.58), channel_id=1, source_target_pairs={{0,8},{4,12},{8,0},{12,4},{16,24},{20,28},{24,16},{28,20},{1,9},{5... | collective-permute-start | bytes 24584 | tf_op jit(solution)/shard_map/ppermute | solution.py:26
  56.0 1.7 %collective-permute-start.18 = (bf16[32,128]{1,0:T(8,128)(2,1)S(1)}, bf16[32,128]{1,0:T(8,128)(2,1)S(1)}, u32[]{:S(2)}, u32[]{:S(2)}) collective-permute-start(bf16[32,128]{1,0:T(8,128)(2,1)S(1)} %get-tuple-element.59), channel_id=1, source_target_pairs={{0,12},{4,8},{8,4},{12,0},{16,28},{20,24},{24,20},{28,16},{1,13},{... | collective-permute-start | bytes 24584 | tf_op jit(solution)/shard_map/ppermute | solution.py:26
  58.1 2.5 %collective-permute-done.18.refs_3_ = bf16[32,128]{1,0:T(8,128)(2,1)S(1)} collective-permute-done((bf16[32,128]{1,0:T(8,128)(2,1)S(1)}, bf16[32,128]{1,0:T(8,128)(2,1)S(1)}, u32[]{:S(2)}, u32[]{:S(2)}) %collective-permute-start.18) | collective-permute-done | bytes 8224 | tf_op jit(solution)/shard_map/ppermute | solution.py:26
  (30 shorter events, 6.6 us)
Async XLA Ops:
  1.6 10.2 %collective-permute-start.9 = (bf16[128,1024]{1,0:T(8,128)(2,1)S(1)}, bf16[128,1024]{1,0:T(8,128)(2,1)S(1)}, u32[]{:S(2)}, u32[]{:S(2)}) collective-permute-start(bf16[128,1024]{1,0:T(8,128)(2,1)S(1)} %slice.15.refs_0_), channel_id=1, source_target_pairs={{0,2},{1,3},{2,0},{3,1},{4,6},{5,7},{6,4},{7,5},{8,10},{9,11},{10,... | collective-permute-start | bytes 786440 | tf_op jit(solution)/shard_map/ppermute | solution.py:26
  5.8 6.0 %collective-permute-start.8 = (bf16[128,1024]{1,0:T(8,128)(2,1)S(1)}, bf16[128,1024]{1,0:T(8,128)(2,1)S(1)}, u32[]{:S(2)}, u32[]{:S(2)}) collective-permute-start(bf16[128,1024]{1,0:T(8,128)(2,1)S(1)} %get-tuple-element.60.refs_0_), channel_id=1, source_target_pairs={{0,1},{1,0},{2,3},{3,2},{4,5},{5,4},{6,7},{7,6},{8,9},{9,8},{10,11... | collective-permute-start | bytes 786440 | tf_op jit(solution)/shard_map/ppermute | solution.py:26
  5.9 7.9 %collective-permute-start.2 = (bf16[128,1024]{1,0:T(8,128)(2,1)S(1)}, bf16[128,1024]{1,0:T(8,128)(2,1)S(1)}, u32[]{:S(2)}, u32[]{:S(2)}) collective-permute-start(bf16[128,1024]{1,0:T(8,128)(2,1)S(1)} %get-tuple-element.62.refs_0_), channel_id=1, source_target_pairs={{0,1},{1,0},{2,3},{3,2},{4,5},{5,4},{6,7},{7,6},{8,9},{9,8},{10,11... | collective-permute-start | bytes 786440 | tf_op jit(solution)/shard_map/ppermute | solution.py:26
  6.4 11.0 %collective-permute-start = (bf16[128,1024]{1,0:T(8,128)(2,1)S(1)}, bf16[128,1024]{1,0:T(8,128)(2,1)S(1)}, u32[]{:S(2)}, u32[]{:S(2)}) collective-permute-start(bf16[128,1024]{1,0:T(8,128)(2,1)S(1)} %get-tuple-element.62.refs_0_), channel_id=1, source_target_pairs={{0,2},{1,3},{2,0},{3,1},{4,6},{5,7},{6,4},{7,5},{8,10},{9,11},{10,... | collective-permute-start | bytes 786440 | tf_op jit(solution)/shard_map/ppermute | solution.py:26
  6.4 16.6 %collective-permute-start.6 = (bf16[128,1024]{1,0:T(8,128)(2,1)S(1)}, bf16[128,1024]{1,0:T(8,128)(2,1)S(1)}, u32[]{:S(2)}, u32[]{:S(2)}) collective-permute-start(bf16[128,1024]{1,0:T(8,128)(2,1)S(1)} %get-tuple-element.60.refs_0_), channel_id=1, source_target_pairs={{0,2},{1,3},{2,0},{3,1},{4,6},{5,7},{6,4},{7,5},{8,10},{9,11},{10,... | collective-permute-start | bytes 786440 | tf_op jit(solution)/shard_map/ppermute | solution.py:26
  11.8 12.3 %collective-permute-start.5 = (bf16[128,1024]{1,0:T(8,128)(2,1)S(1)}, bf16[128,1024]{1,0:T(8,128)(2,1)S(1)}, u32[]{:S(2)}, u32[]{:S(2)}) collective-permute-start(bf16[128,1024]{1,0:T(8,128)(2,1)S(1)} %get-tuple-element.61.refs_0_), channel_id=1, source_target_pairs={{0,1},{1,0},{2,3},{3,2},{4,5},{5,4},{6,7},{7,6},{8,9},{9,8},{10,11... | collective-permute-start | bytes 786440 | tf_op jit(solution)/shard_map/ppermute | solution.py:26
  11.8 16.0 %collective-permute-start.3 = (bf16[128,1024]{1,0:T(8,128)(2,1)S(1)}, bf16[128,1024]{1,0:T(8,128)(2,1)S(1)}, u32[]{:S(2)}, u32[]{:S(2)}) collective-permute-start(bf16[128,1024]{1,0:T(8,128)(2,1)S(1)} %get-tuple-element.61.refs_0_), channel_id=1, source_target_pairs={{0,2},{1,3},{2,0},{3,1},{4,6},{5,7},{6,4},{7,5},{8,10},{9,11},{10,... | collective-permute-start | bytes 786440 | tf_op jit(solution)/shard_map/ppermute | solution.py:26
  13.8 14.8 %collective-permute-start.10 = (bf16[128,1024]{1,0:T(8,128)(2,1)S(1)}, bf16[128,1024]{1,0:T(8,128)(2,1)S(1)}, u32[]{:S(2)}, u32[]{:S(2)}) collective-permute-start(bf16[128,1024]{1,0:T(8,128)(2,1)S(1)} %slice.15.refs_0_), channel_id=1, source_target_pairs={{0,1},{1,0},{2,3},{3,2},{4,5},{5,4},{6,7},{7,6},{8,9},{9,8},{10,11... | collective-permute-start | bytes 786440 | tf_op jit(solution)/shard_map/ppermute | solution.py:26
  17.4 11.3 %collective-permute-start.11 = (bf16[128,1024]{1,0:T(8,128)(2,1)S(1)}, bf16[128,1024]{1,0:T(8,128)(2,1)S(1)}, u32[]{:S(2)}, u32[]{:S(2)}) collective-permute-start(bf16[128,1024]{1,0:T(8,128)(2,1)S(1)} %collective-permute-done.9.refs_1_), channel_id=1, source_target_pairs={{0,1},{1,0},{2,3},{3,2},{4,5},{5,4},{6,7},{7,6},{8,9},{9,8},{10,11... | collective-permute-start | bytes 786440 | tf_op jit(solution)/shard_map/ppermute | solution.py:26
  23.1 8.8 %collective-permute-start.7 = (bf16[128,1024]{1,0:T(8,128)(2,1)S(1)}, bf16[128,1024]{1,0:T(8,128)(2,1)S(1)}, u32[]{:S(2)}, u32[]{:S(2)}) collective-permute-start(bf16[128,1024]{1,0:T(8,128)(2,1)S(1)} %collective-permute-done.6.refs_0_), channel_id=1, source_target_pairs={{0,1},{1,0},{2,3},{3,2},{4,5},{5,4},{6,7},{7,6},{8,9},{9,8},{10,11... | collective-permute-start | bytes 786440 | tf_op jit(solution)/shard_map/ppermute | solution.py:26
  24.1 12.8 %collective-permute-start.1 = (bf16[128,1024]{1,0:T(8,128)(2,1)S(1)}, bf16[128,1024]{1,0:T(8,128)(2,1)S(1)}, u32[]{:S(2)}, u32[]{:S(2)}) collective-permute-start(bf16[128,1024]{1,0:T(8,128)(2,1)S(1)} %collective-permute-done.refs_0_), channel_id=1, source_target_pairs={{0,1},{1,0},{2,3},{3,2},{4,5},{5,4},{6,7},{7,6},{8,9},{9,8},{10,11... | collective-permute-start | bytes 786440 | tf_op jit(solution)/shard_map/ppermute | solution.py:26
  27.8 6.6 %collective-permute-start.4 = (bf16[128,1024]{1,0:T(8,128)(2,1)S(1)}, bf16[128,1024]{1,0:T(8,128)(2,1)S(1)}, u32[]{:S(2)}, u32[]{:S(2)}) collective-permute-start(bf16[128,1024]{1,0:T(8,128)(2,1)S(1)} %collective-permute-done.3.refs_0_), channel_id=1, source_target_pairs={{0,1},{1,0},{2,3},{3,2},{4,5},{5,4},{6,7},{7,6},{8,9},{9,8},{10,11... | collective-permute-start | bytes 786440 | tf_op jit(solution)/shard_map/ppermute | solution.py:26
  36.9 23.6 %copy-start = (bf16[128]{0:T(256)(128)(2,1)S(1)}, bf16[128]{0:T(256)(128)(2,1)}, u32[]{:S(2)}) copy-start(bf16[128]{0:T(256)(128)(2,1)} %param.19) | copy-start | bytes 772
  39.2 4.7 %collective-permute-start.12 = (bf16[144,256]{1,0:T(8,128)(2,1)S(1)}, bf16[144,256]{1,0:T(8,128)(2,1)S(1)}, u32[]{:S(2)}, u32[]{:S(2)}) collective-permute-start(bf16[144,256]{1,0:T(8,128)(2,1)S(1)} %get-tuple-element.50), channel_id=1, source_target_pairs={{0,4},{4,0},{8,12},{12,8},{16,20},{20,16},{24,28},{28,24},{1,5},{5... | collective-permute-start | bytes 221192 | tf_op jit(solution)/shard_map/ppermute | solution.py:26
  41.0 4.7 %collective-permute-start.13 = (bf16[144,256]{1,0:T(8,128)(2,1)S(1)}, bf16[144,256]{1,0:T(8,128)(2,1)S(1)}, u32[]{:S(2)}, u32[]{:S(2)}) collective-permute-start(bf16[144,256]{1,0:T(8,128)(2,1)S(1)} %get-tuple-element.51), channel_id=1, source_target_pairs={{0,8},{4,12},{8,0},{12,4},{16,24},{20,28},{24,16},{28,20},{1,9},{5... | collective-permute-start | bytes 221192 | tf_op jit(solution)/shard_map/ppermute | solution.py:26
  42.6 5.3 %collective-permute-start.14 = (bf16[144,256]{1,0:T(8,128)(2,1)S(1)}, bf16[144,256]{1,0:T(8,128)(2,1)S(1)}, u32[]{:S(2)}, u32[]{:S(2)}) collective-permute-start(bf16[144,256]{1,0:T(8,128)(2,1)S(1)} %get-tuple-element.52), channel_id=1, source_target_pairs={{0,12},{4,8},{8,4},{12,0},{16,28},{20,24},{24,20},{28,16},{1,13},{... | collective-permute-start | bytes 221192 | tf_op jit(solution)/shard_map/ppermute | solution.py:26
  48.4 5.3 %collective-permute-start.15 = (bf16[144,128]{1,0:T(8,128)(2,1)S(1)}, bf16[144,128]{1,0:T(8,128)(2,1)S(1)}, u32[]{:S(2)}, u32[]{:S(2)}) collective-permute-start(bf16[144,128]{1,0:T(8,128)(2,1)S(1)} %get-tuple-element.55), channel_id=1, source_target_pairs={{0,16},{4,20},{8,24},{12,28},{16,0},{20,4},{24,8},{28,12},{1,17},{... | collective-permute-start | bytes 110600 | tf_op jit(solution)/shard_map/ppermute | solution.py:26
  54.2 3.7 %collective-permute-start.16 = (bf16[32,128]{1,0:T(8,128)(2,1)S(1)}, bf16[32,128]{1,0:T(8,128)(2,1)S(1)}, u32[]{:S(2)}, u32[]{:S(2)}) collective-permute-start(bf16[32,128]{1,0:T(8,128)(2,1)S(1)} %get-tuple-element.57), channel_id=1, source_target_pairs={{0,4},{4,0},{8,12},{12,8},{16,20},{20,16},{24,28},{28,24},{1,5},{5... | collective-permute-start | bytes 24584 | tf_op jit(solution)/shard_map/ppermute | solution.py:26
  54.4 3.7 %collective-permute-start.17 = (bf16[32,128]{1,0:T(8,128)(2,1)S(1)}, bf16[32,128]{1,0:T(8,128)(2,1)S(1)}, u32[]{:S(2)}, u32[]{:S(2)}) collective-permute-start(bf16[32,128]{1,0:T(8,128)(2,1)S(1)} %get-tuple-element.58), channel_id=1, source_target_pairs={{0,8},{4,12},{8,0},{12,4},{16,24},{20,28},{24,16},{28,20},{1,9},{5... | collective-permute-start | bytes 24584 | tf_op jit(solution)/shard_map/ppermute | solution.py:26
  56.0 4.5 %collective-permute-start.18 = (bf16[32,128]{1,0:T(8,128)(2,1)S(1)}, bf16[32,128]{1,0:T(8,128)(2,1)S(1)}, u32[]{:S(2)}, u32[]{:S(2)}) collective-permute-start(bf16[32,128]{1,0:T(8,128)(2,1)S(1)} %get-tuple-element.59), channel_id=1, source_target_pairs={{0,12},{4,8},{8,4},{12,0},{16,28},{20,24},{24,20},{28,16},{1,13},{... | collective-permute-start | bytes 24584 | tf_op jit(solution)/shard_map/ppermute | solution.py:26

commit v4 on v3

--- a/solution.py
+++ b/solution.py
@@ -1,4 +1,5 @@
 import functools
+import math
 
 import jax
 import jax.numpy as jnp
@@ -85,10 +86,12 @@
 def project(masks, piece_refs, wk_ref, wv_ref, wg_ref, sums):
     rank = lax.axis_index("tp")
     gates, keys, values = sums
+    share = wk_ref.shape[0] // lax.axis_size("tp")
     placed = []
-    for m, ref in zip(masks, piece_refs):
+    for (m, shift), ref in zip(masks, piece_refs):
         width = ref.shape[1]
-        placed.append((pl.ds(pl.multiple_of((rank ^ m) * width, width), width), ref))
+        start = pl.multiple_of((rank ^ m) * share + shift, math.gcd(share, width))
+        placed.append((pl.ds(start, width), ref))
     for rows, ref in placed:
         g = dot_nt(wg_ref[:, rows], ref[...])
         gates = g if gates is None else gates + g
@@ -224,10 +227,7 @@
     for h in range(heads):
         new = keep[h : h + 1, :] * states[h] + dot(turned[h], fresh[h])
         if last:
-            rest[h][0:DK, :] = new.astype(bf16)
-            asked = jnp.broadcast_to(query_ref[h : h + 1, :], (2 * SUB, DK))
-            asked = jnp.concatenate([asked, jnp.zeros((2 * SUB, DV), f32)], axis=1)
-            rest[h][DK:, :] = asked.astype(bf16)
+            rest[h][...] = passed_on(new, jnp.broadcast_to(query_ref[h : h + 1, :], (SUB, DK)))
         else:
             rest[-1][h] = new
 
@@ -269,22 +269,23 @@
 
 
 def passed_on(total, query):
-    asked = jnp.concatenate([query, query], axis=0)
-    asked = jnp.concatenate([asked, jnp.zeros((2 * SUB, DV), f32)], axis=1)
-    return jnp.concatenate([total, asked], axis=0).astype(bf16)
+    return jnp.concatenate([total[:, :DV], total[:, DV:], query, query], axis=0).astype(bf16)
+
+
+def received(ref):
+    total = jnp.concatenate([ref[:DK, :], ref[DK : 2 * DK, :]], axis=1)
+    return total.astype(f32), ref[2 * DK :, :].astype(f32)[:SUB]
 
 
 def compose_kernel(heads, final, *refs):
     own_ref, got = refs[0], refs[1:heads]
     out, scratch = refs[heads:-1], refs[-1]
     lead = lax.axis_index("sp") % heads
-    scratch[lead] = own_ref[:DK, :].astype(f32)
-    query = own_ref[DK:, :DK].astype(f32)
+    scratch[lead], query = received(own_ref)
     for k in range(1, heads):
-        scratch[lead ^ k] = got[k - 1][:DK, :].astype(f32)
-        query = query + got[k - 1][DK:, :DK].astype(f32)
+        scratch[lead ^ k], asked = received(got[k - 1])
+        query = query + asked
     total = compose([scratch[i] for i in range(heads)], dot)
-    query = query[:SUB]
     if final:
         finish(total, query, out)
     else:
@@ -294,8 +295,8 @@
 
 def merge_kernel(mask, final, own_ref, query_ref, got_ref, *out):
     high = late_side(mask)
-    own, got = own_ref[...], got_ref[:DK, :].astype(f32)
-    query = query_ref[...] + got_ref[DK:, :DK].astype(f32)[:SUB]
+    own, (got, asked) = own_ref[...], received(got_ref)
+    query = query_ref[...] + asked
     early, late = jnp.where(high, got, own), jnp.where(high, own, got)
     total = compose([early, late], dot3)
     if final:
@@ -401,11 +402,18 @@
     owns += [later[c * chunk : (c + 1) * chunk] for c in range(1, chunks)]
     gathered = []
     for c in range(chunks):
-        found = [(0, owns[c])]
-        for hop in range(1, ranks // 2):
-            found.append((2 * hop, swap(owns[c], "tp", 2 * hop)))
-        found.append((1, swap(owns[c], "tp", 1)))
-        found += [(m ^ 1, swap(x, "tp", 1)) for m, x in found[1:-1]]
+        found = [(0, 0, owns[c], False)]
+        found.append((1, 0, swap(owns[c], "tp", 1), False))
+        halves = 2 if c == chunks - 1 and width % 256 == 0 else 1
+        part_width = width // halves
+        for half in range(halves):
+            shift = half * part_width
+            block = owns[c][:, shift : shift + part_width]
+            late = half == halves - 1
+            for hop in range(1, ranks // 2):
+                near = swap(block, "tp", 2 * hop)
+                far = swap(near, "tp", 1)
+                found += [(2 * hop, shift, near, late), (2 * hop + 1, shift, far, late)]
         gathered.append(found)
 
     plain = [
@@ -444,36 +452,37 @@
     sums_shape = [shape((2 * SUB, chunk)), shape((chunk, heads * DK)), shape((chunk, heads * DV))]
 
     def part(found, sums):
-        return call(
-            functools.partial(part_kernel, tuple(m for m, _ in found), len(sums) > 0),
-            [x for _, x in found] + weights + sums,
+        out = call(
+            functools.partial(part_kernel, tuple(f[:2] for f in found), len(sums) > 0),
+            [f[2] for f in found] + weights + sums,
             sums_shape,
             mib=16,
-            flops=2 * chunk * width * len(found) * (2 * heads * DK + DK),
+            flops=2 * chunk * sum(f[2].shape[1] for f in found) * (2 * heads * DK + DK),
         )
+        return list(out)
 
     for c in range(chunks):
         found = gathered[c]
         last = c == chunks - 1
         sums = []
         if c > 0:
-            here = [f for f in found if f[0] < 2]
+            sums = part([f for f in found if f[0] < 2], sums)
             found = [f for f in found if f[0] >= 2]
-            sums = list(part(here, sums))
         if last and len(found) > 1:
-            near = [f for f in found if f[0] % 2 == 0]
-            found = [f for f in found if f[0] % 2 == 1]
-            sums = list(part(near, sums))
-        arrays = [x for _, x in found] + weights + [small, forget] + sums
+            relayed = [f for f in found if f[3] and f[0] % 2 == 1]
+            sums = part([f for f in found if not (f[3] and f[0] % 2 == 1)], sums)
+            found = relayed
+        masks = tuple(f[:2] for f in found)
+        arrays = [f[2] for f in found] + weights + [small, forget] + sums
         if c > 0:
             arrays.append(state)
         outs = [shape((heads, DK, DV + DK))]
         if last:
             arrays.append(query)
-            outs = [shape((DK + 2 * SUB, DV + DK), bf16)] * heads
+            outs = [shape((DK + DV + 2 * SUB, DK), bf16)] * heads
         result = call(
             functools.partial(
-                chunk_kernel, heads, c, last, tuple(m for m, _ in found), len(sums) > 0
+                chunk_kernel, heads, c, last, masks, len(sums) > 0
             ),
             arrays,
             outs,
@@ -487,7 +496,7 @@
     for k in reversed(range(1, heads)):
         got[k] = swap(maps[k], "sp", k)
     done = [shape((DK, DV + DK)), shape((SUB, DK))]
-    open_ended = done + [shape((DK + 2 * SUB, DV + DK), bf16)]
+    open_ended = done + [shape((DK + DV + 2 * SUB, DK), bf16)]
     if groups > 1:
         done.append(shape((DK + 2 * SUB, DV), bf16))
     result = call(

time: 61.4 us -> 62.7 us (1.021)
  local copies, waits for them, and re-layouts: 2.13 us -> 3.12 us
    slice x0 -> x1, local copies, waits for them, and re-layouts: none -> 0.98 us  [per_device(): block = owns[c][:, shift:shift + part_width]]
    ppermute x19 -> x21, starting transfers between devices: 18.2 us -> 18.6 us  [swap(): return lax.ppermute(x, axis, flip(axis, mask))]
    ppermute x19 -> x21, waiting for transfers between devices: 21.1 us -> 21 us  [swap(): return lax.ppermute(x, axis, flip(axis, mask))]
  transfers between devices with their start and end apart: 19 -> 21, of which waited for: 11 -> 11; matrix products, arithmetic and copies ran while one was open for 2% -> 3% of each run, Pallas kernels for 25% -> 24%
where the time goes in v4:
time: 62.7 us; the launch traced here: 62.6 us
  waiting for transfers between devices  21 us (33%)
  Pallas kernels  19.1 us (30%)
  starting transfers between devices  18.6 us (30%)
  local copies, waits for them, and re-layouts  3.12 us (5%)
  between operations  0.79 us (1%)
    ppermute x21, waiting for transfers between devices, swap(): return lax.ppermute(x, axis, flip(axis, mask))  21 us
    ppermute x21, starting transfers between devices, swap(): return lax.ppermute(x, axis, flip(axis, mask))  18.6 us
    pallas_call x11, Pallas kernels, call(): pl.pallas_call(body, out_shape=outs, in_specs=[vmem] * len(arrays), out_s...  15.3 us
    pallas_call x1, Pallas kernels, per_device(): pl.pallas_call(functools.partial(prepare_kernel, heads), out_shape=[shape...  3.84 us
  transfers between devices with their start and end apart: 21, of which 11 were waited for; matrix products, arithmetic and copies ran while one was open for 3% of the time, Pallas kernels for 24%

profile of v4, /device:TPU:0, one launch (start us, length us, event | category | flops | bytes accessed | tf_op | source)
XLA Modules:
  0.0 62.6 jit_solution(7988427277724815750)
XLA Ops:
  1.6 3.1 %collective-permute-start.12 = (bf16[128,1024]{1,0:T(8,128)(2,1)S(1)}, bf16[128,1024]{1,0:T(8,128)(2,1)S(1)}, u32[]{:S(2)}, u32[]{:S(2)}) collective-permute-start(bf16[128,1024]{1,0:T(8,128)(2,1)S(1)} %slice.25.refs_0_), channel_id=1, source_target_pairs={{0,2},{1,3},{2,0},{3,1},{4,6},{5,7},{6,4},{7,5},{8,10},{9,11},{10,... | collective-permute-start | bytes 786440 | tf_op jit(solution)/shard_map/ppermute | solution.py:27
  4.7 1.2 %fusion = (bf16[128,1024]{1,0:T(8,128)(2,1)S(1)}, bf16[128,1024]{1,0:T(8,128)(2,1)S(1)}, bf16[128,1024]{1,0:T(8,128)(2,1)S(1)}) fusion(bf16[512,1024]{1,0:T(8,128)(2,1)} %param.10), kind=kLoop, calls=%fused_computation | loop fusion | bytes 1572864 | tf_op jit(solution)/shard_map/slice | solution.py:402
  6.4 1.0 %fusion.1 = (bf16[128,512]{1,0:T(8,128)(2,1)S(1)}, bf16[128,512]{1,0:T(8,128)(2,1)S(1)}) fusion(bf16[512,1024]{1,0:T(8,128)(2,1)} %param.10), kind=kLoop, calls=%fused_computation.1 | loop fusion | bytes 524288 | tf_op jit(solution)/shard_map/slice | solution.py:411
  7.5 2.0 %collective-permute-start = (bf16[128,512]{1,0:T(8,128)(2,1)S(1)}, bf16[128,512]{1,0:T(8,128)(2,1)S(1)}, u32[]{:S(2)}, u32[]{:S(2)}) collective-permute-start(bf16[128,512]{1,0:T(8,128)(2,1)S(1)} %get-tuple-element.64), channel_id=1, source_target_pairs={{0,2},{1,3},{2,0},{3,1},{4,6},{5,7},{6,4},{7,5},{8,10},{9,11},{10,... | collective-permute-start | bytes 393224 | tf_op jit(solution)/shard_map/ppermute | solution.py:27
  9.5 5.1 %collective-permute-done.2.refs_0_ = bf16[128,512]{1,0:T(8,128)(2,1)S(1)} collective-permute-done((bf16[128,512]{1,0:T(8,128)(2,1)S(1)}, bf16[128,512]{1,0:T(8,128)(2,1)S(1)}, u32[]{:S(2)}, u32[]{:S(2)}) %collective-permute-start.2) | collective-permute-done | bytes 131104 | tf_op jit(solution)/shard_map/ppermute | solution.py:27
  14.6 2.0 %collective-permute-done.refs_2_ = bf16[128,512]{1,0:T(8,128)(2,1)S(1)} collective-permute-done((bf16[128,512]{1,0:T(8,128)(2,1)S(1)}, bf16[128,512]{1,0:T(8,128)(2,1)S(1)}, u32[]{:S(2)}, u32[]{:S(2)}) %collective-permute-start) | collective-permute-done | bytes 131104 | tf_op jit(solution)/shard_map/ppermute | solution.py:27
  16.6 1.7 %collective-permute-start.8 = (bf16[128,1024]{1,0:T(8,128)(2,1)S(1)}, bf16[128,1024]{1,0:T(8,128)(2,1)S(1)}, u32[]{:S(2)}, u32[]{:S(2)}) collective-permute-start(bf16[128,1024]{1,0:T(8,128)(2,1)S(1)} %get-tuple-element.60.refs_0_), channel_id=1, source_target_pairs={{0,2},{1,3},{2,0},{3,1},{4,6},{5,7},{6,4},{7,5},{8,10},{9,11},{10,... | collective-permute-start | bytes 786440 | tf_op jit(solution)/shard_map/ppermute | solution.py:27
  19.2 3.8 %shard_map.113 = (bf16[4096,512]{1,0:T(8,128)(2,1)S(1)}, bf16[4096,512]{1,0:T(8,128)(2,1)S(1)}, bf16[16,4096]{1,0:T(8,128)(2,1)S(1)}, f32[8,128]{1,0:T(8,128)S(1...) custom-call(bf16[4096,512]{1,0:T(8,128)(2,1)} %refs_0_.1, bf16[4096,512]{1,0:T(8,128)(2,1)} %refs_1_.1, ...), custom_call_target="tpu_custom_call" | custom-call | tf_op jit(solution)/shard_map/pallas_call | solution.py:432
  24.6 1.1 %collective-permute-done.8.refs_0_ = bf16[128,1024]{1,0:T(8,128)(2,1)S(1)} collective-permute-done((bf16[128,1024]{1,0:T(8,128)(2,1)S(1)}, bf16[128,1024]{1,0:T(8,128)(2,1)S(1)}, u32[]{:S(2)}, u32[]{:S(2)}) %collective-permute-start.8) | collective-permute-done | bytes 262176 | tf_op jit(solution)/shard_map/ppermute | solution.py:27
  27.2 2.5 %collective-permute-done.5.refs_0_ = bf16[128,1024]{1,0:T(8,128)(2,1)S(1)} collective-permute-done((bf16[128,1024]{1,0:T(8,128)(2,1)S(1)}, bf16[128,1024]{1,0:T(8,128)(2,1)S(1)}, u32[]{:S(2)}, u32[]{:S(2)}) %collective-permute-start.5) | collective-permute-done | bytes 262176 | tf_op jit(solution)/shard_map/ppermute | solution.py:27
  30.6 3.2 %shard_map.118.refs_10_ = f32[4,128,256]{2,1,0:T(8,128)S(1)} custom-call(bf16[128,1024]{1,0:T(8,128)(2,1)S(1)} %slice.25.refs_0_, bf16[128,1024]{1,0:T(8,128)(2,1)S(1)} %collective-permute-done.11.refs_1_, bf16[128,1024]{1,0:T(8,128)(2,1)S(1)} %collective-permute-done.12.refs_2_, bf16[128,1024]{1,0:T(8,128)(2,1)S(1)} %collective-permute-done.13.refs_3_, ...), custom_call_target="tpu_custom_call" | custom-call | flops 1610612736 | tf_op jit(solution)/shard_map/pallas_call | solution.py:366
  33.8 2.5 %shard_map.119.refs_10_ = f32[4,128,256]{2,1,0:T(8,128)S(1)} custom-call(bf16[128,1024]{1,0:T(8,128)(2,1)S(1)} %collective-permute-done.8.refs_0_, bf16[128,1024]{1,0:T(8,128)(2,1)S(1)} %collective-permute-done.9.refs_1_, bf16[4096,512]{1,0:T(8,128)(2,1)S(1)} %get-tuple-element.31.refs_2_.refs_3_.refs_4_.refs_1_, ...), custom_call_target="tpu_custom_call" | custom-call | flops 1610612736 | tf_op jit(solution)/shard_map/pallas_call | solution.py:366
  36.3 2.5 %shard_map.120.refs_9_ = f32[4,128,256]{2,1,0:T(8,128)S(1)} custom-call(bf16[128,1024]{1,0:T(8,128)(2,1)S(1)} %collective-permute-done.5.refs_0_, bf16[128,1024]{1,0:T(8,128)(2,1)S(1)} %collective-permute-done.6.refs_1_, bf16[4096,512]{1,0:T(8,128)(2,1)S(1)} %get-tuple-element.31.refs_2_.refs_3_.refs_4_.refs_1_, ...), custom_call_target="tpu_custom_call" | custom-call | flops 1610612736 | tf_op jit(solution)/shard_map/pallas_call | solution.py:366
  38.8 2.2 %shard_map.121 = (bf16[272,128]{1,0:T(8,128)(2,1)S(1)}, bf16[272,128]{1,0:T(8,128)(2,1)S(1)}, bf16[272,128]{1,0:T(8,128)(2,1)S(1)}, bf16[272,128]{1,0:T(8,128)(2,1)S(1)}) custom-call(bf16[128,512]{1,0:T(8,128)(2,1)S(1)} %collective-permute-done.1.refs_0_, bf16[4096,512]{1,0:T(8,128)(2,1)S(1)} %get-tuple-element.31.refs_2_.refs_3_.refs_4_.refs_1_, ...), custom_call_target="tpu_custom_call" | custom-call | flops 1610612736 | tf_op jit(solution)/shard_map/pallas_call | solution.py:366
  41.0 1.6 %collective-permute-start.14 = (bf16[272,128]{1,0:T(8,128)(2,1)S(1)}, bf16[272,128]{1,0:T(8,128)(2,1)S(1)}, u32[]{:S(2)}, u32[]{:S(2)}) collective-permute-start(bf16[272,128]{1,0:T(8,128)(2,1)S(1)} %get-tuple-element.50), channel_id=1, source_target_pairs={{0,4},{4,0},{8,12},{12,8},{16,20},{20,16},{24,28},{28,24},{1,5},{5... | collective-permute-start | bytes 208904 | tf_op jit(solution)/shard_map/ppermute | solution.py:27
  42.5 1.6 %collective-permute-start.15 = (bf16[272,128]{1,0:T(8,128)(2,1)S(1)}, bf16[272,128]{1,0:T(8,128)(2,1)S(1)}, u32[]{:S(2)}, u32[]{:S(2)}) collective-permute-start(bf16[272,128]{1,0:T(8,128)(2,1)S(1)} %get-tuple-element.51), channel_id=1, source_target_pairs={{0,8},{4,12},{8,0},{12,4},{16,24},{20,28},{24,16},{28,20},{1,9},{5... | collective-permute-start | bytes 208904 | tf_op jit(solution)/shard_map/ppermute | solution.py:27
  44.5 1.1 %collective-permute-done.14.refs_1_ = bf16[272,128]{1,0:T(8,128)(2,1)S(1)} collective-permute-done((bf16[272,128]{1,0:T(8,128)(2,1)S(1)}, bf16[272,128]{1,0:T(8,128)(2,1)S(1)}, u32[]{:S(2)}, u32[]{:S(2)}) %collective-permute-start.14) | collective-permute-done | bytes 69664 | tf_op jit(solution)/shard_map/ppermute | solution.py:27
  45.7 1.3 %collective-permute-done.15.refs_2_ = bf16[272,128]{1,0:T(8,128)(2,1)S(1)} collective-permute-done((bf16[272,128]{1,0:T(8,128)(2,1)S(1)}, bf16[272,128]{1,0:T(8,128)(2,1)S(1)}, u32[]{:S(2)}, u32[]{:S(2)}) %collective-permute-start.15) | collective-permute-done | bytes 69664 | tf_op jit(solution)/shard_map/ppermute | solution.py:27
  47.0 2.3 %collective-permute-done.16.refs_3_ = bf16[272,128]{1,0:T(8,128)(2,1)S(1)} collective-permute-done((bf16[272,128]{1,0:T(8,128)(2,1)S(1)}, bf16[272,128]{1,0:T(8,128)(2,1)S(1)}, u32[]{:S(2)}, u32[]{:S(2)}) %collective-permute-start.16) | collective-permute-done | bytes 69664 | tf_op jit(solution)/shard_map/ppermute | solution.py:27
  49.9 2.6 %collective-permute-start.17 = (bf16[144,128]{1,0:T(8,128)(2,1)S(1)}, bf16[144,128]{1,0:T(8,128)(2,1)S(1)}, u32[]{:S(2)}, u32[]{:S(2)}) collective-permute-start(bf16[144,128]{1,0:T(8,128)(2,1)S(1)} %get-tuple-element.55), channel_id=1, source_target_pairs={{0,16},{4,20},{8,24},{12,28},{16,0},{20,4},{24,8},{28,12},{1,17},{... | collective-permute-start | bytes 110600 | tf_op jit(solution)/shard_map/ppermute | solution.py:27
  52.5 2.7 %collective-permute-done.17.refs_0_ = bf16[144,128]{1,0:T(8,128)(2,1)S(1)} collective-permute-done((bf16[144,128]{1,0:T(8,128)(2,1)S(1)}, bf16[144,128]{1,0:T(8,128)(2,1)S(1)}, u32[]{:S(2)}, u32[]{:S(2)}) %collective-permute-start.17) | collective-permute-done | bytes 36896 | tf_op jit(solution)/shard_map/ppermute | solution.py:27
  55.8 1.5 %collective-permute-start.19 = (bf16[32,128]{1,0:T(8,128)(2,1)S(1)}, bf16[32,128]{1,0:T(8,128)(2,1)S(1)}, u32[]{:S(2)}, u32[]{:S(2)}) collective-permute-start(bf16[32,128]{1,0:T(8,128)(2,1)S(1)} %get-tuple-element.58), channel_id=1, source_target_pairs={{0,8},{4,12},{8,0},{12,4},{16,24},{20,28},{24,16},{28,20},{1,9},{5... | collective-permute-start | bytes 24584 | tf_op jit(solution)/shard_map/ppermute | solution.py:27
  57.3 1.8 %collective-permute-start.20 = (bf16[32,128]{1,0:T(8,128)(2,1)S(1)}, bf16[32,128]{1,0:T(8,128)(2,1)S(1)}, u32[]{:S(2)}, u32[]{:S(2)}) collective-permute-start(bf16[32,128]{1,0:T(8,128)(2,1)S(1)} %get-tuple-element.59), channel_id=1, source_target_pairs={{0,12},{4,8},{8,4},{12,0},{16,28},{20,24},{24,20},{28,16},{1,13},{... | collective-permute-start | bytes 24584 | tf_op jit(solution)/shard_map/ppermute | solution.py:27
  59.4 2.4 %collective-permute-done.20.refs_3_ = bf16[32,128]{1,0:T(8,128)(2,1)S(1)} collective-permute-done((bf16[32,128]{1,0:T(8,128)(2,1)S(1)}, bf16[32,128]{1,0:T(8,128)(2,1)S(1)}, u32[]{:S(2)}, u32[]{:S(2)}) %collective-permute-start.20) | collective-permute-done | bytes 8224 | tf_op jit(solution)/shard_map/ppermute | solution.py:27
  (35 shorter events, 8.9 us)
Async XLA Ops:
  1.6 16.7 %collective-permute-start.12 = (bf16[128,1024]{1,0:T(8,128)(2,1)S(1)}, bf16[128,1024]{1,0:T(8,128)(2,1)S(1)}, u32[]{:S(2)}, u32[]{:S(2)}) collective-permute-start(bf16[128,1024]{1,0:T(8,128)(2,1)S(1)} %slice.25.refs_0_), channel_id=1, source_target_pairs={{0,2},{1,3},{2,0},{3,1},{4,6},{5,7},{6,4},{7,5},{8,10},{9,11},{10,... | collective-permute-start | bytes 786440 | tf_op jit(solution)/shard_map/ppermute | solution.py:27
  5.8 12.5 %collective-permute-start.10 = (bf16[128,1024]{1,0:T(8,128)(2,1)S(1)}, bf16[128,1024]{1,0:T(8,128)(2,1)S(1)}, u32[]{:S(2)}, u32[]{:S(2)}) collective-permute-start(bf16[128,1024]{1,0:T(8,128)(2,1)S(1)} %get-tuple-element.60.refs_0_), channel_id=1, source_target_pairs={{0,1},{1,0},{2,3},{3,2},{4,5},{5,4},{6,7},{7,6},{8,9},{9,8},{10,11... | collective-permute-start | bytes 786440 | tf_op jit(solution)/shard_map/ppermute | solution.py:27
  5.9 12.8 %collective-permute-start.4 = (bf16[128,1024]{1,0:T(8,128)(2,1)S(1)}, bf16[128,1024]{1,0:T(8,128)(2,1)S(1)}, u32[]{:S(2)}, u32[]{:S(2)}) collective-permute-start(bf16[128,1024]{1,0:T(8,128)(2,1)S(1)} %get-tuple-element.62.refs_0_), channel_id=1, source_target_pairs={{0,1},{1,0},{2,3},{3,2},{4,5},{5,4},{6,7},{7,6},{8,9},{9,8},{10,11... | collective-permute-start | bytes 786440 | tf_op jit(solution)/shard_map/ppermute | solution.py:27
  7.4 7.2 %collective-permute-start.2 = (bf16[128,512]{1,0:T(8,128)(2,1)S(1)}, bf16[128,512]{1,0:T(8,128)(2,1)S(1)}, u32[]{:S(2)}, u32[]{:S(2)}) collective-permute-start(bf16[128,512]{1,0:T(8,128)(2,1)S(1)} %get-tuple-element.63), channel_id=1, source_target_pairs={{0,2},{1,3},{2,0},{3,1},{4,6},{5,7},{6,4},{7,5},{8,10},{9,11},{10,... | collective-permute-start | bytes 393224 | tf_op jit(solution)/shard_map/ppermute | solution.py:27
  7.5 9.1 %collective-permute-start = (bf16[128,512]{1,0:T(8,128)(2,1)S(1)}, bf16[128,512]{1,0:T(8,128)(2,1)S(1)}, u32[]{:S(2)}, u32[]{:S(2)}) collective-permute-start(bf16[128,512]{1,0:T(8,128)(2,1)S(1)} %get-tuple-element.64), channel_id=1, source_target_pairs={{0,2},{1,3},{2,0},{3,1},{4,6},{5,7},{6,4},{7,5},{8,10},{9,11},{10,... | collective-permute-start | bytes 393224 | tf_op jit(solution)/shard_map/ppermute | solution.py:27
  14.6 4.3 %collective-permute-start.3 = (bf16[128,512]{1,0:T(8,128)(2,1)S(1)}, bf16[128,512]{1,0:T(8,128)(2,1)S(1)}, u32[]{:S(2)}, u32[]{:S(2)}) collective-permute-start(bf16[128,512]{1,0:T(8,128)(2,1)S(1)} %collective-permute-done.2.refs_0_), channel_id=1, source_target_pairs={{0,1},{1,0},{2,3},{3,2},{4,5},{5,4},{6,7},{7,6},{8,9},{9,8},{10,11... | collective-permute-start | bytes 393224 | tf_op jit(solution)/shard_map/ppermute | solution.py:27
  16.6 9.2 %collective-permute-start.8 = (bf16[128,1024]{1,0:T(8,128)(2,1)S(1)}, bf16[128,1024]{1,0:T(8,128)(2,1)S(1)}, u32[]{:S(2)}, u32[]{:S(2)}) collective-permute-start(bf16[128,1024]{1,0:T(8,128)(2,1)S(1)} %get-tuple-element.60.refs_0_), channel_id=1, source_target_pairs={{0,2},{1,3},{2,0},{3,1},{4,6},{5,7},{6,4},{7,5},{8,10},{9,11},{10,... | collective-permute-start | bytes 786440 | tf_op jit(solution)/shard_map/ppermute | solution.py:27
  18.3 8.3 %collective-permute-start.7 = (bf16[128,1024]{1,0:T(8,128)(2,1)S(1)}, bf16[128,1024]{1,0:T(8,128)(2,1)S(1)}, u32[]{:S(2)}, u32[]{:S(2)}) collective-permute-start(bf16[128,1024]{1,0:T(8,128)(2,1)S(1)} %get-tuple-element.61.refs_0_), channel_id=1, source_target_pairs={{0,1},{1,0},{2,3},{3,2},{4,5},{5,4},{6,7},{7,6},{8,9},{9,8},{10,11... | collective-permute-start | bytes 786440 | tf_op jit(solution)/shard_map/ppermute | solution.py:27
  18.3 11.3 %collective-permute-start.5 = (bf16[128,1024]{1,0:T(8,128)(2,1)S(1)}, bf16[128,1024]{1,0:T(8,128)(2,1)S(1)}, u32[]{:S(2)}, u32[]{:S(2)}) collective-permute-start(bf16[128,1024]{1,0:T(8,128)(2,1)S(1)} %get-tuple-element.61.refs_0_), channel_id=1, source_target_pairs={{0,2},{1,3},{2,0},{3,1},{4,6},{5,7},{6,4},{7,5},{8,10},{9,11},{10,... | collective-permute-start | bytes 786440 | tf_op jit(solution)/shard_map/ppermute | solution.py:27
  18.7 11.9 %collective-permute-start.11 = (bf16[128,1024]{1,0:T(8,128)(2,1)S(1)}, bf16[128,1024]{1,0:T(8,128)(2,1)S(1)}, u32[]{:S(2)}, u32[]{:S(2)}) collective-permute-start(bf16[128,1024]{1,0:T(8,128)(2,1)S(1)} %slice.25.refs_0_), channel_id=1, source_target_pairs={{0,1},{1,0},{2,3},{3,2},{4,5},{5,4},{6,7},{7,6},{8,9},{9,8},{10,11... | collective-permute-start | bytes 786440 | tf_op jit(solution)/shard_map/ppermute | solution.py:27
  18.9 11.6 %collective-permute-start.13 = (bf16[128,1024]{1,0:T(8,128)(2,1)S(1)}, bf16[128,1024]{1,0:T(8,128)(2,1)S(1)}, u32[]{:S(2)}, u32[]{:S(2)}) collective-permute-start(bf16[128,1024]{1,0:T(8,128)(2,1)S(1)} %collective-permute-done.12.refs_2_), channel_id=1, source_target_pairs={{0,1},{1,0},{2,3},{3,2},{4,5},{5,4},{6,7},{7,6},{8,9},{9,8},{10,11... | collective-permute-start | bytes 786440 | tf_op jit(solution)/shard_map/ppermute | solution.py:27
  25.8 8.0 %collective-permute-start.9 = (bf16[128,1024]{1,0:T(8,128)(2,1)S(1)}, bf16[128,1024]{1,0:T(8,128)(2,1)S(1)}, u32[]{:S(2)}, u32[]{:S(2)}) collective-permute-start(bf16[128,1024]{1,0:T(8,128)(2,1)S(1)} %collective-permute-done.8.refs_0_), channel_id=1, source_target_pairs={{0,1},{1,0},{2,3},{3,2},{4,5},{5,4},{6,7},{7,6},{8,9},{9,8},{10,11... | collective-permute-start | bytes 786440 | tf_op jit(solution)/shard_map/ppermute | solution.py:27
  26.6 12.1 %collective-permute-start.1 = (bf16[128,512]{1,0:T(8,128)(2,1)S(1)}, bf16[128,512]{1,0:T(8,128)(2,1)S(1)}, u32[]{:S(2)}, u32[]{:S(2)}) collective-permute-start(bf16[128,512]{1,0:T(8,128)(2,1)S(1)} %collective-permute-done.refs_2_), channel_id=1, source_target_pairs={{0,1},{1,0},{2,3},{3,2},{4,5},{5,4},{6,7},{7,6},{8,9},{9,8},{10,11... | collective-permute-start | bytes 393224 | tf_op jit(solution)/shard_map/ppermute | solution.py:27
  29.7 6.6 %collective-permute-start.6 = (bf16[128,1024]{1,0:T(8,128)(2,1)S(1)}, bf16[128,1024]{1,0:T(8,128)(2,1)S(1)}, u32[]{:S(2)}, u32[]{:S(2)}) collective-permute-start(bf16[128,1024]{1,0:T(8,128)(2,1)S(1)} %collective-permute-done.5.refs_0_), channel_id=1, source_target_pairs={{0,1},{1,0},{2,3},{3,2},{4,5},{5,4},{6,7},{7,6},{8,9},{9,8},{10,11... | collective-permute-start | bytes 786440 | tf_op jit(solution)/shard_map/ppermute | solution.py:27
  38.8 23.1 %copy-start = (bf16[128]{0:T(256)(128)(2,1)S(1)}, bf16[128]{0:T(256)(128)(2,1)}, u32[]{:S(2)}) copy-start(bf16[128]{0:T(256)(128)(2,1)} %param.19) | copy-start | bytes 772
  41.0 4.7 %collective-permute-start.14 = (bf16[272,128]{1,0:T(8,128)(2,1)S(1)}, bf16[272,128]{1,0:T(8,128)(2,1)S(1)}, u32[]{:S(2)}, u32[]{:S(2)}) collective-permute-start(bf16[272,128]{1,0:T(8,128)(2,1)S(1)} %get-tuple-element.50), channel_id=1, source_target_pairs={{0,4},{4,0},{8,12},{12,8},{16,20},{20,16},{24,28},{28,24},{1,5},{5... | collective-permute-start | bytes 208904 | tf_op jit(solution)/shard_map/ppermute | solution.py:27
  42.5 4.5 %collective-permute-start.15 = (bf16[272,128]{1,0:T(8,128)(2,1)S(1)}, bf16[272,128]{1,0:T(8,128)(2,1)S(1)}, u32[]{:S(2)}, u32[]{:S(2)}) collective-permute-start(bf16[272,128]{1,0:T(8,128)(2,1)S(1)} %get-tuple-element.51), channel_id=1, source_target_pairs={{0,8},{4,12},{8,0},{12,4},{16,24},{20,28},{24,16},{28,20},{1,9},{5... | collective-permute-start | bytes 208904 | tf_op jit(solution)/shard_map/ppermute | solution.py:27
  44.1 5.2 %collective-permute-start.16 = (bf16[272,128]{1,0:T(8,128)(2,1)S(1)}, bf16[272,128]{1,0:T(8,128)(2,1)S(1)}, u32[]{:S(2)}, u32[]{:S(2)}) collective-permute-start(bf16[272,128]{1,0:T(8,128)(2,1)S(1)} %get-tuple-element.52), channel_id=1, source_target_pairs={{0,12},{4,8},{8,4},{12,0},{16,28},{20,24},{24,20},{28,16},{1,13},{... | collective-permute-start | bytes 208904 | tf_op jit(solution)/shard_map/ppermute | solution.py:27
  49.9 5.3 %collective-permute-start.17 = (bf16[144,128]{1,0:T(8,128)(2,1)S(1)}, bf16[144,128]{1,0:T(8,128)(2,1)S(1)}, u32[]{:S(2)}, u32[]{:S(2)}) collective-permute-start(bf16[144,128]{1,0:T(8,128)(2,1)S(1)} %get-tuple-element.55), channel_id=1, source_target_pairs={{0,16},{4,20},{8,24},{12,28},{16,0},{20,4},{24,8},{28,12},{1,17},{... | collective-permute-start | bytes 110600 | tf_op jit(solution)/shard_map/ppermute | solution.py:27
  55.7 3.7 %collective-permute-start.18 = (bf16[32,128]{1,0:T(8,128)(2,1)S(1)}, bf16[32,128]{1,0:T(8,128)(2,1)S(1)}, u32[]{:S(2)}, u32[]{:S(2)}) collective-permute-start(bf16[32,128]{1,0:T(8,128)(2,1)S(1)} %get-tuple-element.57), channel_id=1, source_target_pairs={{0,4},{4,0},{8,12},{12,8},{16,20},{20,16},{24,28},{28,24},{1,5},{5... | collective-permute-start | bytes 24584 | tf_op jit(solution)/shard_map/ppermute | solution.py:27
  55.8 3.7 %collective-permute-start.19 = (bf16[32,128]{1,0:T(8,128)(2,1)S(1)}, bf16[32,128]{1,0:T(8,128)(2,1)S(1)}, u32[]{:S(2)}, u32[]{:S(2)}) collective-permute-start(bf16[32,128]{1,0:T(8,128)(2,1)S(1)} %get-tuple-element.58), channel_id=1, source_target_pairs={{0,8},{4,12},{8,0},{12,4},{16,24},{20,28},{24,16},{28,20},{1,9},{5... | collective-permute-start | bytes 24584 | tf_op jit(solution)/shard_map/ppermute | solution.py:27
  57.3 4.5 %collective-permute-start.20 = (bf16[32,128]{1,0:T(8,128)(2,1)S(1)}, bf16[32,128]{1,0:T(8,128)(2,1)S(1)}, u32[]{:S(2)}, u32[]{:S(2)}) collective-permute-start(bf16[32,128]{1,0:T(8,128)(2,1)S(1)} %get-tuple-element.59), channel_id=1, source_target_pairs={{0,12},{4,8},{8,4},{12,0},{16,28},{20,24},{24,20},{28,16},{1,13},{... | collective-permute-start | bytes 24584 | tf_op jit(solution)/shard_map/ppermute | solution.py:27

commit v5 on v3

--- a/solution.py
+++ b/solution.py
@@ -224,10 +224,7 @@
     for h in range(heads):
         new = keep[h : h + 1, :] * states[h] + dot(turned[h], fresh[h])
         if last:
-            rest[h][0:DK, :] = new.astype(bf16)
-            asked = jnp.broadcast_to(query_ref[h : h + 1, :], (2 * SUB, DK))
-            asked = jnp.concatenate([asked, jnp.zeros((2 * SUB, DV), f32)], axis=1)
-            rest[h][DK:, :] = asked.astype(bf16)
+            rest[h][...] = passed_on(new, jnp.broadcast_to(query_ref[h : h + 1, :], (SUB, DK)))
         else:
             rest[-1][h] = new
 
@@ -269,22 +266,23 @@
 
 
 def passed_on(total, query):
-    asked = jnp.concatenate([query, query], axis=0)
-    asked = jnp.concatenate([asked, jnp.zeros((2 * SUB, DV), f32)], axis=1)
-    return jnp.concatenate([total, asked], axis=0).astype(bf16)
+    return jnp.concatenate([total[:, :DV], total[:, DV:], query, query], axis=0).astype(bf16)
+
+
+def received(ref):
+    total = jnp.concatenate([ref[:DK, :], ref[DK : 2 * DK, :]], axis=1)
+    return total.astype(f32), ref[2 * DK :, :].astype(f32)[:SUB]
 
 
 def compose_kernel(heads, final, *refs):
     own_ref, got = refs[0], refs[1:heads]
     out, scratch = refs[heads:-1], refs[-1]
     lead = lax.axis_index("sp") % heads
-    scratch[lead] = own_ref[:DK, :].astype(f32)
-    query = own_ref[DK:, :DK].astype(f32)
+    scratch[lead], query = received(own_ref)
     for k in range(1, heads):
-        scratch[lead ^ k] = got[k - 1][:DK, :].astype(f32)
-        query = query + got[k - 1][DK:, :DK].astype(f32)
+        scratch[lead ^ k], asked = received(got[k - 1])
+        query = query + asked
     total = compose([scratch[i] for i in range(heads)], dot)
-    query = query[:SUB]
     if final:
         finish(total, query, out)
     else:
@@ -294,8 +292,8 @@
 
 def merge_kernel(mask, final, own_ref, query_ref, got_ref, *out):
     high = late_side(mask)
-    own, got = own_ref[...], got_ref[:DK, :].astype(f32)
-    query = query_ref[...] + got_ref[DK:, :DK].astype(f32)[:SUB]
+    own, (got, asked) = own_ref[...], received(got_ref)
+    query = query_ref[...] + asked
     early, late = jnp.where(high, got, own), jnp.where(high, own, got)
     total = compose([early, late], dot3)
     if final:
@@ -470,7 +468,7 @@
         outs = [shape((heads, DK, DV + DK))]
         if last:
             arrays.append(query)
-            outs = [shape((DK + 2 * SUB, DV + DK), bf16)] * heads
+            outs = [shape((DK + DV + 2 * SUB, DK), bf16)] * heads
         result = call(
             functools.partial(
                 chunk_kernel, heads, c, last, tuple(m for m, _ in found), len(sums) > 0
@@ -487,7 +485,7 @@
     for k in reversed(range(1, heads)):
         got[k] = swap(maps[k], "sp", k)
     done = [shape((DK, DV + DK)), shape((SUB, DK))]
-    open_ended = done + [shape((DK + 2 * SUB, DV + DK), bf16)]
+    open_ended = done + [shape((DK + DV + 2 * SUB, DK), bf16)]
     if groups > 1:
         done.append(shape((DK + 2 * SUB, DV), bf16))
     result = call(

time: 61.4 us -> 61.2 us (level)
  no operation moved by 1% of the time
where the time goes in v5:
time: 61.2 us; the launch traced here: 61.1 us
  waiting for transfers between devices  20.9 us (34%)
  Pallas kernels  19.1 us (31%)
  starting transfers between devices  18.2 us (30%)
  local copies, waits for them, and re-layouts  2.13 us (3%)
  between operations  0.78 us (1%)
    ppermute x19, waiting for transfers between devices, swap(): return lax.ppermute(x, axis, flip(axis, mask))  20.9 us
    ppermute x19, starting transfers between devices, swap(): return lax.ppermute(x, axis, flip(axis, mask))  18.2 us
    pallas_call x11, Pallas kernels, call(): pl.pallas_call(body, out_shape=outs, in_specs=[vmem] * len(arrays), out_s...  15.3 us
    pallas_call x1, Pallas kernels, per_device(): pl.pallas_call(functools.partial(prepare_kernel, heads), out_shape=[shape...  3.84 us
  transfers between devices with their start and end apart: 19, of which 11 were waited for; matrix products, arithmetic and copies ran while one was open for 2% of the time, Pallas kernels for 25%

profile of v5, /device:TPU:0, one launch (start us, length us, event | category | flops | bytes accessed | tf_op | source)
XLA Modules:
  0.0 61.1 jit_solution(13632278714450972606)
XLA Ops:
  0.6 1.0 %slice.15.refs_0_ = bf16[128,1024]{1,0:T(8,128)(2,1)S(1)} slice(bf16[512,1024]{1,0:T(8,128)(2,1)} %param.10), slice={[0:128], [0:1024]} | slice | bytes 524288 | tf_op jit(solution)/shard_map/slice | solution.py:397
  1.6 3.1 %collective-permute-start.9 = (bf16[128,1024]{1,0:T(8,128)(2,1)S(1)}, bf16[128,1024]{1,0:T(8,128)(2,1)S(1)}, u32[]{:S(2)}, u32[]{:S(2)}) collective-permute-start(bf16[128,1024]{1,0:T(8,128)(2,1)S(1)} %slice.15.refs_0_), channel_id=1, source_target_pairs={{0,2},{1,3},{2,0},{3,1},{4,6},{5,7},{6,4},{7,5},{8,10},{9,11},{10,... | collective-permute-start | bytes 786440 | tf_op jit(solution)/shard_map/ppermute | solution.py:26
  4.7 1.2 %fusion = (bf16[128,1024]{1,0:T(8,128)(2,1)S(1)}, bf16[128,1024]{1,0:T(8,128)(2,1)S(1)}, bf16[128,1024]{1,0:T(8,128)(2,1)S(1)}) fusion(bf16[512,1024]{1,0:T(8,128)(2,1)} %param.10), kind=kLoop, calls=%fused_computation | loop fusion | bytes 1572864 | tf_op jit(solution)/shard_map/slice | solution.py:399
  6.4 2.0 %collective-permute-start.6 = (bf16[128,1024]{1,0:T(8,128)(2,1)S(1)}, bf16[128,1024]{1,0:T(8,128)(2,1)S(1)}, u32[]{:S(2)}, u32[]{:S(2)}) collective-permute-start(bf16[128,1024]{1,0:T(8,128)(2,1)S(1)} %get-tuple-element.60.refs_0_), channel_id=1, source_target_pairs={{0,2},{1,3},{2,0},{3,1},{4,6},{5,7},{6,4},{7,5},{8,10},{9,11},{10,... | collective-permute-start | bytes 786440 | tf_op jit(solution)/shard_map/ppermute | solution.py:26
  8.4 3.4 %collective-permute-done.9.refs_1_ = bf16[128,1024]{1,0:T(8,128)(2,1)S(1)} collective-permute-done((bf16[128,1024]{1,0:T(8,128)(2,1)S(1)}, bf16[128,1024]{1,0:T(8,128)(2,1)S(1)}, u32[]{:S(2)}, u32[]{:S(2)}) %collective-permute-start.9) | collective-permute-done | bytes 262176 | tf_op jit(solution)/shard_map/ppermute | solution.py:26
  11.8 2.0 %collective-permute-start.3 = (bf16[128,1024]{1,0:T(8,128)(2,1)S(1)}, bf16[128,1024]{1,0:T(8,128)(2,1)S(1)}, u32[]{:S(2)}, u32[]{:S(2)}) collective-permute-start(bf16[128,1024]{1,0:T(8,128)(2,1)S(1)} %get-tuple-element.61.refs_0_), channel_id=1, source_target_pairs={{0,2},{1,3},{2,0},{3,1},{4,6},{5,7},{6,4},{7,5},{8,10},{9,11},{10,... | collective-permute-start | bytes 786440 | tf_op jit(solution)/shard_map/ppermute | solution.py:26
  14.1 3.4 %collective-permute-done.refs_0_ = bf16[128,1024]{1,0:T(8,128)(2,1)S(1)} collective-permute-done((bf16[128,1024]{1,0:T(8,128)(2,1)S(1)}, bf16[128,1024]{1,0:T(8,128)(2,1)S(1)}, u32[]{:S(2)}, u32[]{:S(2)}) %collective-permute-start) | collective-permute-done | bytes 262176 | tf_op jit(solution)/shard_map/ppermute | solution.py:26
  17.4 3.8 %shard_map.113 = (bf16[4096,512]{1,0:T(8,128)(2,1)S(1)}, bf16[4096,512]{1,0:T(8,128)(2,1)S(1)}, bf16[16,4096]{1,0:T(8,128)(2,1)S(1)}, f32[8,128]{1,0:T(8,128)S(1...) custom-call(bf16[4096,512]{1,0:T(8,128)(2,1)} %refs_0_.1, bf16[4096,512]{1,0:T(8,128)(2,1)} %refs_1_.1, ...), custom_call_target="tpu_custom_call" | custom-call | tf_op jit(solution)/shard_map/pallas_call | solution.py:422
  23.3 0.9 %shard_map.117 = (f32[16,128]{1,0:T(8,128)S(1)}, f32[128,512]{1,0:T(8,128)S(1)}, f32[128,512]{1,0:T(8,128)S(1)}) custom-call(bf16[128,1024]{1,0:T(8,128)(2,1)S(1)} %get-tuple-element.60.refs_0_, bf16[128,1024]{1,0:T(8,128)(2,1)S(1)} %collective-permute-done.8.refs_1_, bf16[4096,512]{1,0:T(8,128)(2,1)S(1)} %get-tuple-element.31.refs_2_.refs_1_.refs_4_, ...), custom_call_target="tpu_custom_call" | custom-call | flops 603979776 | tf_op jit(solution)/shard_map/pallas_call | solution.py:363
  24.5 3.3 %collective-permute-done.3.refs_0_ = bf16[128,1024]{1,0:T(8,128)(2,1)S(1)} collective-permute-done((bf16[128,1024]{1,0:T(8,128)(2,1)S(1)}, bf16[128,1024]{1,0:T(8,128)(2,1)S(1)}, u32[]{:S(2)}, u32[]{:S(2)}) %collective-permute-start.3) | collective-permute-done | bytes 262176 | tf_op jit(solution)/shard_map/ppermute | solution.py:26
  28.7 3.2 %shard_map.118.refs_10_ = f32[4,128,256]{2,1,0:T(8,128)S(1)} custom-call(bf16[128,1024]{1,0:T(8,128)(2,1)S(1)} %slice.15.refs_0_, bf16[128,1024]{1,0:T(8,128)(2,1)S(1)} %collective-permute-done.9.refs_1_, bf16[128,1024]{1,0:T(8,128)(2,1)S(1)} %collective-permute-done.10.refs_2_, bf16[128,1024]{1,0:T(8,128)(2,1)S(1)} %collective-permute-done.11.refs_3_, ...), custom_call_target="tpu_custom_call" | custom-call | flops 1610612736 | tf_op jit(solution)/shard_map/pallas_call | solution.py:363
  31.9 2.5 %shard_map.119.refs_10_ = f32[4,128,256]{2,1,0:T(8,128)S(1)} custom-call(bf16[128,1024]{1,0:T(8,128)(2,1)S(1)} %collective-permute-done.6.refs_0_, bf16[128,1024]{1,0:T(8,128)(2,1)S(1)} %collective-permute-done.7.refs_1_, bf16[4096,512]{1,0:T(8,128)(2,1)S(1)} %get-tuple-element.31.refs_2_.refs_1_.refs_4_, ...), custom_call_target="tpu_custom_call" | custom-call | flops 1610612736 | tf_op jit(solution)/shard_map/pallas_call | solution.py:363
  34.4 2.5 %shard_map.120.refs_9_ = f32[4,128,256]{2,1,0:T(8,128)S(1)} custom-call(bf16[128,1024]{1,0:T(8,128)(2,1)S(1)} %collective-permute-done.3.refs_0_, bf16[128,1024]{1,0:T(8,128)(2,1)S(1)} %collective-permute-done.4.refs_1_, bf16[4096,512]{1,0:T(8,128)(2,1)S(1)} %get-tuple-element.31.refs_2_.refs_1_.refs_4_, ...), custom_call_target="tpu_custom_call" | custom-call | flops 1610612736 | tf_op jit(solution)/shard_map/pallas_call | solution.py:363
  36.9 2.3 %shard_map.121 = (bf16[272,128]{1,0:T(8,128)(2,1)S(1)}, bf16[272,128]{1,0:T(8,128)(2,1)S(1)}, bf16[272,128]{1,0:T(8,128)(2,1)S(1)}, bf16[272,128]{1,0:T(8,128)(2,1)S(1)}) custom-call(bf16[128,1024]{1,0:T(8,128)(2,1)S(1)} %collective-permute-done.1.refs_0_, bf16[4096,512]{1,0:T(8,128)(2,1)S(1)} %get-tuple-element.31.refs_2_.refs_1_.refs_4_, ...), custom_call_target="tpu_custom_call" | custom-call | flops 1610612736 | tf_op jit(solution)/shard_map/pallas_call | solution.py:363
  39.2 1.8 %collective-permute-start.12 = (bf16[272,128]{1,0:T(8,128)(2,1)S(1)}, bf16[272,128]{1,0:T(8,128)(2,1)S(1)}, u32[]{:S(2)}, u32[]{:S(2)}) collective-permute-start(bf16[272,128]{1,0:T(8,128)(2,1)S(1)} %get-tuple-element.50), channel_id=1, source_target_pairs={{0,4},{4,0},{8,12},{12,8},{16,20},{20,16},{24,28},{28,24},{1,5},{5... | collective-permute-start | bytes 208904 | tf_op jit(solution)/shard_map/ppermute | solution.py:26
  41.0 1.6 %collective-permute-start.13 = (bf16[272,128]{1,0:T(8,128)(2,1)S(1)}, bf16[272,128]{1,0:T(8,128)(2,1)S(1)}, u32[]{:S(2)}, u32[]{:S(2)}) collective-permute-start(bf16[272,128]{1,0:T(8,128)(2,1)S(1)} %get-tuple-element.51), channel_id=1, source_target_pairs={{0,8},{4,12},{8,0},{12,4},{16,24},{20,28},{24,16},{28,20},{1,9},{5... | collective-permute-start | bytes 208904 | tf_op jit(solution)/shard_map/ppermute | solution.py:26
  42.8 1.1 %collective-permute-done.12.refs_1_ = bf16[272,128]{1,0:T(8,128)(2,1)S(1)} collective-permute-done((bf16[272,128]{1,0:T(8,128)(2,1)S(1)}, bf16[272,128]{1,0:T(8,128)(2,1)S(1)}, u32[]{:S(2)}, u32[]{:S(2)}) %collective-permute-start.12) | collective-permute-done | bytes 69664 | tf_op jit(solution)/shard_map/ppermute | solution.py:26
  43.9 1.6 %collective-permute-done.13.refs_2_ = bf16[272,128]{1,0:T(8,128)(2,1)S(1)} collective-permute-done((bf16[272,128]{1,0:T(8,128)(2,1)S(1)}, bf16[272,128]{1,0:T(8,128)(2,1)S(1)}, u32[]{:S(2)}, u32[]{:S(2)}) %collective-permute-start.13) | collective-permute-done | bytes 69664 | tf_op jit(solution)/shard_map/ppermute | solution.py:26
  45.6 2.2 %collective-permute-done.14.refs_3_ = bf16[272,128]{1,0:T(8,128)(2,1)S(1)} collective-permute-done((bf16[272,128]{1,0:T(8,128)(2,1)S(1)}, bf16[272,128]{1,0:T(8,128)(2,1)S(1)}, u32[]{:S(2)}, u32[]{:S(2)}) %collective-permute-start.14) | collective-permute-done | bytes 69664 | tf_op jit(solution)/shard_map/ppermute | solution.py:26
  48.4 2.6 %collective-permute-start.15 = (bf16[144,128]{1,0:T(8,128)(2,1)S(1)}, bf16[144,128]{1,0:T(8,128)(2,1)S(1)}, u32[]{:S(2)}, u32[]{:S(2)}) collective-permute-start(bf16[144,128]{1,0:T(8,128)(2,1)S(1)} %get-tuple-element.55), channel_id=1, source_target_pairs={{0,16},{4,20},{8,24},{12,28},{16,0},{20,4},{24,8},{28,12},{1,17},{... | collective-permute-start | bytes 110600 | tf_op jit(solution)/shard_map/ppermute | solution.py:26
  51.0 2.7 %collective-permute-done.15.refs_0_ = bf16[144,128]{1,0:T(8,128)(2,1)S(1)} collective-permute-done((bf16[144,128]{1,0:T(8,128)(2,1)S(1)}, bf16[144,128]{1,0:T(8,128)(2,1)S(1)}, u32[]{:S(2)}, u32[]{:S(2)}) %collective-permute-start.15) | collective-permute-done | bytes 36896 | tf_op jit(solution)/shard_map/ppermute | solution.py:26
  54.3 1.5 %collective-permute-start.17 = (bf16[32,128]{1,0:T(8,128)(2,1)S(1)}, bf16[32,128]{1,0:T(8,128)(2,1)S(1)}, u32[]{:S(2)}, u32[]{:S(2)}) collective-permute-start(bf16[32,128]{1,0:T(8,128)(2,1)S(1)} %get-tuple-element.58), channel_id=1, source_target_pairs={{0,8},{4,12},{8,0},{12,4},{16,24},{20,28},{24,16},{28,20},{1,9},{5... | collective-permute-start | bytes 24584 | tf_op jit(solution)/shard_map/ppermute | solution.py:26
  55.8 1.8 %collective-permute-start.18 = (bf16[32,128]{1,0:T(8,128)(2,1)S(1)}, bf16[32,128]{1,0:T(8,128)(2,1)S(1)}, u32[]{:S(2)}, u32[]{:S(2)}) collective-permute-start(bf16[32,128]{1,0:T(8,128)(2,1)S(1)} %get-tuple-element.59), channel_id=1, source_target_pairs={{0,12},{4,8},{8,4},{12,0},{16,28},{20,24},{24,20},{28,16},{1,13},{... | collective-permute-start | bytes 24584 | tf_op jit(solution)/shard_map/ppermute | solution.py:26
  57.9 2.4 %collective-permute-done.18.refs_3_ = bf16[32,128]{1,0:T(8,128)(2,1)S(1)} collective-permute-done((bf16[32,128]{1,0:T(8,128)(2,1)S(1)}, bf16[32,128]{1,0:T(8,128)(2,1)S(1)}, u32[]{:S(2)}, u32[]{:S(2)}) %collective-permute-start.18) | collective-permute-done | bytes 8224 | tf_op jit(solution)/shard_map/ppermute | solution.py:26
  (30 shorter events, 6.4 us)
Async XLA Ops:
  1.6 10.2 %collective-permute-start.9 = (bf16[128,1024]{1,0:T(8,128)(2,1)S(1)}, bf16[128,1024]{1,0:T(8,128)(2,1)S(1)}, u32[]{:S(2)}, u32[]{:S(2)}) collective-permute-start(bf16[128,1024]{1,0:T(8,128)(2,1)S(1)} %slice.15.refs_0_), channel_id=1, source_target_pairs={{0,2},{1,3},{2,0},{3,1},{4,6},{5,7},{6,4},{7,5},{8,10},{9,11},{10,... | collective-permute-start | bytes 786440 | tf_op jit(solution)/shard_map/ppermute | solution.py:26
  5.8 6.0 %collective-permute-start.8 = (bf16[128,1024]{1,0:T(8,128)(2,1)S(1)}, bf16[128,1024]{1,0:T(8,128)(2,1)S(1)}, u32[]{:S(2)}, u32[]{:S(2)}) collective-permute-start(bf16[128,1024]{1,0:T(8,128)(2,1)S(1)} %get-tuple-element.60.refs_0_), channel_id=1, source_target_pairs={{0,1},{1,0},{2,3},{3,2},{4,5},{5,4},{6,7},{7,6},{8,9},{9,8},{10,11... | collective-permute-start | bytes 786440 | tf_op jit(solution)/shard_map/ppermute | solution.py:26
  5.9 7.9 %collective-permute-start.2 = (bf16[128,1024]{1,0:T(8,128)(2,1)S(1)}, bf16[128,1024]{1,0:T(8,128)(2,1)S(1)}, u32[]{:S(2)}, u32[]{:S(2)}) collective-permute-start(bf16[128,1024]{1,0:T(8,128)(2,1)S(1)} %get-tuple-element.62.refs_0_), channel_id=1, source_target_pairs={{0,1},{1,0},{2,3},{3,2},{4,5},{5,4},{6,7},{7,6},{8,9},{9,8},{10,11... | collective-permute-start | bytes 786440 | tf_op jit(solution)/shard_map/ppermute | solution.py:26
  6.4 11.0 %collective-permute-start = (bf16[128,1024]{1,0:T(8,128)(2,1)S(1)}, bf16[128,1024]{1,0:T(8,128)(2,1)S(1)}, u32[]{:S(2)}, u32[]{:S(2)}) collective-permute-start(bf16[128,1024]{1,0:T(8,128)(2,1)S(1)} %get-tuple-element.62.refs_0_), channel_id=1, source_target_pairs={{0,2},{1,3},{2,0},{3,1},{4,6},{5,7},{6,4},{7,5},{8,10},{9,11},{10,... | collective-permute-start | bytes 786440 | tf_op jit(solution)/shard_map/ppermute | solution.py:26
  6.4 16.6 %collective-permute-start.6 = (bf16[128,1024]{1,0:T(8,128)(2,1)S(1)}, bf16[128,1024]{1,0:T(8,128)(2,1)S(1)}, u32[]{:S(2)}, u32[]{:S(2)}) collective-permute-start(bf16[128,1024]{1,0:T(8,128)(2,1)S(1)} %get-tuple-element.60.refs_0_), channel_id=1, source_target_pairs={{0,2},{1,3},{2,0},{3,1},{4,6},{5,7},{6,4},{7,5},{8,10},{9,11},{10,... | collective-permute-start | bytes 786440 | tf_op jit(solution)/shard_map/ppermute | solution.py:26
  11.8 12.3 %collective-permute-start.5 = (bf16[128,1024]{1,0:T(8,128)(2,1)S(1)}, bf16[128,1024]{1,0:T(8,128)(2,1)S(1)}, u32[]{:S(2)}, u32[]{:S(2)}) collective-permute-start(bf16[128,1024]{1,0:T(8,128)(2,1)S(1)} %get-tuple-element.61.refs_0_), channel_id=1, source_target_pairs={{0,1},{1,0},{2,3},{3,2},{4,5},{5,4},{6,7},{7,6},{8,9},{9,8},{10,11... | collective-permute-start | bytes 786440 | tf_op jit(solution)/shard_map/ppermute | solution.py:26
  11.8 16.0 %collective-permute-start.3 = (bf16[128,1024]{1,0:T(8,128)(2,1)S(1)}, bf16[128,1024]{1,0:T(8,128)(2,1)S(1)}, u32[]{:S(2)}, u32[]{:S(2)}) collective-permute-start(bf16[128,1024]{1,0:T(8,128)(2,1)S(1)} %get-tuple-element.61.refs_0_), channel_id=1, source_target_pairs={{0,2},{1,3},{2,0},{3,1},{4,6},{5,7},{6,4},{7,5},{8,10},{9,11},{10,... | collective-permute-start | bytes 786440 | tf_op jit(solution)/shard_map/ppermute | solution.py:26
  13.8 14.8 %collective-permute-start.10 = (bf16[128,1024]{1,0:T(8,128)(2,1)S(1)}, bf16[128,1024]{1,0:T(8,128)(2,1)S(1)}, u32[]{:S(2)}, u32[]{:S(2)}) collective-permute-start(bf16[128,1024]{1,0:T(8,128)(2,1)S(1)} %slice.15.refs_0_), channel_id=1, source_target_pairs={{0,1},{1,0},{2,3},{3,2},{4,5},{5,4},{6,7},{7,6},{8,9},{9,8},{10,11... | collective-permute-start | bytes 786440 | tf_op jit(solution)/shard_map/ppermute | solution.py:26
  17.4 11.3 %collective-permute-start.11 = (bf16[128,1024]{1,0:T(8,128)(2,1)S(1)}, bf16[128,1024]{1,0:T(8,128)(2,1)S(1)}, u32[]{:S(2)}, u32[]{:S(2)}) collective-permute-start(bf16[128,1024]{1,0:T(8,128)(2,1)S(1)} %collective-permute-done.9.refs_1_), channel_id=1, source_target_pairs={{0,1},{1,0},{2,3},{3,2},{4,5},{5,4},{6,7},{7,6},{8,9},{9,8},{10,11... | collective-permute-start | bytes 786440 | tf_op jit(solution)/shard_map/ppermute | solution.py:26
  23.1 8.8 %collective-permute-start.7 = (bf16[128,1024]{1,0:T(8,128)(2,1)S(1)}, bf16[128,1024]{1,0:T(8,128)(2,1)S(1)}, u32[]{:S(2)}, u32[]{:S(2)}) collective-permute-start(bf16[128,1024]{1,0:T(8,128)(2,1)S(1)} %collective-permute-done.6.refs_0_), channel_id=1, source_target_pairs={{0,1},{1,0},{2,3},{3,2},{4,5},{5,4},{6,7},{7,6},{8,9},{9,8},{10,11... | collective-permute-start | bytes 786440 | tf_op jit(solution)/shard_map/ppermute | solution.py:26
  24.1 12.8 %collective-permute-start.1 = (bf16[128,1024]{1,0:T(8,128)(2,1)S(1)}, bf16[128,1024]{1,0:T(8,128)(2,1)S(1)}, u32[]{:S(2)}, u32[]{:S(2)}) collective-permute-start(bf16[128,1024]{1,0:T(8,128)(2,1)S(1)} %collective-permute-done.refs_0_), channel_id=1, source_target_pairs={{0,1},{1,0},{2,3},{3,2},{4,5},{5,4},{6,7},{7,6},{8,9},{9,8},{10,11... | collective-permute-start | bytes 786440 | tf_op jit(solution)/shard_map/ppermute | solution.py:26
  27.8 6.6 %collective-permute-start.4 = (bf16[128,1024]{1,0:T(8,128)(2,1)S(1)}, bf16[128,1024]{1,0:T(8,128)(2,1)S(1)}, u32[]{:S(2)}, u32[]{:S(2)}) collective-permute-start(bf16[128,1024]{1,0:T(8,128)(2,1)S(1)} %collective-permute-done.3.refs_0_), channel_id=1, source_target_pairs={{0,1},{1,0},{2,3},{3,2},{4,5},{5,4},{6,7},{7,6},{8,9},{9,8},{10,11... | collective-permute-start | bytes 786440 | tf_op jit(solution)/shard_map/ppermute | solution.py:26
  36.9 23.4 %copy-start = (bf16[128]{0:T(256)(128)(2,1)S(1)}, bf16[128]{0:T(256)(128)(2,1)}, u32[]{:S(2)}) copy-start(bf16[128]{0:T(256)(128)(2,1)} %param.19) | copy-start | bytes 772
  39.2 4.7 %collective-permute-start.12 = (bf16[272,128]{1,0:T(8,128)(2,1)S(1)}, bf16[272,128]{1,0:T(8,128)(2,1)S(1)}, u32[]{:S(2)}, u32[]{:S(2)}) collective-permute-start(bf16[272,128]{1,0:T(8,128)(2,1)S(1)} %get-tuple-element.50), channel_id=1, source_target_pairs={{0,4},{4,0},{8,12},{12,8},{16,20},{20,16},{24,28},{28,24},{1,5},{5... | collective-permute-start | bytes 208904 | tf_op jit(solution)/shard_map/ppermute | solution.py:26
  41.0 4.5 %collective-permute-start.13 = (bf16[272,128]{1,0:T(8,128)(2,1)S(1)}, bf16[272,128]{1,0:T(8,128)(2,1)S(1)}, u32[]{:S(2)}, u32[]{:S(2)}) collective-permute-start(bf16[272,128]{1,0:T(8,128)(2,1)S(1)} %get-tuple-element.51), channel_id=1, source_target_pairs={{0,8},{4,12},{8,0},{12,4},{16,24},{20,28},{24,16},{28,20},{1,9},{5... | collective-permute-start | bytes 208904 | tf_op jit(solution)/shard_map/ppermute | solution.py:26
  42.6 5.2 %collective-permute-start.14 = (bf16[272,128]{1,0:T(8,128)(2,1)S(1)}, bf16[272,128]{1,0:T(8,128)(2,1)S(1)}, u32[]{:S(2)}, u32[]{:S(2)}) collective-permute-start(bf16[272,128]{1,0:T(8,128)(2,1)S(1)} %get-tuple-element.52), channel_id=1, source_target_pairs={{0,12},{4,8},{8,4},{12,0},{16,28},{20,24},{24,20},{28,16},{1,13},{... | collective-permute-start | bytes 208904 | tf_op jit(solution)/shard_map/ppermute | solution.py:26
  48.4 5.3 %collective-permute-start.15 = (bf16[144,128]{1,0:T(8,128)(2,1)S(1)}, bf16[144,128]{1,0:T(8,128)(2,1)S(1)}, u32[]{:S(2)}, u32[]{:S(2)}) collective-permute-start(bf16[144,128]{1,0:T(8,128)(2,1)S(1)} %get-tuple-element.55), channel_id=1, source_target_pairs={{0,16},{4,20},{8,24},{12,28},{16,0},{20,4},{24,8},{28,12},{1,17},{... | collective-permute-start | bytes 110600 | tf_op jit(solution)/shard_map/ppermute | solution.py:26
  54.1 3.7 %collective-permute-start.16 = (bf16[32,128]{1,0:T(8,128)(2,1)S(1)}, bf16[32,128]{1,0:T(8,128)(2,1)S(1)}, u32[]{:S(2)}, u32[]{:S(2)}) collective-permute-start(bf16[32,128]{1,0:T(8,128)(2,1)S(1)} %get-tuple-element.57), channel_id=1, source_target_pairs={{0,4},{4,0},{8,12},{12,8},{16,20},{20,16},{24,28},{28,24},{1,5},{5... | collective-permute-start | bytes 24584 | tf_op jit(solution)/shard_map/ppermute | solution.py:26
  54.3 3.7 %collective-permute-start.17 = (bf16[32,128]{1,0:T(8,128)(2,1)S(1)}, bf16[32,128]{1,0:T(8,128)(2,1)S(1)}, u32[]{:S(2)}, u32[]{:S(2)}) collective-permute-start(bf16[32,128]{1,0:T(8,128)(2,1)S(1)} %get-tuple-element.58), channel_id=1, source_target_pairs={{0,8},{4,12},{8,0},{12,4},{16,24},{20,28},{24,16},{28,20},{1,9},{5... | collective-permute-start | bytes 24584 | tf_op jit(solution)/shard_map/ppermute | solution.py:26
  55.8 4.5 %collective-permute-start.18 = (bf16[32,128]{1,0:T(8,128)(2,1)S(1)}, bf16[32,128]{1,0:T(8,128)(2,1)S(1)}, u32[]{:S(2)}, u32[]{:S(2)}) collective-permute-start(bf16[32,128]{1,0:T(8,128)(2,1)S(1)} %get-tuple-element.59), channel_id=1, source_target_pairs={{0,12},{4,8},{8,4},{12,0},{16,28},{20,24},{24,20},{28,16},{1,13},{... | collective-permute-start | bytes 24584 | tf_op jit(solution)/shard_map/ppermute | solution.py:26

commit v6 on v5

--- a/solution.py
+++ b/solution.py
@@ -109,6 +109,12 @@
         sums, rest = tuple(ref[...] for ref in rest[:3]), rest[3:]
     for ref, x in zip(rest, project(masks, refs[:pieces], *weights, sums)):
         ref[...] = x
+
+
+def rows_copy_kernel(tokens_hbm, out_ref, sem):
+    copy = pltpu.make_async_copy(tokens_hbm.at[: out_ref.shape[0]], out_ref, sem)
+    copy.start()
+    copy.wait()
 
 
 def prepare_kernel(heads, *refs):
@@ -394,9 +400,15 @@
     chunk = min(CHUNK, length)
     chunks = length // chunk
 
-    owns = [tokens[:chunk]]
-    later = lax.optimization_barrier(tokens)
-    owns += [later[c * chunk : (c + 1) * chunk] for c in range(1, chunks)]
+    first_rows = pl.pallas_call(
+        rows_copy_kernel,
+        out_shape=shape((chunk, width), bf16),
+        in_specs=[pl.BlockSpec(memory_space=pltpu.HBM)],
+        out_specs=vmem,
+        scratch_shapes=[pltpu.SemaphoreType.DMA(())],
+        compiler_params=pltpu.CompilerParams(vmem_limit_bytes=4 * 1024 * 1024),
+    )(pltpu.with_memory_space_constraint(tokens, pltpu.HBM))
+    owns = [first_rows] + [tokens[c * chunk : (c + 1) * chunk] for c in range(1, chunks)]
     gathered = []
     for c in range(chunks):
         found = [(0, owns[c])]

time: 61.2 us -> 61.2 us (level)
  local copies, waits for them, and re-layouts: 2.13 us -> 1.16 us
  Pallas kernels: 19.1 us -> 20 us
    slice x2 -> x1, local copies, waits for them, and re-layouts: 2.13 us -> 1.16 us  [per_device(): tokens[c * chunk:(c + 1) * chunk]]
    pallas_call x0 -> x1, Pallas kernels: none -> 0.96 us  [per_device(): pl.pallas_call(rows_copy_kernel, out_shape=shape((chunk, width), bf16), i...]
where the time goes in v6:
time: 61.2 us; the launch traced here: 61 us
  waiting for transfers between devices  20.9 us (34%)
  Pallas kernels  20 us (33%)
  starting transfers between devices  18.2 us (30%)
  local copies, waits for them, and re-layouts  1.16 us (2%)
  between operations  0.79 us (1%)
    ppermute x19, waiting for transfers between devices, swap(): return lax.ppermute(x, axis, flip(axis, mask))  20.9 us
    ppermute x19, starting transfers between devices, swap(): return lax.ppermute(x, axis, flip(axis, mask))  18.2 us
    pallas_call x11, Pallas kernels, call(): pl.pallas_call(body, out_shape=outs, in_specs=[vmem] * len(arrays), out_s...  15.2 us
    pallas_call x1, Pallas kernels, per_device(): pl.pallas_call(functools.partial(prepare_kernel, heads), out_shape=[shape...  3.84 us
  transfers between devices with their start and end apart: 19, of which 11 were waited for; matrix products, arithmetic and copies ran while one was open for 2% of the time, Pallas kernels for 25%

profile of v6, /device:TPU:0, one launch (start us, length us, event | category | flops | bytes accessed | tf_op | source)
XLA Modules:
  0.0 61.0 jit_solution(14991578484554156657)
XLA Ops:
  0.6 1.0 %shard_map.118.refs_0_ = bf16[128,1024]{1,0:T(8,128)(2,1)S(1)} custom-call(bf16[512,1024]{1,0:T(8,128)(2,1)} %tokens_hbm.1), custom_call_target="tpu_custom_call" | custom-call | tf_op jit(solution)/shard_map/pallas_call | solution.py:403
  1.6 3.1 %collective-permute-start.9 = (bf16[128,1024]{1,0:T(8,128)(2,1)S(1)}, bf16[128,1024]{1,0:T(8,128)(2,1)S(1)}, u32[]{:S(2)}, u32[]{:S(2)}) collective-permute-start(bf16[128,1024]{1,0:T(8,128)(2,1)S(1)} %shard_map.118.refs_0_), channel_id=1, source_target_pairs={{0,2},{1,3},{2,0},{3,1},{4,6},{5,7},{6,4},{7,5},{8,10},{9,11},{10,... | collective-permute-start | bytes 786440 | tf_op jit(solution)/shard_map/ppermute | solution.py:26
  4.7 1.2 %fusion = (bf16[128,1024]{1,0:T(8,128)(2,1)S(1)}, bf16[128,1024]{1,0:T(8,128)(2,1)S(1)}, bf16[128,1024]{1,0:T(8,128)(2,1)S(1)}) fusion(bf16[512,1024]{1,0:T(8,128)(2,1)} %tokens_hbm.1), kind=kLoop, calls=%fused_computation | loop fusion | bytes 1572864 | tf_op jit(solution)/shard_map/slice | solution.py:411
  6.4 2.0 %collective-permute-start.6 = (bf16[128,1024]{1,0:T(8,128)(2,1)S(1)}, bf16[128,1024]{1,0:T(8,128)(2,1)S(1)}, u32[]{:S(2)}, u32[]{:S(2)}) collective-permute-start(bf16[128,1024]{1,0:T(8,128)(2,1)S(1)} %get-tuple-element.60.refs_0_), channel_id=1, source_target_pairs={{0,2},{1,3},{2,0},{3,1},{4,6},{5,7},{6,4},{7,5},{8,10},{9,11},{10,... | collective-permute-start | bytes 786440 | tf_op jit(solution)/shard_map/ppermute | solution.py:26
  8.4 3.4 %collective-permute-done.9.refs_1_ = bf16[128,1024]{1,0:T(8,128)(2,1)S(1)} collective-permute-done((bf16[128,1024]{1,0:T(8,128)(2,1)S(1)}, bf16[128,1024]{1,0:T(8,128)(2,1)S(1)}, u32[]{:S(2)}, u32[]{:S(2)}) %collective-permute-start.9) | collective-permute-done | bytes 262176 | tf_op jit(solution)/shard_map/ppermute | solution.py:26
  11.8 2.0 %collective-permute-start.3 = (bf16[128,1024]{1,0:T(8,128)(2,1)S(1)}, bf16[128,1024]{1,0:T(8,128)(2,1)S(1)}, u32[]{:S(2)}, u32[]{:S(2)}) collective-permute-start(bf16[128,1024]{1,0:T(8,128)(2,1)S(1)} %get-tuple-element.61.refs_0_), channel_id=1, source_target_pairs={{0,2},{1,3},{2,0},{3,1},{4,6},{5,7},{6,4},{7,5},{8,10},{9,11},{10,... | collective-permute-start | bytes 786440 | tf_op jit(solution)/shard_map/ppermute | solution.py:26
  14.1 3.4 %collective-permute-done.refs_0_ = bf16[128,1024]{1,0:T(8,128)(2,1)S(1)} collective-permute-done((bf16[128,1024]{1,0:T(8,128)(2,1)S(1)}, bf16[128,1024]{1,0:T(8,128)(2,1)S(1)}, u32[]{:S(2)}, u32[]{:S(2)}) %collective-permute-start) | collective-permute-done | bytes 262176 | tf_op jit(solution)/shard_map/ppermute | solution.py:26
  17.4 3.8 %shard_map.113 = (bf16[4096,512]{1,0:T(8,128)(2,1)S(1)}, bf16[4096,512]{1,0:T(8,128)(2,1)S(1)}, bf16[16,4096]{1,0:T(8,128)(2,1)S(1)}, f32[8,128]{1,0:T(8,128)S(1...) custom-call(bf16[4096,512]{1,0:T(8,128)(2,1)} %refs_0_.1, bf16[4096,512]{1,0:T(8,128)(2,1)} %refs_1_.1, ...), custom_call_target="tpu_custom_call" | custom-call | tf_op jit(solution)/shard_map/pallas_call | solution.py:434
  21.3 0.9 %shard_map.114 = (f32[16,128]{1,0:T(8,128)S(1)}, f32[128,512]{1,0:T(8,128)S(1)}, f32[128,512]{1,0:T(8,128)S(1)}) custom-call(bf16[128,1024]{1,0:T(8,128)(2,1)S(1)} %get-tuple-element.62.refs_0_, bf16[128,1024]{1,0:T(8,128)(2,1)S(1)} %collective-permute-done.2.refs_1_, bf16[4096,512]{1,0:T(8,128)(2,1)S(1)} %get-tuple-element.31.refs_2_.refs_1_.refs_4_, ...), custom_call_target="tpu_custom_call" | custom-call | flops 603979776 | tf_op jit(solution)/shard_map/pallas_call | solution.py:369
  24.5 3.3 %collective-permute-done.3.refs_0_ = bf16[128,1024]{1,0:T(8,128)(2,1)S(1)} collective-permute-done((bf16[128,1024]{1,0:T(8,128)(2,1)S(1)}, bf16[128,1024]{1,0:T(8,128)(2,1)S(1)}, u32[]{:S(2)}, u32[]{:S(2)}) %collective-permute-start.3) | collective-permute-done | bytes 262176 | tf_op jit(solution)/shard_map/ppermute | solution.py:26
  28.7 3.2 %shard_map.119.refs_10_ = f32[4,128,256]{2,1,0:T(8,128)S(1)} custom-call(bf16[128,1024]{1,0:T(8,128)(2,1)S(1)} %shard_map.118.refs_0_, bf16[128,1024]{1,0:T(8,128)(2,1)S(1)} %collective-permute-done.9.refs_1_, bf16[128,1024]{1,0:T(8,128)(2,1)S(1)} %collective-permute-done.10.refs_2_, bf16[128,1024]{1,0:T(8,128)(2,1)S(1)} %collective-permute-done.11.refs_3_, ...), custom_call_target="tpu_custom_call" | custom-call | flops 1610612736 | tf_op jit(solution)/shard_map/pallas_call | solution.py:369
  31.9 2.5 %shard_map.120.refs_10_ = f32[4,128,256]{2,1,0:T(8,128)S(1)} custom-call(bf16[128,1024]{1,0:T(8,128)(2,1)S(1)} %collective-permute-done.6.refs_0_, bf16[128,1024]{1,0:T(8,128)(2,1)S(1)} %collective-permute-done.7.refs_1_, bf16[4096,512]{1,0:T(8,128)(2,1)S(1)} %get-tuple-element.31.refs_2_.refs_1_.refs_4_, ...), custom_call_target="tpu_custom_call" | custom-call | flops 1610612736 | tf_op jit(solution)/shard_map/pallas_call | solution.py:369
  34.4 2.5 %shard_map.121.refs_9_ = f32[4,128,256]{2,1,0:T(8,128)S(1)} custom-call(bf16[128,1024]{1,0:T(8,128)(2,1)S(1)} %collective-permute-done.3.refs_0_, bf16[128,1024]{1,0:T(8,128)(2,1)S(1)} %collective-permute-done.4.refs_1_, bf16[4096,512]{1,0:T(8,128)(2,1)S(1)} %get-tuple-element.31.refs_2_.refs_1_.refs_4_, ...), custom_call_target="tpu_custom_call" | custom-call | flops 1610612736 | tf_op jit(solution)/shard_map/pallas_call | solution.py:369
  36.9 2.3 %shard_map.122 = (bf16[272,128]{1,0:T(8,128)(2,1)S(1)}, bf16[272,128]{1,0:T(8,128)(2,1)S(1)}, bf16[272,128]{1,0:T(8,128)(2,1)S(1)}, bf16[272,128]{1,0:T(8,128)(2,1)S(1)}) custom-call(bf16[128,1024]{1,0:T(8,128)(2,1)S(1)} %collective-permute-done.1.refs_0_, bf16[4096,512]{1,0:T(8,128)(2,1)S(1)} %get-tuple-element.31.refs_2_.refs_1_.refs_4_, ...), custom_call_target="tpu_custom_call" | custom-call | flops 1610612736 | tf_op jit(solution)/shard_map/pallas_call | solution.py:369
  39.2 1.8 %collective-permute-start.12 = (bf16[272,128]{1,0:T(8,128)(2,1)S(1)}, bf16[272,128]{1,0:T(8,128)(2,1)S(1)}, u32[]{:S(2)}, u32[]{:S(2)}) collective-permute-start(bf16[272,128]{1,0:T(8,128)(2,1)S(1)} %get-tuple-element.50), channel_id=1, source_target_pairs={{0,4},{4,0},{8,12},{12,8},{16,20},{20,16},{24,28},{28,24},{1,5},{5... | collective-permute-start | bytes 208904 | tf_op jit(solution)/shard_map/ppermute | solution.py:26
  41.0 1.6 %collective-permute-start.13 = (bf16[272,128]{1,0:T(8,128)(2,1)S(1)}, bf16[272,128]{1,0:T(8,128)(2,1)S(1)}, u32[]{:S(2)}, u32[]{:S(2)}) collective-permute-start(bf16[272,128]{1,0:T(8,128)(2,1)S(1)} %get-tuple-element.51), channel_id=1, source_target_pairs={{0,8},{4,12},{8,0},{12,4},{16,24},{20,28},{24,16},{28,20},{1,9},{5... | collective-permute-start | bytes 208904 | tf_op jit(solution)/shard_map/ppermute | solution.py:26
  42.8 1.1 %collective-permute-done.12.refs_1_ = bf16[272,128]{1,0:T(8,128)(2,1)S(1)} collective-permute-done((bf16[272,128]{1,0:T(8,128)(2,1)S(1)}, bf16[272,128]{1,0:T(8,128)(2,1)S(1)}, u32[]{:S(2)}, u32[]{:S(2)}) %collective-permute-start.12) | collective-permute-done | bytes 69664 | tf_op jit(solution)/shard_map/ppermute | solution.py:26
  43.9 1.7 %collective-permute-done.13.refs_2_ = bf16[272,128]{1,0:T(8,128)(2,1)S(1)} collective-permute-done((bf16[272,128]{1,0:T(8,128)(2,1)S(1)}, bf16[272,128]{1,0:T(8,128)(2,1)S(1)}, u32[]{:S(2)}, u32[]{:S(2)}) %collective-permute-start.13) | collective-permute-done | bytes 69664 | tf_op jit(solution)/shard_map/ppermute | solution.py:26
  45.6 2.2 %collective-permute-done.14.refs_3_ = bf16[272,128]{1,0:T(8,128)(2,1)S(1)} collective-permute-done((bf16[272,128]{1,0:T(8,128)(2,1)S(1)}, bf16[272,128]{1,0:T(8,128)(2,1)S(1)}, u32[]{:S(2)}, u32[]{:S(2)}) %collective-permute-start.14) | collective-permute-done | bytes 69664 | tf_op jit(solution)/shard_map/ppermute | solution.py:26
  48.4 2.6 %collective-permute-start.15 = (bf16[144,128]{1,0:T(8,128)(2,1)S(1)}, bf16[144,128]{1,0:T(8,128)(2,1)S(1)}, u32[]{:S(2)}, u32[]{:S(2)}) collective-permute-start(bf16[144,128]{1,0:T(8,128)(2,1)S(1)} %get-tuple-element.55), channel_id=1, source_target_pairs={{0,16},{4,20},{8,24},{12,28},{16,0},{20,4},{24,8},{28,12},{1,17},{... | collective-permute-start | bytes 110600 | tf_op jit(solution)/shard_map/ppermute | solution.py:26
  51.0 2.7 %collective-permute-done.15.refs_0_ = bf16[144,128]{1,0:T(8,128)(2,1)S(1)} collective-permute-done((bf16[144,128]{1,0:T(8,128)(2,1)S(1)}, bf16[144,128]{1,0:T(8,128)(2,1)S(1)}, u32[]{:S(2)}, u32[]{:S(2)}) %collective-permute-start.15) | collective-permute-done | bytes 36896 | tf_op jit(solution)/shard_map/ppermute | solution.py:26
  54.3 1.5 %collective-permute-start.17 = (bf16[32,128]{1,0:T(8,128)(2,1)S(1)}, bf16[32,128]{1,0:T(8,128)(2,1)S(1)}, u32[]{:S(2)}, u32[]{:S(2)}) collective-permute-start(bf16[32,128]{1,0:T(8,128)(2,1)S(1)} %get-tuple-element.58), channel_id=1, source_target_pairs={{0,8},{4,12},{8,0},{12,4},{16,24},{20,28},{24,16},{28,20},{1,9},{5... | collective-permute-start | bytes 24584 | tf_op jit(solution)/shard_map/ppermute | solution.py:26
  55.8 1.8 %collective-permute-start.18 = (bf16[32,128]{1,0:T(8,128)(2,1)S(1)}, bf16[32,128]{1,0:T(8,128)(2,1)S(1)}, u32[]{:S(2)}, u32[]{:S(2)}) collective-permute-start(bf16[32,128]{1,0:T(8,128)(2,1)S(1)} %get-tuple-element.59), channel_id=1, source_target_pairs={{0,12},{4,8},{8,4},{12,0},{16,28},{20,24},{24,20},{28,16},{1,13},{... | collective-permute-start | bytes 24584 | tf_op jit(solution)/shard_map/ppermute | solution.py:26
  57.9 2.4 %collective-permute-done.18.refs_3_ = bf16[32,128]{1,0:T(8,128)(2,1)S(1)} collective-permute-done((bf16[32,128]{1,0:T(8,128)(2,1)S(1)}, bf16[32,128]{1,0:T(8,128)(2,1)S(1)}, u32[]{:S(2)}, u32[]{:S(2)}) %collective-permute-start.18) | collective-permute-done | bytes 8224 | tf_op jit(solution)/shard_map/ppermute | solution.py:26
  (30 shorter events, 6.4 us)
Async XLA Ops:
  1.6 10.2 %collective-permute-start.9 = (bf16[128,1024]{1,0:T(8,128)(2,1)S(1)}, bf16[128,1024]{1,0:T(8,128)(2,1)S(1)}, u32[]{:S(2)}, u32[]{:S(2)}) collective-permute-start(bf16[128,1024]{1,0:T(8,128)(2,1)S(1)} %shard_map.118.refs_0_), channel_id=1, source_target_pairs={{0,2},{1,3},{2,0},{3,1},{4,6},{5,7},{6,4},{7,5},{8,10},{9,11},{10,... | collective-permute-start | bytes 786440 | tf_op jit(solution)/shard_map/ppermute | solution.py:26
  5.8 6.0 %collective-permute-start.8 = (bf16[128,1024]{1,0:T(8,128)(2,1)S(1)}, bf16[128,1024]{1,0:T(8,128)(2,1)S(1)}, u32[]{:S(2)}, u32[]{:S(2)}) collective-permute-start(bf16[128,1024]{1,0:T(8,128)(2,1)S(1)} %get-tuple-element.60.refs_0_), channel_id=1, source_target_pairs={{0,1},{1,0},{2,3},{3,2},{4,5},{5,4},{6,7},{7,6},{8,9},{9,8},{10,11... | collective-permute-start | bytes 786440 | tf_op jit(solution)/shard_map/ppermute | solution.py:26
  5.9 7.9 %collective-permute-start.2 = (bf16[128,1024]{1,0:T(8,128)(2,1)S(1)}, bf16[128,1024]{1,0:T(8,128)(2,1)S(1)}, u32[]{:S(2)}, u32[]{:S(2)}) collective-permute-start(bf16[128,1024]{1,0:T(8,128)(2,1)S(1)} %get-tuple-element.62.refs_0_), channel_id=1, source_target_pairs={{0,1},{1,0},{2,3},{3,2},{4,5},{5,4},{6,7},{7,6},{8,9},{9,8},{10,11... | collective-permute-start | bytes 786440 | tf_op jit(solution)/shard_map/ppermute | solution.py:26
  6.4 11.0 %collective-permute-start = (bf16[128,1024]{1,0:T(8,128)(2,1)S(1)}, bf16[128,1024]{1,0:T(8,128)(2,1)S(1)}, u32[]{:S(2)}, u32[]{:S(2)}) collective-permute-start(bf16[128,1024]{1,0:T(8,128)(2,1)S(1)} %get-tuple-element.62.refs_0_), channel_id=1, source_target_pairs={{0,2},{1,3},{2,0},{3,1},{4,6},{5,7},{6,4},{7,5},{8,10},{9,11},{10,... | collective-permute-start | bytes 786440 | tf_op jit(solution)/shard_map/ppermute | solution.py:26
  6.4 16.6 %collective-permute-start.6 = (bf16[128,1024]{1,0:T(8,128)(2,1)S(1)}, bf16[128,1024]{1,0:T(8,128)(2,1)S(1)}, u32[]{:S(2)}, u32[]{:S(2)}) collective-permute-start(bf16[128,1024]{1,0:T(8,128)(2,1)S(1)} %get-tuple-element.60.refs_0_), channel_id=1, source_target_pairs={{0,2},{1,3},{2,0},{3,1},{4,6},{5,7},{6,4},{7,5},{8,10},{9,11},{10,... | collective-permute-start | bytes 786440 | tf_op jit(solution)/shard_map/ppermute | solution.py:26
  11.8 12.3 %collective-permute-start.5 = (bf16[128,1024]{1,0:T(8,128)(2,1)S(1)}, bf16[128,1024]{1,0:T(8,128)(2,1)S(1)}, u32[]{:S(2)}, u32[]{:S(2)}) collective-permute-start(bf16[128,1024]{1,0:T(8,128)(2,1)S(1)} %get-tuple-element.61.refs_0_), channel_id=1, source_target_pairs={{0,1},{1,0},{2,3},{3,2},{4,5},{5,4},{6,7},{7,6},{8,9},{9,8},{10,11... | collective-permute-start | bytes 786440 | tf_op jit(solution)/shard_map/ppermute | solution.py:26
  11.8 16.0 %collective-permute-start.3 = (bf16[128,1024]{1,0:T(8,128)(2,1)S(1)}, bf16[128,1024]{1,0:T(8,128)(2,1)S(1)}, u32[]{:S(2)}, u32[]{:S(2)}) collective-permute-start(bf16[128,1024]{1,0:T(8,128)(2,1)S(1)} %get-tuple-element.61.refs_0_), channel_id=1, source_target_pairs={{0,2},{1,3},{2,0},{3,1},{4,6},{5,7},{6,4},{7,5},{8,10},{9,11},{10,... | collective-permute-start | bytes 786440 | tf_op jit(solution)/shard_map/ppermute | solution.py:26
  13.8 14.8 %collective-permute-start.10 = (bf16[128,1024]{1,0:T(8,128)(2,1)S(1)}, bf16[128,1024]{1,0:T(8,128)(2,1)S(1)}, u32[]{:S(2)}, u32[]{:S(2)}) collective-permute-start(bf16[128,1024]{1,0:T(8,128)(2,1)S(1)} %shard_map.118.refs_0_), channel_id=1, source_target_pairs={{0,1},{1,0},{2,3},{3,2},{4,5},{5,4},{6,7},{7,6},{8,9},{9,8},{10,11... | collective-permute-start | bytes 786440 | tf_op jit(solution)/shard_map/ppermute | solution.py:26
  17.4 11.3 %collective-permute-start.11 = (bf16[128,1024]{1,0:T(8,128)(2,1)S(1)}, bf16[128,1024]{1,0:T(8,128)(2,1)S(1)}, u32[]{:S(2)}, u32[]{:S(2)}) collective-permute-start(bf16[128,1024]{1,0:T(8,128)(2,1)S(1)} %collective-permute-done.9.refs_1_), channel_id=1, source_target_pairs={{0,1},{1,0},{2,3},{3,2},{4,5},{5,4},{6,7},{7,6},{8,9},{9,8},{10,11... | collective-permute-start | bytes 786440 | tf_op jit(solution)/shard_map/ppermute | solution.py:26
  23.1 8.8 %collective-permute-start.7 = (bf16[128,1024]{1,0:T(8,128)(2,1)S(1)}, bf16[128,1024]{1,0:T(8,128)(2,1)S(1)}, u32[]{:S(2)}, u32[]{:S(2)}) collective-permute-start(bf16[128,1024]{1,0:T(8,128)(2,1)S(1)} %collective-permute-done.6.refs_0_), channel_id=1, source_target_pairs={{0,1},{1,0},{2,3},{3,2},{4,5},{5,4},{6,7},{7,6},{8,9},{9,8},{10,11... | collective-permute-start | bytes 786440 | tf_op jit(solution)/shard_map/ppermute | solution.py:26
  24.1 12.8 %collective-permute-start.1 = (bf16[128,1024]{1,0:T(8,128)(2,1)S(1)}, bf16[128,1024]{1,0:T(8,128)(2,1)S(1)}, u32[]{:S(2)}, u32[]{:S(2)}) collective-permute-start(bf16[128,1024]{1,0:T(8,128)(2,1)S(1)} %collective-permute-done.refs_0_), channel_id=1, source_target_pairs={{0,1},{1,0},{2,3},{3,2},{4,5},{5,4},{6,7},{7,6},{8,9},{9,8},{10,11... | collective-permute-start | bytes 786440 | tf_op jit(solution)/shard_map/ppermute | solution.py:26
  27.8 6.6 %collective-permute-start.4 = (bf16[128,1024]{1,0:T(8,128)(2,1)S(1)}, bf16[128,1024]{1,0:T(8,128)(2,1)S(1)}, u32[]{:S(2)}, u32[]{:S(2)}) collective-permute-start(bf16[128,1024]{1,0:T(8,128)(2,1)S(1)} %collective-permute-done.3.refs_0_), channel_id=1, source_target_pairs={{0,1},{1,0},{2,3},{3,2},{4,5},{5,4},{6,7},{7,6},{8,9},{9,8},{10,11... | collective-permute-start | bytes 786440 | tf_op jit(solution)/shard_map/ppermute | solution.py:26
  36.9 23.4 %copy-start = (bf16[128]{0:T(256)(128)(2,1)S(1)}, bf16[128]{0:T(256)(128)(2,1)}, u32[]{:S(2)}) copy-start(bf16[128]{0:T(256)(128)(2,1)} %param.19) | copy-start | bytes 772
  39.2 4.7 %collective-permute-start.12 = (bf16[272,128]{1,0:T(8,128)(2,1)S(1)}, bf16[272,128]{1,0:T(8,128)(2,1)S(1)}, u32[]{:S(2)}, u32[]{:S(2)}) collective-permute-start(bf16[272,128]{1,0:T(8,128)(2,1)S(1)} %get-tuple-element.50), channel_id=1, source_target_pairs={{0,4},{4,0},{8,12},{12,8},{16,20},{20,16},{24,28},{28,24},{1,5},{5... | collective-permute-start | bytes 208904 | tf_op jit(solution)/shard_map/ppermute | solution.py:26
  41.0 4.5 %collective-permute-start.13 = (bf16[272,128]{1,0:T(8,128)(2,1)S(1)}, bf16[272,128]{1,0:T(8,128)(2,1)S(1)}, u32[]{:S(2)}, u32[]{:S(2)}) collective-permute-start(bf16[272,128]{1,0:T(8,128)(2,1)S(1)} %get-tuple-element.51), channel_id=1, source_target_pairs={{0,8},{4,12},{8,0},{12,4},{16,24},{20,28},{24,16},{28,20},{1,9},{5... | collective-permute-start | bytes 208904 | tf_op jit(solution)/shard_map/ppermute | solution.py:26
  42.6 5.2 %collective-permute-start.14 = (bf16[272,128]{1,0:T(8,128)(2,1)S(1)}, bf16[272,128]{1,0:T(8,128)(2,1)S(1)}, u32[]{:S(2)}, u32[]{:S(2)}) collective-permute-start(bf16[272,128]{1,0:T(8,128)(2,1)S(1)} %get-tuple-element.52), channel_id=1, source_target_pairs={{0,12},{4,8},{8,4},{12,0},{16,28},{20,24},{24,20},{28,16},{1,13},{... | collective-permute-start | bytes 208904 | tf_op jit(solution)/shard_map/ppermute | solution.py:26
  48.4 5.3 %collective-permute-start.15 = (bf16[144,128]{1,0:T(8,128)(2,1)S(1)}, bf16[144,128]{1,0:T(8,128)(2,1)S(1)}, u32[]{:S(2)}, u32[]{:S(2)}) collective-permute-start(bf16[144,128]{1,0:T(8,128)(2,1)S(1)} %get-tuple-element.55), channel_id=1, source_target_pairs={{0,16},{4,20},{8,24},{12,28},{16,0},{20,4},{24,8},{28,12},{1,17},{... | collective-permute-start | bytes 110600 | tf_op jit(solution)/shard_map/ppermute | solution.py:26
  54.1 3.7 %collective-permute-start.16 = (bf16[32,128]{1,0:T(8,128)(2,1)S(1)}, bf16[32,128]{1,0:T(8,128)(2,1)S(1)}, u32[]{:S(2)}, u32[]{:S(2)}) collective-permute-start(bf16[32,128]{1,0:T(8,128)(2,1)S(1)} %get-tuple-element.57), channel_id=1, source_target_pairs={{0,4},{4,0},{8,12},{12,8},{16,20},{20,16},{24,28},{28,24},{1,5},{5... | collective-permute-start | bytes 24584 | tf_op jit(solution)/shard_map/ppermute | solution.py:26
  54.3 3.7 %collective-permute-start.17 = (bf16[32,128]{1,0:T(8,128)(2,1)S(1)}, bf16[32,128]{1,0:T(8,128)(2,1)S(1)}, u32[]{:S(2)}, u32[]{:S(2)}) collective-permute-start(bf16[32,128]{1,0:T(8,128)(2,1)S(1)} %get-tuple-element.58), channel_id=1, source_target_pairs={{0,8},{4,12},{8,0},{12,4},{16,24},{20,28},{24,16},{28,20},{1,9},{5... | collective-permute-start | bytes 24584 | tf_op jit(solution)/shard_map/ppermute | solution.py:26
  55.8 4.5 %collective-permute-start.18 = (bf16[32,128]{1,0:T(8,128)(2,1)S(1)}, bf16[32,128]{1,0:T(8,128)(2,1)S(1)}, u32[]{:S(2)}, u32[]{:S(2)}) collective-permute-start(bf16[32,128]{1,0:T(8,128)(2,1)S(1)} %get-tuple-element.59), channel_id=1, source_target_pairs={{0,12},{4,8},{8,4},{12,0},{16,28},{20,24},{24,20},{28,16},{1,13},{... | collective-permute-start | bytes 24584 | tf_op jit(solution)/shard_map/ppermute | solution.py:26

commit v7 on v5

--- a/solution.py
+++ b/solution.py
@@ -169,7 +169,7 @@
         copy.wait()
 
 
-def chunk_kernel(heads, index, last, masks, prior, *refs):
+def chunk_kernel(heads, begin, last, masks, prior, *refs):
     pieces = len(masks)
     piece_refs = refs[:pieces]
     wk_ref, wv_ref, wg_ref, small_ref, forget_ref = refs[pieces : pieces + 5]
@@ -177,14 +177,14 @@
     sums = (None, None, None)
     if prior:
         sums, rest = tuple(ref[...] for ref in rest[:3]), rest[3:]
-    if index > 0:
+    if begin > 0:
         state_ref, rest = rest[0], rest[1:]
     if last:
         query_ref, rest = rest[0], rest[1:]
     gates, key_acc, value_acc = project(masks, piece_refs, wk_ref, wv_ref, wg_ref, sums)
     size = key_acc.shape[0]
     bias, rate = small_ref[:, 0:1], small_ref[:, 1:2]
-    forget = forget_ref[:, index * size : (index + 1) * size]
+    forget = forget_ref[:, begin : begin + size]
     beta_row = jax.nn.sigmoid(gates[0:SUB] + bias)
     log_row = forget - rate * jax.nn.softplus(gates[SUB : 2 * SUB])
     row = lax.broadcasted_iota(jnp.int32, (size, size), 0)
@@ -202,7 +202,7 @@
         ku = kw * lax.rsqrt(jnp.sum(kw * kw, axis=-1, keepdims=True) + norm_eps)
         keys.append(ku)
         lowers.append(jnp.where(strict, dot_nt(ku, ku), 0.0) * beta_row[h : h + 1, :])
-    if index > 0:
+    if begin > 0:
         states = [state_ref[h] for h in range(heads)]
     else:
         kr = lax.broadcasted_iota(jnp.int32, (DK, DV + DK), 0)
@@ -217,10 +217,11 @@
         turned.append(keys[h].T * beta_row[h : h + 1, :])
     fresh = []
     for h, inverse in enumerate(unit_inverses(lowers, size)):
-        left = jnp.concatenate(
-            [inverse * remain[h : h + 1, :], inverse * -keep[h : h + 1, :]], axis=1
-        )
-        fresh.append(dot(left, rights[h]))
+        ours, theirs = inverse * remain[h : h + 1, :], inverse * -keep[h : h + 1, :]
+        if size % DK == 0:
+            fresh.append(dot(jnp.concatenate([ours, theirs], axis=1), rights[h]))
+        else:
+            fresh.append(dot(ours, rights[h][:size]) + dot(theirs, rights[h][size:]))
     for h in range(heads):
         new = keep[h : h + 1, :] * states[h] + dot(turned[h], fresh[h])
         if last:
@@ -393,10 +394,14 @@
     rows = DK // count
     chunk = min(CHUNK, length)
     chunks = length // chunk
-
-    owns = [tokens[:chunk]]
+    moved_on = chunk // 4 if chunks > 1 and chunk % 64 == 0 else 0
+    sizes = [chunk] * chunks
+    sizes[0], sizes[-1] = sizes[0] + moved_on, sizes[-1] - moved_on
+    begins = [sum(sizes[:c]) for c in range(chunks)]
+
+    owns = [tokens[: sizes[0]]]
     later = lax.optimization_barrier(tokens)
-    owns += [later[c * chunk : (c + 1) * chunk] for c in range(1, chunks)]
+    owns += [later[b : b + size] for b, size in zip(begins[1:], sizes[1:])]
     gathered = []
     for c in range(chunks):
         found = [(0, owns[c])]
@@ -439,15 +444,15 @@
     state = None
     flops = 2 * chunk * width * ranks * (2 * heads * DK + DK) + heads * 24 * 2 * chunk * chunk * DK
     weights = [w_key, w_value, gate_weights]
-    sums_shape = [shape((2 * SUB, chunk)), shape((chunk, heads * DK)), shape((chunk, heads * DV))]
 
     def part(found, sums):
+        size = found[0][1].shape[0]
         return call(
             functools.partial(part_kernel, tuple(m for m, _ in found), len(sums) > 0),
             [x for _, x in found] + weights + sums,
-            sums_shape,
+            [shape((2 * SUB, size)), shape((size, heads * DK)), shape((size, heads * DV))],
             mib=16,
-            flops=2 * chunk * width * len(found) * (2 * heads * DK + DK),
+            flops=2 * size * width * len(found) * (2 * heads * DK + DK),
         )
 
     for c in range(chunks):
@@ -471,7 +476,7 @@
             outs = [shape((DK + DV + 2 * SUB, DK), bf16)] * heads
         result = call(
             functools.partial(
-                chunk_kernel, heads, c, last, tuple(m for m, _ in found), len(sums) > 0
+                chunk_kernel, heads, begins[c], last, tuple(m for m, _ in found), len(sums) > 0
             ),
             arrays,
             outs,

time: 61.2 us -> 62.2 us (1.016)
  Pallas kernels: 19.1 us -> 20.1 us
  local copies, waits for them, and re-layouts: 2.13 us -> 3.01 us
  waiting for transfers between devices: 20.9 us -> 20.1 us
    pallas_call x11, Pallas kernels: 15.3 us -> 16.2 us  [call(): pl.pallas_call(body, out_shape=outs, in_specs=[vmem] * len(arrays), out_s...]
    slice x2 -> x3, local copies, waits for them, and re-layouts: 2.13 us -> 3 us  [the longest x2 2.01 us: per_device(): owns += [later[b:b + size] for b, size in zip(begins[1:], sizes[1:])]]
    ppermute x19, waiting for transfers between devices: 20.9 us -> 20.1 us  [swap(): return lax.ppermute(x, axis, flip(axis, mask))]
  transfers between devices with their start and end apart: 19 -> 19, of which waited for: 11 -> 10; matrix products, arithmetic and copies ran while one was open for 2% -> 3% of each run, Pallas kernels for 25% -> 26%
where the time goes in v7:
time: 62.2 us; the launch traced here: 62 us
  waiting for transfers between devices  20.1 us (32%)
  Pallas kernels  20.1 us (32%)
  starting transfers between devices  18.1 us (29%)
  local copies, waits for them, and re-layouts  3.01 us (5%)
  between operations  0.77 us (1%)
    ppermute x19, waiting for transfers between devices, swap(): return lax.ppermute(x, axis, flip(axis, mask))  20.1 us
    ppermute x19, starting transfers between devices, swap(): return lax.ppermute(x, axis, flip(axis, mask))  18.1 us
    pallas_call x11, Pallas kernels, call(): pl.pallas_call(body, out_shape=outs, in_specs=[vmem] * len(arrays), out_s...  16.2 us
    pallas_call x1, Pallas kernels, per_device(): pl.pallas_call(functools.partial(prepare_kernel, heads), out_shape=[shape...  3.84 us
    slice x2, local copies, waits for them, and re-layouts, per_device(): owns += [later[b:b + size] for b, size in zip(begins[1:], sizes[1:])]  2.01 us
  transfers between devices with their start and end apart: 19, of which 10 were waited for; matrix products, arithmetic and copies ran while one was open for 3% of the time, Pallas kernels for 26%

profile of v7, /device:TPU:0, one launch (start us, length us, event | category | flops | bytes accessed | tf_op | source)
XLA Modules:
  0.0 62.0 jit_solution(14128218587839325002)
XLA Ops:
  0.6 1.0 %slice.15.refs_0_ = bf16[160,1024]{1,0:T(8,128)(2,1)S(1)} slice(bf16[512,1024]{1,0:T(8,128)(2,1)} %param.10), slice={[0:160], [0:1024]} | slice | bytes 655360 | tf_op jit(solution)/shard_map/slice | solution.py:402
  1.6 3.1 %collective-permute-start.9 = (bf16[160,1024]{1,0:T(8,128)(2,1)S(1)}, bf16[160,1024]{1,0:T(8,128)(2,1)S(1)}, u32[]{:S(2)}, u32[]{:S(2)}) collective-permute-start(bf16[160,1024]{1,0:T(8,128)(2,1)S(1)} %slice.15.refs_0_), channel_id=1, source_target_pairs={{0,2},{1,3},{2,0},{3,1},{4,6},{5,7},{6,4},{7,5},{8,10},{9,11},{10,... | collective-permute-start | bytes 983048 | tf_op jit(solution)/shard_map/ppermute | solution.py:26
  4.7 1.1 %fusion = (bf16[128,1024]{1,0:T(8,128)(2,1)S(1)}, bf16[128,1024]{1,0:T(8,128)(2,1)S(1)}) fusion(bf16[512,1024]{1,0:T(8,128)(2,1)} %param.10), kind=kLoop, calls=%fused_computation | loop fusion | bytes 1048576 | tf_op jit(solution)/shard_map/slice | solution.py:404
  5.8 0.9 %slice.16.refs_0_ = bf16[96,1024]{1,0:T(8,128)(2,1)S(1)} slice(bf16[512,1024]{1,0:T(8,128)(2,1)} %param.10), slice={[416:512], [0:1024]} | slice | bytes 393216 | tf_op jit(solution)/shard_map/slice | solution.py:404
  7.4 2.0 %collective-permute-start.6 = (bf16[128,1024]{1,0:T(8,128)(2,1)S(1)}, bf16[128,1024]{1,0:T(8,128)(2,1)S(1)}, u32[]{:S(2)}, u32[]{:S(2)}) collective-permute-start(bf16[128,1024]{1,0:T(8,128)(2,1)S(1)} %get-tuple-element.60.refs_0_), channel_id=1, source_target_pairs={{0,2},{1,3},{2,0},{3,1},{4,6},{5,7},{6,4},{7,5},{8,10},{9,11},{10,... | collective-permute-start | bytes 786440 | tf_op jit(solution)/shard_map/ppermute | solution.py:26
  9.4 3.9 %collective-permute-done.9.refs_1_ = bf16[160,1024]{1,0:T(8,128)(2,1)S(1)} collective-permute-done((bf16[160,1024]{1,0:T(8,128)(2,1)S(1)}, bf16[160,1024]{1,0:T(8,128)(2,1)S(1)}, u32[]{:S(2)}, u32[]{:S(2)}) %collective-permute-start.9) | collective-permute-done | bytes 327712 | tf_op jit(solution)/shard_map/ppermute | solution.py:26
  13.3 4.2 %collective-permute-done.refs_0_ = bf16[96,1024]{1,0:T(8,128)(2,1)S(1)} collective-permute-done((bf16[96,1024]{1,0:T(8,128)(2,1)S(1)}, bf16[96,1024]{1,0:T(8,128)(2,1)S(1)}, u32[]{:S(2)}, u32[]{:S(2)}) %collective-permute-start) | collective-permute-done | bytes 196640 | tf_op jit(solution)/shard_map/ppermute | solution.py:26
  17.5 2.0 %collective-permute-start.3 = (bf16[128,1024]{1,0:T(8,128)(2,1)S(1)}, bf16[128,1024]{1,0:T(8,128)(2,1)S(1)}, u32[]{:S(2)}, u32[]{:S(2)}) collective-permute-start(bf16[128,1024]{1,0:T(8,128)(2,1)S(1)} %get-tuple-element.61.refs_0_), channel_id=1, source_target_pairs={{0,2},{1,3},{2,0},{3,1},{4,6},{5,7},{6,4},{7,5},{8,10},{9,11},{10,... | collective-permute-start | bytes 786440 | tf_op jit(solution)/shard_map/ppermute | solution.py:26
  19.5 3.8 %shard_map.113 = (bf16[4096,512]{1,0:T(8,128)(2,1)S(1)}, bf16[4096,512]{1,0:T(8,128)(2,1)S(1)}, bf16[16,4096]{1,0:T(8,128)(2,1)S(1)}, f32[8,128]{1,0:T(8,128)S(1...) custom-call(bf16[4096,512]{1,0:T(8,128)(2,1)} %refs_0_.1, bf16[4096,512]{1,0:T(8,128)(2,1)} %refs_1_.1, ...), custom_call_target="tpu_custom_call" | custom-call | tf_op jit(solution)/shard_map/pallas_call | solution.py:427
  26.3 1.6 %collective-permute-done.3.refs_0_ = bf16[128,1024]{1,0:T(8,128)(2,1)S(1)} collective-permute-done((bf16[128,1024]{1,0:T(8,128)(2,1)S(1)}, bf16[128,1024]{1,0:T(8,128)(2,1)S(1)}, u32[]{:S(2)}, u32[]{:S(2)}) %collective-permute-start.3) | collective-permute-done | bytes 262176 | tf_op jit(solution)/shard_map/ppermute | solution.py:26
  28.7 4.2 %shard_map.118.refs_10_ = f32[4,128,256]{2,1,0:T(8,128)S(1)} custom-call(bf16[160,1024]{1,0:T(8,128)(2,1)S(1)} %slice.15.refs_0_, bf16[160,1024]{1,0:T(8,128)(2,1)S(1)} %collective-permute-done.9.refs_1_, bf16[160,1024]{1,0:T(8,128)(2,1)S(1)} %collective-permute-done.10.refs_2_, bf16[160,1024]{1,0:T(8,128)(2,1)S(1)} %collective-permute-done.11.refs_3_, ...), custom_call_target="tpu_custom_call" | custom-call | flops 1610612736 | tf_op jit(solution)/shard_map/pallas_call | solution.py:364
  32.9 2.5 %shard_map.119.refs_10_ = f32[4,128,256]{2,1,0:T(8,128)S(1)} custom-call(bf16[128,1024]{1,0:T(8,128)(2,1)S(1)} %collective-permute-done.6.refs_0_, bf16[128,1024]{1,0:T(8,128)(2,1)S(1)} %collective-permute-done.7.refs_1_, bf16[4096,512]{1,0:T(8,128)(2,1)S(1)} %get-tuple-element.31.refs_2_.refs_1_.refs_4_, ...), custom_call_target="tpu_custom_call" | custom-call | flops 1610612736 | tf_op jit(solution)/shard_map/pallas_call | solution.py:364
  35.5 2.5 %shard_map.120.refs_9_ = f32[4,128,256]{2,1,0:T(8,128)S(1)} custom-call(bf16[128,1024]{1,0:T(8,128)(2,1)S(1)} %collective-permute-done.3.refs_0_, bf16[128,1024]{1,0:T(8,128)(2,1)S(1)} %collective-permute-done.4.refs_1_, bf16[4096,512]{1,0:T(8,128)(2,1)S(1)} %get-tuple-element.31.refs_2_.refs_1_.refs_4_, ...), custom_call_target="tpu_custom_call" | custom-call | flops 1610612736 | tf_op jit(solution)/shard_map/pallas_call | solution.py:364
  38.0 2.2 %shard_map.121 = (bf16[272,128]{1,0:T(8,128)(2,1)S(1)}, bf16[272,128]{1,0:T(8,128)(2,1)S(1)}, bf16[272,128]{1,0:T(8,128)(2,1)S(1)}, bf16[272,128]{1,0:T(8,128)(2,1)S(1)}) custom-call(bf16[96,1024]{1,0:T(8,128)(2,1)S(1)} %collective-permute-done.1.refs_0_, bf16[4096,512]{1,0:T(8,128)(2,1)S(1)} %get-tuple-element.31.refs_2_.refs_1_.refs_4_, ...), custom_call_target="tpu_custom_call" | custom-call | flops 1610612736 | tf_op jit(solution)/shard_map/pallas_call | solution.py:364
  40.2 1.8 %collective-permute-start.12 = (bf16[272,128]{1,0:T(8,128)(2,1)S(1)}, bf16[272,128]{1,0:T(8,128)(2,1)S(1)}, u32[]{:S(2)}, u32[]{:S(2)}) collective-permute-start(bf16[272,128]{1,0:T(8,128)(2,1)S(1)} %get-tuple-element.50), channel_id=1, source_target_pairs={{0,4},{4,0},{8,12},{12,8},{16,20},{20,16},{24,28},{28,24},{1,5},{5... | collective-permute-start | bytes 208904 | tf_op jit(solution)/shard_map/ppermute | solution.py:26
  42.0 1.5 %collective-permute-start.13 = (bf16[272,128]{1,0:T(8,128)(2,1)S(1)}, bf16[272,128]{1,0:T(8,128)(2,1)S(1)}, u32[]{:S(2)}, u32[]{:S(2)}) collective-permute-start(bf16[272,128]{1,0:T(8,128)(2,1)S(1)} %get-tuple-element.51), channel_id=1, source_target_pairs={{0,8},{4,12},{8,0},{12,4},{16,24},{20,28},{24,16},{28,20},{1,9},{5... | collective-permute-start | bytes 208904 | tf_op jit(solution)/shard_map/ppermute | solution.py:26
  43.7 1.1 %collective-permute-done.12.refs_1_ = bf16[272,128]{1,0:T(8,128)(2,1)S(1)} collective-permute-done((bf16[272,128]{1,0:T(8,128)(2,1)S(1)}, bf16[272,128]{1,0:T(8,128)(2,1)S(1)}, u32[]{:S(2)}, u32[]{:S(2)}) %collective-permute-start.12) | collective-permute-done | bytes 69664 | tf_op jit(solution)/shard_map/ppermute | solution.py:26
  44.8 1.7 %collective-permute-done.13.refs_2_ = bf16[272,128]{1,0:T(8,128)(2,1)S(1)} collective-permute-done((bf16[272,128]{1,0:T(8,128)(2,1)S(1)}, bf16[272,128]{1,0:T(8,128)(2,1)S(1)}, u32[]{:S(2)}, u32[]{:S(2)}) %collective-permute-start.13) | collective-permute-done | bytes 69664 | tf_op jit(solution)/shard_map/ppermute | solution.py:26
  46.5 2.2 %collective-permute-done.14.refs_3_ = bf16[272,128]{1,0:T(8,128)(2,1)S(1)} collective-permute-done((bf16[272,128]{1,0:T(8,128)(2,1)S(1)}, bf16[272,128]{1,0:T(8,128)(2,1)S(1)}, u32[]{:S(2)}, u32[]{:S(2)}) %collective-permute-start.14) | collective-permute-done | bytes 69664 | tf_op jit(solution)/shard_map/ppermute | solution.py:26
  49.3 2.6 %collective-permute-start.15 = (bf16[144,128]{1,0:T(8,128)(2,1)S(1)}, bf16[144,128]{1,0:T(8,128)(2,1)S(1)}, u32[]{:S(2)}, u32[]{:S(2)}) collective-permute-start(bf16[144,128]{1,0:T(8,128)(2,1)S(1)} %get-tuple-element.55), channel_id=1, source_target_pairs={{0,16},{4,20},{8,24},{12,28},{16,0},{20,4},{24,8},{28,12},{1,17},{... | collective-permute-start | bytes 110600 | tf_op jit(solution)/shard_map/ppermute | solution.py:26
  51.9 2.7 %collective-permute-done.15.refs_0_ = bf16[144,128]{1,0:T(8,128)(2,1)S(1)} collective-permute-done((bf16[144,128]{1,0:T(8,128)(2,1)S(1)}, bf16[144,128]{1,0:T(8,128)(2,1)S(1)}, u32[]{:S(2)}, u32[]{:S(2)}) %collective-permute-start.15) | collective-permute-done | bytes 36896 | tf_op jit(solution)/shard_map/ppermute | solution.py:26
  55.2 1.5 %collective-permute-start.17 = (bf16[32,128]{1,0:T(8,128)(2,1)S(1)}, bf16[32,128]{1,0:T(8,128)(2,1)S(1)}, u32[]{:S(2)}, u32[]{:S(2)}) collective-permute-start(bf16[32,128]{1,0:T(8,128)(2,1)S(1)} %get-tuple-element.58), channel_id=1, source_target_pairs={{0,8},{4,12},{8,0},{12,4},{16,24},{20,28},{24,16},{28,20},{1,9},{5... | collective-permute-start | bytes 24584 | tf_op jit(solution)/shard_map/ppermute | solution.py:26
  56.7 1.8 %collective-permute-start.18 = (bf16[32,128]{1,0:T(8,128)(2,1)S(1)}, bf16[32,128]{1,0:T(8,128)(2,1)S(1)}, u32[]{:S(2)}, u32[]{:S(2)}) collective-permute-start(bf16[32,128]{1,0:T(8,128)(2,1)S(1)} %get-tuple-element.59), channel_id=1, source_target_pairs={{0,12},{4,8},{8,4},{12,0},{16,28},{20,24},{24,20},{28,16},{1,13},{... | collective-permute-start | bytes 24584 | tf_op jit(solution)/shard_map/ppermute | solution.py:26
  58.8 2.4 %collective-permute-done.18.refs_3_ = bf16[32,128]{1,0:T(8,128)(2,1)S(1)} collective-permute-done((bf16[32,128]{1,0:T(8,128)(2,1)S(1)}, bf16[32,128]{1,0:T(8,128)(2,1)S(1)}, u32[]{:S(2)}, u32[]{:S(2)}) %collective-permute-start.18) | collective-permute-done | bytes 8224 | tf_op jit(solution)/shard_map/ppermute | solution.py:26
  (31 shorter events, 6.8 us)
Async XLA Ops:
  1.6 11.6 %collective-permute-start.9 = (bf16[160,1024]{1,0:T(8,128)(2,1)S(1)}, bf16[160,1024]{1,0:T(8,128)(2,1)S(1)}, u32[]{:S(2)}, u32[]{:S(2)}) collective-permute-start(bf16[160,1024]{1,0:T(8,128)(2,1)S(1)} %slice.15.refs_0_), channel_id=1, source_target_pairs={{0,2},{1,3},{2,0},{3,1},{4,6},{5,7},{6,4},{7,5},{8,10},{9,11},{10,... | collective-permute-start | bytes 983048 | tf_op jit(solution)/shard_map/ppermute | solution.py:26
  5.8 11.7 %collective-permute-start.8 = (bf16[128,1024]{1,0:T(8,128)(2,1)S(1)}, bf16[128,1024]{1,0:T(8,128)(2,1)S(1)}, u32[]{:S(2)}, u32[]{:S(2)}) collective-permute-start(bf16[128,1024]{1,0:T(8,128)(2,1)S(1)} %get-tuple-element.60.refs_0_), channel_id=1, source_target_pairs={{0,1},{1,0},{2,3},{3,2},{4,5},{5,4},{6,7},{7,6},{8,9},{9,8},{10,11... | collective-permute-start | bytes 786440 | tf_op jit(solution)/shard_map/ppermute | solution.py:26
  6.8 2.6 %collective-permute-start.2 = (bf16[96,1024]{1,0:T(8,128)(2,1)S(1)}, bf16[96,1024]{1,0:T(8,128)(2,1)S(1)}, u32[]{:S(2)}, u32[]{:S(2)}) collective-permute-start(bf16[96,1024]{1,0:T(8,128)(2,1)S(1)} %slice.16.refs_0_), channel_id=1, source_target_pairs={{0,1},{1,0},{2,3},{3,2},{4,5},{5,4},{6,7},{7,6},{8,9},{9,8},{10,11... | collective-permute-start | bytes 589832 | tf_op jit(solution)/shard_map/ppermute | solution.py:26
  7.3 10.1 %collective-permute-start = (bf16[96,1024]{1,0:T(8,128)(2,1)S(1)}, bf16[96,1024]{1,0:T(8,128)(2,1)S(1)}, u32[]{:S(2)}, u32[]{:S(2)}) collective-permute-start(bf16[96,1024]{1,0:T(8,128)(2,1)S(1)} %slice.16.refs_0_), channel_id=1, source_target_pairs={{0,2},{1,3},{2,0},{3,1},{4,6},{5,7},{6,4},{7,5},{8,10},{9,11},{10,... | collective-permute-start | bytes 589832 | tf_op jit(solution)/shard_map/ppermute | solution.py:26
  7.4 17.4 %collective-permute-start.6 = (bf16[128,1024]{1,0:T(8,128)(2,1)S(1)}, bf16[128,1024]{1,0:T(8,128)(2,1)S(1)}, u32[]{:S(2)}, u32[]{:S(2)}) collective-permute-start(bf16[128,1024]{1,0:T(8,128)(2,1)S(1)} %get-tuple-element.60.refs_0_), channel_id=1, source_target_pairs={{0,2},{1,3},{2,0},{3,1},{4,6},{5,7},{6,4},{7,5},{8,10},{9,11},{10,... | collective-permute-start | bytes 786440 | tf_op jit(solution)/shard_map/ppermute | solution.py:26
  9.4 19.3 %collective-permute-start.10 = (bf16[160,1024]{1,0:T(8,128)(2,1)S(1)}, bf16[160,1024]{1,0:T(8,128)(2,1)S(1)}, u32[]{:S(2)}, u32[]{:S(2)}) collective-permute-start(bf16[160,1024]{1,0:T(8,128)(2,1)S(1)} %slice.15.refs_0_), channel_id=1, source_target_pairs={{0,1},{1,0},{2,3},{3,2},{4,5},{5,4},{6,7},{7,6},{8,9},{9,8},{10,11... | collective-permute-start | bytes 983048 | tf_op jit(solution)/shard_map/ppermute | solution.py:26
  13.2 15.5 %collective-permute-start.11 = (bf16[160,1024]{1,0:T(8,128)(2,1)S(1)}, bf16[160,1024]{1,0:T(8,128)(2,1)S(1)}, u32[]{:S(2)}, u32[]{:S(2)}) collective-permute-start(bf16[160,1024]{1,0:T(8,128)(2,1)S(1)} %collective-permute-done.9.refs_1_), channel_id=1, source_target_pairs={{0,1},{1,0},{2,3},{3,2},{4,5},{5,4},{6,7},{7,6},{8,9},{9,8},{10,11... | collective-permute-start | bytes 983048 | tf_op jit(solution)/shard_map/ppermute | solution.py:26
  17.5 8.5 %collective-permute-start.5 = (bf16[128,1024]{1,0:T(8,128)(2,1)S(1)}, bf16[128,1024]{1,0:T(8,128)(2,1)S(1)}, u32[]{:S(2)}, u32[]{:S(2)}) collective-permute-start(bf16[128,1024]{1,0:T(8,128)(2,1)S(1)} %get-tuple-element.61.refs_0_), channel_id=1, source_target_pairs={{0,1},{1,0},{2,3},{3,2},{4,5},{5,4},{6,7},{7,6},{8,9},{9,8},{10,11... | collective-permute-start | bytes 786440 | tf_op jit(solution)/shard_map/ppermute | solution.py:26
  17.5 10.4 %collective-permute-start.3 = (bf16[128,1024]{1,0:T(8,128)(2,1)S(1)}, bf16[128,1024]{1,0:T(8,128)(2,1)S(1)}, u32[]{:S(2)}, u32[]{:S(2)}) collective-permute-start(bf16[128,1024]{1,0:T(8,128)(2,1)S(1)} %get-tuple-element.61.refs_0_), channel_id=1, source_target_pairs={{0,2},{1,3},{2,0},{3,1},{4,6},{5,7},{6,4},{7,5},{8,10},{9,11},{10,... | collective-permute-start | bytes 786440 | tf_op jit(solution)/shard_map/ppermute | solution.py:26
  24.8 8.1 %collective-permute-start.7 = (bf16[128,1024]{1,0:T(8,128)(2,1)S(1)}, bf16[128,1024]{1,0:T(8,128)(2,1)S(1)}, u32[]{:S(2)}, u32[]{:S(2)}) collective-permute-start(bf16[128,1024]{1,0:T(8,128)(2,1)S(1)} %collective-permute-done.6.refs_0_), channel_id=1, source_target_pairs={{0,1},{1,0},{2,3},{3,2},{4,5},{5,4},{6,7},{7,6},{8,9},{9,8},{10,11... | collective-permute-start | bytes 786440 | tf_op jit(solution)/shard_map/ppermute | solution.py:26
  25.9 12.1 %collective-permute-start.1 = (bf16[96,1024]{1,0:T(8,128)(2,1)S(1)}, bf16[96,1024]{1,0:T(8,128)(2,1)S(1)}, u32[]{:S(2)}, u32[]{:S(2)}) collective-permute-start(bf16[96,1024]{1,0:T(8,128)(2,1)S(1)} %collective-permute-done.refs_0_), channel_id=1, source_target_pairs={{0,1},{1,0},{2,3},{3,2},{4,5},{5,4},{6,7},{7,6},{8,9},{9,8},{10,11... | collective-permute-start | bytes 589832 | tf_op jit(solution)/shard_map/ppermute | solution.py:26
  27.8 7.6 %collective-permute-start.4 = (bf16[128,1024]{1,0:T(8,128)(2,1)S(1)}, bf16[128,1024]{1,0:T(8,128)(2,1)S(1)}, u32[]{:S(2)}, u32[]{:S(2)}) collective-permute-start(bf16[128,1024]{1,0:T(8,128)(2,1)S(1)} %collective-permute-done.3.refs_0_), channel_id=1, source_target_pairs={{0,1},{1,0},{2,3},{3,2},{4,5},{5,4},{6,7},{7,6},{8,9},{9,8},{10,11... | collective-permute-start | bytes 786440 | tf_op jit(solution)/shard_map/ppermute | solution.py:26
  38.0 23.3 %copy-start = (bf16[128]{0:T(256)(128)(2,1)S(1)}, bf16[128]{0:T(256)(128)(2,1)}, u32[]{:S(2)}) copy-start(bf16[128]{0:T(256)(128)(2,1)} %param.19) | copy-start | bytes 772
  40.2 4.6 %collective-permute-start.12 = (bf16[272,128]{1,0:T(8,128)(2,1)S(1)}, bf16[272,128]{1,0:T(8,128)(2,1)S(1)}, u32[]{:S(2)}, u32[]{:S(2)}) collective-permute-start(bf16[272,128]{1,0:T(8,128)(2,1)S(1)} %get-tuple-element.50), channel_id=1, source_target_pairs={{0,4},{4,0},{8,12},{12,8},{16,20},{20,16},{24,28},{28,24},{1,5},{5... | collective-permute-start | bytes 208904 | tf_op jit(solution)/shard_map/ppermute | solution.py:26
  42.0 4.6 %collective-permute-start.13 = (bf16[272,128]{1,0:T(8,128)(2,1)S(1)}, bf16[272,128]{1,0:T(8,128)(2,1)S(1)}, u32[]{:S(2)}, u32[]{:S(2)}) collective-permute-start(bf16[272,128]{1,0:T(8,128)(2,1)S(1)} %get-tuple-element.51), channel_id=1, source_target_pairs={{0,8},{4,12},{8,0},{12,4},{16,24},{20,28},{24,16},{28,20},{1,9},{5... | collective-permute-start | bytes 208904 | tf_op jit(solution)/shard_map/ppermute | solution.py:26
  43.5 5.2 %collective-permute-start.14 = (bf16[272,128]{1,0:T(8,128)(2,1)S(1)}, bf16[272,128]{1,0:T(8,128)(2,1)S(1)}, u32[]{:S(2)}, u32[]{:S(2)}) collective-permute-start(bf16[272,128]{1,0:T(8,128)(2,1)S(1)} %get-tuple-element.52), channel_id=1, source_target_pairs={{0,12},{4,8},{8,4},{12,0},{16,28},{20,24},{24,20},{28,16},{1,13},{... | collective-permute-start | bytes 208904 | tf_op jit(solution)/shard_map/ppermute | solution.py:26
  49.3 5.3 %collective-permute-start.15 = (bf16[144,128]{1,0:T(8,128)(2,1)S(1)}, bf16[144,128]{1,0:T(8,128)(2,1)S(1)}, u32[]{:S(2)}, u32[]{:S(2)}) collective-permute-start(bf16[144,128]{1,0:T(8,128)(2,1)S(1)} %get-tuple-element.55), channel_id=1, source_target_pairs={{0,16},{4,20},{8,24},{12,28},{16,0},{20,4},{24,8},{28,12},{1,17},{... | collective-permute-start | bytes 110600 | tf_op jit(solution)/shard_map/ppermute | solution.py:26
  55.0 3.7 %collective-permute-start.16 = (bf16[32,128]{1,0:T(8,128)(2,1)S(1)}, bf16[32,128]{1,0:T(8,128)(2,1)S(1)}, u32[]{:S(2)}, u32[]{:S(2)}) collective-permute-start(bf16[32,128]{1,0:T(8,128)(2,1)S(1)} %get-tuple-element.57), channel_id=1, source_target_pairs={{0,4},{4,0},{8,12},{12,8},{16,20},{20,16},{24,28},{28,24},{1,5},{5... | collective-permute-start | bytes 24584 | tf_op jit(solution)/shard_map/ppermute | solution.py:26
  55.2 3.7 %collective-permute-start.17 = (bf16[32,128]{1,0:T(8,128)(2,1)S(1)}, bf16[32,128]{1,0:T(8,128)(2,1)S(1)}, u32[]{:S(2)}, u32[]{:S(2)}) collective-permute-start(bf16[32,128]{1,0:T(8,128)(2,1)S(1)} %get-tuple-element.58), channel_id=1, source_target_pairs={{0,8},{4,12},{8,0},{12,4},{16,24},{20,28},{24,16},{28,20},{1,9},{5... | collective-permute-start | bytes 24584 | tf_op jit(solution)/shard_map/ppermute | solution.py:26
  56.7 4.5 %collective-permute-start.18 = (bf16[32,128]{1,0:T(8,128)(2,1)S(1)}, bf16[32,128]{1,0:T(8,128)(2,1)S(1)}, u32[]{:S(2)}, u32[]{:S(2)}) collective-permute-start(bf16[32,128]{1,0:T(8,128)(2,1)S(1)} %get-tuple-element.59), channel_id=1, source_target_pairs={{0,12},{4,8},{8,4},{12,0},{16,28},{20,24},{24,20},{28,16},{1,13},{... | collective-permute-start | bytes 24584 | tf_op jit(solution)/shard_map/ppermute | solution.py:26

commit v8 on v5

--- a/solution.py
+++ b/solution.py
@@ -38,7 +38,8 @@
 def dot3(left, right):
     lh, ll = split(left)
     rh, rl = split(right)
-    return dot(lh, rh) + (dot(lh, rl) + dot(ll, rh))
+    whole = dot(jnp.concatenate([lh, ll], axis=1), jnp.concatenate([rh, rh], axis=0))
+    return whole + dot(lh, rl)
 
 
 def dot_ones(left, ones):
@@ -64,22 +65,26 @@
     near = (row // width) == (col // width)
     inner = [jnp.where(near, low, 0.0) for low in lowers]
     results = [jnp.where(row == col, 1.0, 0.0) - low for low in inner]
-    powers = inner
-    covered = 2
-    while covered < width:
-        powers = [dot(p, p) for p in powers]
-        results = [r + dot(r, p) for r, p in zip(results, powers)]
-        covered *= 2
+    if width > 2:
+        results = series([dot(low, low) for low in inner], results, width, size)
     if width == size:
         return results
     powers = [dot(r, jnp.where(near, 0.0, low)) for r, low in zip(results, lowers)]
-    results = [r - dot(p, r) for r, p in zip(results, powers)]
+    if size // width == 2:
+        return [r - dot(p, r) for r, p in zip(results, powers)]
+    both = [dot(p, jnp.concatenate([p, r], axis=1)) for r, p in zip(results, powers)]
+    results = [r - x[:, size:] for r, x in zip(results, both)]
+    return series([x[:, :size] for x in both], results, size // width, size)
+
+
+def series(powers, results, reach, size):
     covered = 2
-    while covered * width < size:
-        powers = [dot(p, p) for p in powers]
-        results = [r + dot(p, r) for r, p in zip(results, powers)]
+    while 2 * covered < reach:
+        both = [dot(p, jnp.concatenate([p, r], axis=1)) for r, p in zip(results, powers)]
+        results = [r + x[:, size:] for r, x in zip(results, both)]
+        powers = [x[:, :size] for x in both]
         covered *= 2
-    return results
+    return [r + dot(p, r) for r, p in zip(results, powers)]
 
 
 def project(masks, piece_refs, wk_ref, wv_ref, wg_ref, sums):

time: 61.2 us -> 60.9 us (level)
  no operation moved by 1% of the time
where the time goes in v8:
time: 60.9 us; the launch traced here: 60.7 us
  waiting for transfers between devices  20.9 us (34%)
  Pallas kernels  18.7 us (31%)
  starting transfers between devices  18.2 us (30%)
  local copies, waits for them, and re-layouts  2.13 us (3%)
  between operations  0.78 us (1%)
    ppermute x19, waiting for transfers between devices, swap(): return lax.ppermute(x, axis, flip(axis, mask))  20.9 us
    ppermute x19, starting transfers between devices, swap(): return lax.ppermute(x, axis, flip(axis, mask))  18.2 us
    pallas_call x11, Pallas kernels, call(): pl.pallas_call(body, out_shape=outs, in_specs=[vmem] * len(arrays), out_s...  14.9 us
    pallas_call x1, Pallas kernels, per_device(): pl.pallas_call(functools.partial(prepare_kernel, heads), out_shape=[shape...  3.84 us
  transfers between devices with their start and end apart: 19, of which 11 were waited for; matrix products, arithmetic and copies ran while one was open for 2% of the time, Pallas kernels for 25%

profile of v8, /device:TPU:0, one launch (start us, length us, event | category | flops | bytes accessed | tf_op | source)
XLA Modules:
  0.0 60.7 jit_solution(14381468740449223053)
XLA Ops:
  0.6 1.0 %slice.15.refs_0_ = bf16[128,1024]{1,0:T(8,128)(2,1)S(1)} slice(bf16[512,1024]{1,0:T(8,128)(2,1)} %param.10), slice={[0:128], [0:1024]} | slice | bytes 524288 | tf_op jit(solution)/shard_map/slice | solution.py:402
  1.6 3.1 %collective-permute-start.9 = (bf16[128,1024]{1,0:T(8,128)(2,1)S(1)}, bf16[128,1024]{1,0:T(8,128)(2,1)S(1)}, u32[]{:S(2)}, u32[]{:S(2)}) collective-permute-start(bf16[128,1024]{1,0:T(8,128)(2,1)S(1)} %slice.15.refs_0_), channel_id=1, source_target_pairs={{0,2},{1,3},{2,0},{3,1},{4,6},{5,7},{6,4},{7,5},{8,10},{9,11},{10,... | collective-permute-start | bytes 786440 | tf_op jit(solution)/shard_map/ppermute | solution.py:26
  4.7 1.2 %fusion = (bf16[128,1024]{1,0:T(8,128)(2,1)S(1)}, bf16[128,1024]{1,0:T(8,128)(2,1)S(1)}, bf16[128,1024]{1,0:T(8,128)(2,1)S(1)}) fusion(bf16[512,1024]{1,0:T(8,128)(2,1)} %param.10), kind=kLoop, calls=%fused_computation | loop fusion | bytes 1572864 | tf_op jit(solution)/shard_map/slice | solution.py:404
  6.4 2.0 %collective-permute-start.6 = (bf16[128,1024]{1,0:T(8,128)(2,1)S(1)}, bf16[128,1024]{1,0:T(8,128)(2,1)S(1)}, u32[]{:S(2)}, u32[]{:S(2)}) collective-permute-start(bf16[128,1024]{1,0:T(8,128)(2,1)S(1)} %get-tuple-element.60.refs_0_), channel_id=1, source_target_pairs={{0,2},{1,3},{2,0},{3,1},{4,6},{5,7},{6,4},{7,5},{8,10},{9,11},{10,... | collective-permute-start | bytes 786440 | tf_op jit(solution)/shard_map/ppermute | solution.py:26
  8.4 3.4 %collective-permute-done.9.refs_1_ = bf16[128,1024]{1,0:T(8,128)(2,1)S(1)} collective-permute-done((bf16[128,1024]{1,0:T(8,128)(2,1)S(1)}, bf16[128,1024]{1,0:T(8,128)(2,1)S(1)}, u32[]{:S(2)}, u32[]{:S(2)}) %collective-permute-start.9) | collective-permute-done | bytes 262176 | tf_op jit(solution)/shard_map/ppermute | solution.py:26
  11.8 2.0 %collective-permute-start.3 = (bf16[128,1024]{1,0:T(8,128)(2,1)S(1)}, bf16[128,1024]{1,0:T(8,128)(2,1)S(1)}, u32[]{:S(2)}, u32[]{:S(2)}) collective-permute-start(bf16[128,1024]{1,0:T(8,128)(2,1)S(1)} %get-tuple-element.61.refs_0_), channel_id=1, source_target_pairs={{0,2},{1,3},{2,0},{3,1},{4,6},{5,7},{6,4},{7,5},{8,10},{9,11},{10,... | collective-permute-start | bytes 786440 | tf_op jit(solution)/shard_map/ppermute | solution.py:26
  14.1 3.4 %collective-permute-done.refs_0_ = bf16[128,1024]{1,0:T(8,128)(2,1)S(1)} collective-permute-done((bf16[128,1024]{1,0:T(8,128)(2,1)S(1)}, bf16[128,1024]{1,0:T(8,128)(2,1)S(1)}, u32[]{:S(2)}, u32[]{:S(2)}) %collective-permute-start) | collective-permute-done | bytes 262176 | tf_op jit(solution)/shard_map/ppermute | solution.py:26
  17.4 3.8 %shard_map.113 = (bf16[4096,512]{1,0:T(8,128)(2,1)S(1)}, bf16[4096,512]{1,0:T(8,128)(2,1)S(1)}, bf16[16,4096]{1,0:T(8,128)(2,1)S(1)}, f32[8,128]{1,0:T(8,128)S(1...) custom-call(bf16[4096,512]{1,0:T(8,128)(2,1)} %refs_0_.1, bf16[4096,512]{1,0:T(8,128)(2,1)} %refs_1_.1, ...), custom_call_target="tpu_custom_call" | custom-call | tf_op jit(solution)/shard_map/pallas_call | solution.py:427
  23.3 0.9 %shard_map.117 = (f32[16,128]{1,0:T(8,128)S(1)}, f32[128,512]{1,0:T(8,128)S(1)}, f32[128,512]{1,0:T(8,128)S(1)}) custom-call(bf16[128,1024]{1,0:T(8,128)(2,1)S(1)} %get-tuple-element.60.refs_0_, bf16[128,1024]{1,0:T(8,128)(2,1)S(1)} %collective-permute-done.8.refs_1_, bf16[4096,512]{1,0:T(8,128)(2,1)S(1)} %get-tuple-element.31.refs_2_.refs_1_.refs_4_, ...), custom_call_target="tpu_custom_call" | custom-call | flops 603979776 | tf_op jit(solution)/shard_map/pallas_call | solution.py:368
  24.5 3.3 %collective-permute-done.3.refs_0_ = bf16[128,1024]{1,0:T(8,128)(2,1)S(1)} collective-permute-done((bf16[128,1024]{1,0:T(8,128)(2,1)S(1)}, bf16[128,1024]{1,0:T(8,128)(2,1)S(1)}, u32[]{:S(2)}, u32[]{:S(2)}) %collective-permute-start.3) | collective-permute-done | bytes 262176 | tf_op jit(solution)/shard_map/ppermute | solution.py:26
  28.7 3.1 %shard_map.118.refs_10_ = f32[4,128,256]{2,1,0:T(8,128)S(1)} custom-call(bf16[128,1024]{1,0:T(8,128)(2,1)S(1)} %slice.15.refs_0_, bf16[128,1024]{1,0:T(8,128)(2,1)S(1)} %collective-permute-done.9.refs_1_, bf16[128,1024]{1,0:T(8,128)(2,1)S(1)} %collective-permute-done.10.refs_2_, bf16[128,1024]{1,0:T(8,128)(2,1)S(1)} %collective-permute-done.11.refs_3_, ...), custom_call_target="tpu_custom_call" | custom-call | flops 1610612736 | tf_op jit(solution)/shard_map/pallas_call | solution.py:368
  31.8 2.4 %shard_map.119.refs_10_ = f32[4,128,256]{2,1,0:T(8,128)S(1)} custom-call(bf16[128,1024]{1,0:T(8,128)(2,1)S(1)} %collective-permute-done.6.refs_0_, bf16[128,1024]{1,0:T(8,128)(2,1)S(1)} %collective-permute-done.7.refs_1_, bf16[4096,512]{1,0:T(8,128)(2,1)S(1)} %get-tuple-element.31.refs_2_.refs_1_.refs_4_, ...), custom_call_target="tpu_custom_call" | custom-call | flops 1610612736 | tf_op jit(solution)/shard_map/pallas_call | solution.py:368
  34.3 2.5 %shard_map.120.refs_9_ = f32[4,128,256]{2,1,0:T(8,128)S(1)} custom-call(bf16[128,1024]{1,0:T(8,128)(2,1)S(1)} %collective-permute-done.3.refs_0_, bf16[128,1024]{1,0:T(8,128)(2,1)S(1)} %collective-permute-done.4.refs_1_, bf16[4096,512]{1,0:T(8,128)(2,1)S(1)} %get-tuple-element.31.refs_2_.refs_1_.refs_4_, ...), custom_call_target="tpu_custom_call" | custom-call | flops 1610612736 | tf_op jit(solution)/shard_map/pallas_call | solution.py:368
  36.8 2.1 %shard_map.121 = (bf16[272,128]{1,0:T(8,128)(2,1)S(1)}, bf16[272,128]{1,0:T(8,128)(2,1)S(1)}, bf16[272,128]{1,0:T(8,128)(2,1)S(1)}, bf16[272,128]{1,0:T(8,128)(2,1)S(1)}) custom-call(bf16[128,1024]{1,0:T(8,128)(2,1)S(1)} %collective-permute-done.1.refs_0_, bf16[4096,512]{1,0:T(8,128)(2,1)S(1)} %get-tuple-element.31.refs_2_.refs_1_.refs_4_, ...), custom_call_target="tpu_custom_call" | custom-call | flops 1610612736 | tf_op jit(solution)/shard_map/pallas_call | solution.py:368
  38.9 1.8 %collective-permute-start.12 = (bf16[272,128]{1,0:T(8,128)(2,1)S(1)}, bf16[272,128]{1,0:T(8,128)(2,1)S(1)}, u32[]{:S(2)}, u32[]{:S(2)}) collective-permute-start(bf16[272,128]{1,0:T(8,128)(2,1)S(1)} %get-tuple-element.50), channel_id=1, source_target_pairs={{0,4},{4,0},{8,12},{12,8},{16,20},{20,16},{24,28},{28,24},{1,5},{5... | collective-permute-start | bytes 208904 | tf_op jit(solution)/shard_map/ppermute | solution.py:26
  40.7 1.6 %collective-permute-start.13 = (bf16[272,128]{1,0:T(8,128)(2,1)S(1)}, bf16[272,128]{1,0:T(8,128)(2,1)S(1)}, u32[]{:S(2)}, u32[]{:S(2)}) collective-permute-start(bf16[272,128]{1,0:T(8,128)(2,1)S(1)} %get-tuple-element.51), channel_id=1, source_target_pairs={{0,8},{4,12},{8,0},{12,4},{16,24},{20,28},{24,16},{28,20},{1,9},{5... | collective-permute-start | bytes 208904 | tf_op jit(solution)/shard_map/ppermute | solution.py:26
  42.5 1.1 %collective-permute-done.12.refs_1_ = bf16[272,128]{1,0:T(8,128)(2,1)S(1)} collective-permute-done((bf16[272,128]{1,0:T(8,128)(2,1)S(1)}, bf16[272,128]{1,0:T(8,128)(2,1)S(1)}, u32[]{:S(2)}, u32[]{:S(2)}) %collective-permute-start.12) | collective-permute-done | bytes 69664 | tf_op jit(solution)/shard_map/ppermute | solution.py:26
  43.6 1.6 %collective-permute-done.13.refs_2_ = bf16[272,128]{1,0:T(8,128)(2,1)S(1)} collective-permute-done((bf16[272,128]{1,0:T(8,128)(2,1)S(1)}, bf16[272,128]{1,0:T(8,128)(2,1)S(1)}, u32[]{:S(2)}, u32[]{:S(2)}) %collective-permute-start.13) | collective-permute-done | bytes 69664 | tf_op jit(solution)/shard_map/ppermute | solution.py:26
  45.2 2.3 %collective-permute-done.14.refs_3_ = bf16[272,128]{1,0:T(8,128)(2,1)S(1)} collective-permute-done((bf16[272,128]{1,0:T(8,128)(2,1)S(1)}, bf16[272,128]{1,0:T(8,128)(2,1)S(1)}, u32[]{:S(2)}, u32[]{:S(2)}) %collective-permute-start.14) | collective-permute-done | bytes 69664 | tf_op jit(solution)/shard_map/ppermute | solution.py:26
  48.0 2.6 %collective-permute-start.15 = (bf16[144,128]{1,0:T(8,128)(2,1)S(1)}, bf16[144,128]{1,0:T(8,128)(2,1)S(1)}, u32[]{:S(2)}, u32[]{:S(2)}) collective-permute-start(bf16[144,128]{1,0:T(8,128)(2,1)S(1)} %get-tuple-element.55), channel_id=1, source_target_pairs={{0,16},{4,20},{8,24},{12,28},{16,0},{20,4},{24,8},{28,12},{1,17},{... | collective-permute-start | bytes 110600 | tf_op jit(solution)/shard_map/ppermute | solution.py:26
  50.7 2.7 %collective-permute-done.15.refs_0_ = bf16[144,128]{1,0:T(8,128)(2,1)S(1)} collective-permute-done((bf16[144,128]{1,0:T(8,128)(2,1)S(1)}, bf16[144,128]{1,0:T(8,128)(2,1)S(1)}, u32[]{:S(2)}, u32[]{:S(2)}) %collective-permute-start.15) | collective-permute-done | bytes 36896 | tf_op jit(solution)/shard_map/ppermute | solution.py:26
  53.9 1.5 %collective-permute-start.17 = (bf16[32,128]{1,0:T(8,128)(2,1)S(1)}, bf16[32,128]{1,0:T(8,128)(2,1)S(1)}, u32[]{:S(2)}, u32[]{:S(2)}) collective-permute-start(bf16[32,128]{1,0:T(8,128)(2,1)S(1)} %get-tuple-element.58), channel_id=1, source_target_pairs={{0,8},{4,12},{8,0},{12,4},{16,24},{20,28},{24,16},{28,20},{1,9},{5... | collective-permute-start | bytes 24584 | tf_op jit(solution)/shard_map/ppermute | solution.py:26
  55.5 1.8 %collective-permute-start.18 = (bf16[32,128]{1,0:T(8,128)(2,1)S(1)}, bf16[32,128]{1,0:T(8,128)(2,1)S(1)}, u32[]{:S(2)}, u32[]{:S(2)}) collective-permute-start(bf16[32,128]{1,0:T(8,128)(2,1)S(1)} %get-tuple-element.59), channel_id=1, source_target_pairs={{0,12},{4,8},{8,4},{12,0},{16,28},{20,24},{24,20},{28,16},{1,13},{... | collective-permute-start | bytes 24584 | tf_op jit(solution)/shard_map/ppermute | solution.py:26
  57.6 2.4 %collective-permute-done.18.refs_3_ = bf16[32,128]{1,0:T(8,128)(2,1)S(1)} collective-permute-done((bf16[32,128]{1,0:T(8,128)(2,1)S(1)}, bf16[32,128]{1,0:T(8,128)(2,1)S(1)}, u32[]{:S(2)}, u32[]{:S(2)}) %collective-permute-start.18) | collective-permute-done | bytes 8224 | tf_op jit(solution)/shard_map/ppermute | solution.py:26
  (30 shorter events, 6.3 us)
Async XLA Ops:
  1.6 10.2 %collective-permute-start.9 = (bf16[128,1024]{1,0:T(8,128)(2,1)S(1)}, bf16[128,1024]{1,0:T(8,128)(2,1)S(1)}, u32[]{:S(2)}, u32[]{:S(2)}) collective-permute-start(bf16[128,1024]{1,0:T(8,128)(2,1)S(1)} %slice.15.refs_0_), channel_id=1, source_target_pairs={{0,2},{1,3},{2,0},{3,1},{4,6},{5,7},{6,4},{7,5},{8,10},{9,11},{10,... | collective-permute-start | bytes 786440 | tf_op jit(solution)/shard_map/ppermute | solution.py:26
  5.8 6.0 %collective-permute-start.8 = (bf16[128,1024]{1,0:T(8,128)(2,1)S(1)}, bf16[128,1024]{1,0:T(8,128)(2,1)S(1)}, u32[]{:S(2)}, u32[]{:S(2)}) collective-permute-start(bf16[128,1024]{1,0:T(8,128)(2,1)S(1)} %get-tuple-element.60.refs_0_), channel_id=1, source_target_pairs={{0,1},{1,0},{2,3},{3,2},{4,5},{5,4},{6,7},{7,6},{8,9},{9,8},{10,11... | collective-permute-start | bytes 786440 | tf_op jit(solution)/shard_map/ppermute | solution.py:26
  5.9 7.9 %collective-permute-start.2 = (bf16[128,1024]{1,0:T(8,128)(2,1)S(1)}, bf16[128,1024]{1,0:T(8,128)(2,1)S(1)}, u32[]{:S(2)}, u32[]{:S(2)}) collective-permute-start(bf16[128,1024]{1,0:T(8,128)(2,1)S(1)} %get-tuple-element.62.refs_0_), channel_id=1, source_target_pairs={{0,1},{1,0},{2,3},{3,2},{4,5},{5,4},{6,7},{7,6},{8,9},{9,8},{10,11... | collective-permute-start | bytes 786440 | tf_op jit(solution)/shard_map/ppermute | solution.py:26
  6.4 11.0 %collective-permute-start = (bf16[128,1024]{1,0:T(8,128)(2,1)S(1)}, bf16[128,1024]{1,0:T(8,128)(2,1)S(1)}, u32[]{:S(2)}, u32[]{:S(2)}) collective-permute-start(bf16[128,1024]{1,0:T(8,128)(2,1)S(1)} %get-tuple-element.62.refs_0_), channel_id=1, source_target_pairs={{0,2},{1,3},{2,0},{3,1},{4,6},{5,7},{6,4},{7,5},{8,10},{9,11},{10,... | collective-permute-start | bytes 786440 | tf_op jit(solution)/shard_map/ppermute | solution.py:26
  6.4 16.6 %collective-permute-start.6 = (bf16[128,1024]{1,0:T(8,128)(2,1)S(1)}, bf16[128,1024]{1,0:T(8,128)(2,1)S(1)}, u32[]{:S(2)}, u32[]{:S(2)}) collective-permute-start(bf16[128,1024]{1,0:T(8,128)(2,1)S(1)} %get-tuple-element.60.refs_0_), channel_id=1, source_target_pairs={{0,2},{1,3},{2,0},{3,1},{4,6},{5,7},{6,4},{7,5},{8,10},{9,11},{10,... | collective-permute-start | bytes 786440 | tf_op jit(solution)/shard_map/ppermute | solution.py:26
  11.8 12.3 %collective-permute-start.5 = (bf16[128,1024]{1,0:T(8,128)(2,1)S(1)}, bf16[128,1024]{1,0:T(8,128)(2,1)S(1)}, u32[]{:S(2)}, u32[]{:S(2)}) collective-permute-start(bf16[128,1024]{1,0:T(8,128)(2,1)S(1)} %get-tuple-element.61.refs_0_), channel_id=1, source_target_pairs={{0,1},{1,0},{2,3},{3,2},{4,5},{5,4},{6,7},{7,6},{8,9},{9,8},{10,11... | collective-permute-start | bytes 786440 | tf_op jit(solution)/shard_map/ppermute | solution.py:26
  11.8 16.0 %collective-permute-start.3 = (bf16[128,1024]{1,0:T(8,128)(2,1)S(1)}, bf16[128,1024]{1,0:T(8,128)(2,1)S(1)}, u32[]{:S(2)}, u32[]{:S(2)}) collective-permute-start(bf16[128,1024]{1,0:T(8,128)(2,1)S(1)} %get-tuple-element.61.refs_0_), channel_id=1, source_target_pairs={{0,2},{1,3},{2,0},{3,1},{4,6},{5,7},{6,4},{7,5},{8,10},{9,11},{10,... | collective-permute-start | bytes 786440 | tf_op jit(solution)/shard_map/ppermute | solution.py:26
  13.8 14.8 %collective-permute-start.10 = (bf16[128,1024]{1,0:T(8,128)(2,1)S(1)}, bf16[128,1024]{1,0:T(8,128)(2,1)S(1)}, u32[]{:S(2)}, u32[]{:S(2)}) collective-permute-start(bf16[128,1024]{1,0:T(8,128)(2,1)S(1)} %slice.15.refs_0_), channel_id=1, source_target_pairs={{0,1},{1,0},{2,3},{3,2},{4,5},{5,4},{6,7},{7,6},{8,9},{9,8},{10,11... | collective-permute-start | bytes 786440 | tf_op jit(solution)/shard_map/ppermute | solution.py:26
  17.4 11.3 %collective-permute-start.11 = (bf16[128,1024]{1,0:T(8,128)(2,1)S(1)}, bf16[128,1024]{1,0:T(8,128)(2,1)S(1)}, u32[]{:S(2)}, u32[]{:S(2)}) collective-permute-start(bf16[128,1024]{1,0:T(8,128)(2,1)S(1)} %collective-permute-done.9.refs_1_), channel_id=1, source_target_pairs={{0,1},{1,0},{2,3},{3,2},{4,5},{5,4},{6,7},{7,6},{8,9},{9,8},{10,11... | collective-permute-start | bytes 786440 | tf_op jit(solution)/shard_map/ppermute | solution.py:26
  23.1 8.8 %collective-permute-start.7 = (bf16[128,1024]{1,0:T(8,128)(2,1)S(1)}, bf16[128,1024]{1,0:T(8,128)(2,1)S(1)}, u32[]{:S(2)}, u32[]{:S(2)}) collective-permute-start(bf16[128,1024]{1,0:T(8,128)(2,1)S(1)} %collective-permute-done.6.refs_0_), channel_id=1, source_target_pairs={{0,1},{1,0},{2,3},{3,2},{4,5},{5,4},{6,7},{7,6},{8,9},{9,8},{10,11... | collective-permute-start | bytes 786440 | tf_op jit(solution)/shard_map/ppermute | solution.py:26
  24.1 12.7 %collective-permute-start.1 = (bf16[128,1024]{1,0:T(8,128)(2,1)S(1)}, bf16[128,1024]{1,0:T(8,128)(2,1)S(1)}, u32[]{:S(2)}, u32[]{:S(2)}) collective-permute-start(bf16[128,1024]{1,0:T(8,128)(2,1)S(1)} %collective-permute-done.refs_0_), channel_id=1, source_target_pairs={{0,1},{1,0},{2,3},{3,2},{4,5},{5,4},{6,7},{7,6},{8,9},{9,8},{10,11... | collective-permute-start | bytes 786440 | tf_op jit(solution)/shard_map/ppermute | solution.py:26
  27.8 6.5 %collective-permute-start.4 = (bf16[128,1024]{1,0:T(8,128)(2,1)S(1)}, bf16[128,1024]{1,0:T(8,128)(2,1)S(1)}, u32[]{:S(2)}, u32[]{:S(2)}) collective-permute-start(bf16[128,1024]{1,0:T(8,128)(2,1)S(1)} %collective-permute-done.3.refs_0_), channel_id=1, source_target_pairs={{0,1},{1,0},{2,3},{3,2},{4,5},{5,4},{6,7},{7,6},{8,9},{9,8},{10,11... | collective-permute-start | bytes 786440 | tf_op jit(solution)/shard_map/ppermute | solution.py:26
  36.8 23.2 %copy-start = (bf16[128]{0:T(256)(128)(2,1)S(1)}, bf16[128]{0:T(256)(128)(2,1)}, u32[]{:S(2)}) copy-start(bf16[128]{0:T(256)(128)(2,1)} %param.19) | copy-start | bytes 772
  38.9 4.7 %collective-permute-start.12 = (bf16[272,128]{1,0:T(8,128)(2,1)S(1)}, bf16[272,128]{1,0:T(8,128)(2,1)S(1)}, u32[]{:S(2)}, u32[]{:S(2)}) collective-permute-start(bf16[272,128]{1,0:T(8,128)(2,1)S(1)} %get-tuple-element.50), channel_id=1, source_target_pairs={{0,4},{4,0},{8,12},{12,8},{16,20},{20,16},{24,28},{28,24},{1,5},{5... | collective-permute-start | bytes 208904 | tf_op jit(solution)/shard_map/ppermute | solution.py:26
  40.7 4.5 %collective-permute-start.13 = (bf16[272,128]{1,0:T(8,128)(2,1)S(1)}, bf16[272,128]{1,0:T(8,128)(2,1)S(1)}, u32[]{:S(2)}, u32[]{:S(2)}) collective-permute-start(bf16[272,128]{1,0:T(8,128)(2,1)S(1)} %get-tuple-element.51), channel_id=1, source_target_pairs={{0,8},{4,12},{8,0},{12,4},{16,24},{20,28},{24,16},{28,20},{1,9},{5... | collective-permute-start | bytes 208904 | tf_op jit(solution)/shard_map/ppermute | solution.py:26
  42.3 5.2 %collective-permute-start.14 = (bf16[272,128]{1,0:T(8,128)(2,1)S(1)}, bf16[272,128]{1,0:T(8,128)(2,1)S(1)}, u32[]{:S(2)}, u32[]{:S(2)}) collective-permute-start(bf16[272,128]{1,0:T(8,128)(2,1)S(1)} %get-tuple-element.52), channel_id=1, source_target_pairs={{0,12},{4,8},{8,4},{12,0},{16,28},{20,24},{24,20},{28,16},{1,13},{... | collective-permute-start | bytes 208904 | tf_op jit(solution)/shard_map/ppermute | solution.py:26
  48.0 5.3 %collective-permute-start.15 = (bf16[144,128]{1,0:T(8,128)(2,1)S(1)}, bf16[144,128]{1,0:T(8,128)(2,1)S(1)}, u32[]{:S(2)}, u32[]{:S(2)}) collective-permute-start(bf16[144,128]{1,0:T(8,128)(2,1)S(1)} %get-tuple-element.55), channel_id=1, source_target_pairs={{0,16},{4,20},{8,24},{12,28},{16,0},{20,4},{24,8},{28,12},{1,17},{... | collective-permute-start | bytes 110600 | tf_op jit(solution)/shard_map/ppermute | solution.py:26
  53.8 3.7 %collective-permute-start.16 = (bf16[32,128]{1,0:T(8,128)(2,1)S(1)}, bf16[32,128]{1,0:T(8,128)(2,1)S(1)}, u32[]{:S(2)}, u32[]{:S(2)}) collective-permute-start(bf16[32,128]{1,0:T(8,128)(2,1)S(1)} %get-tuple-element.57), channel_id=1, source_target_pairs={{0,4},{4,0},{8,12},{12,8},{16,20},{20,16},{24,28},{28,24},{1,5},{5... | collective-permute-start | bytes 24584 | tf_op jit(solution)/shard_map/ppermute | solution.py:26
  53.9 3.7 %collective-permute-start.17 = (bf16[32,128]{1,0:T(8,128)(2,1)S(1)}, bf16[32,128]{1,0:T(8,128)(2,1)S(1)}, u32[]{:S(2)}, u32[]{:S(2)}) collective-permute-start(bf16[32,128]{1,0:T(8,128)(2,1)S(1)} %get-tuple-element.58), channel_id=1, source_target_pairs={{0,8},{4,12},{8,0},{12,4},{16,24},{20,28},{24,16},{28,20},{1,9},{5... | collective-permute-start | bytes 24584 | tf_op jit(solution)/shard_map/ppermute | solution.py:26
  55.5 4.5 %collective-permute-start.18 = (bf16[32,128]{1,0:T(8,128)(2,1)S(1)}, bf16[32,128]{1,0:T(8,128)(2,1)S(1)}, u32[]{:S(2)}, u32[]{:S(2)}) collective-permute-start(bf16[32,128]{1,0:T(8,128)(2,1)S(1)} %get-tuple-element.59), channel_id=1, source_target_pairs={{0,12},{4,8},{8,4},{12,0},{16,28},{20,24},{24,20},{28,16},{1,13},{... | collective-permute-start | bytes 24584 | tf_op jit(solution)/shard_map/ppermute | solution.py:26
